TPU v7x, 128 devices: a whole 4x4x4 slice. The times are simulated.
128 devices in a mesh: sp: 32 (over z, y, core), tp: 4 (over x).
Axes of the slice: x: 4, y: 4, z: 4, core: 2. Of those that a mesh axis runs over, the one named last changes fastest.
Arguments:
- tokens: bfloat16 [12288, 2048], P('sp', 'tp'), may hold values from -6 to 6
- norm_gain: float32 [2048], replicated, may hold values from 0.1 to 1.9
- w_query_down: bfloat16 [2048, 512], replicated, may hold values from -0.125 to 0.125
- query_gain: float32 [512], replicated, may hold values from 0.1 to 1.9
- w_query_up: bfloat16 [512, 1536], P(None, 'tp'), may hold values from -0.25 to 0.25
- w_latent_down: bfloat16 [2048, 256], replicated, may hold values from -0.125 to 0.125
- latent_gain: float32 [256], replicated, may hold values from 0.1 to 1.9
- w_rotary_key: bfloat16 [2048, 32], replicated, may hold values from -0.125 to 0.125
- w_latent_up: bfloat16 [256, 2048], P(None, 'tp'), may hold values from -0.375 to 0.375
- query_head_gain: float32 [96], replicated, may hold values from 0.1 to 1.9
- key_head_gain: float32 [96], replicated, may hold values from 0.1 to 1.9
- w_pool_in: bfloat16 [2048, 1024], P(None, 'tp'), may hold values from -0.125 to 0.125
- w_pool_mix: bfloat16 [4, 256, 256], P('tp'), may hold values from -0.375 to 0.375
- pool_scale: float32 [1024], P('tp'), may hold values from 0.1 to 1.9
- w_attn_out: bfloat16 [1024, 2048], P('tp'), may hold values from -12 to 12
- w_pool_out: bfloat16 [1024, 2048], P('tp'), may hold values from -0.5 to 0.5
- w_gate_attn: bfloat16 [2048, 2048], P(None, 'tp'), may hold values from -0.125 to 0.125
- w_gate_pool: bfloat16 [2048, 2048], P(None, 'tp'), may hold values from -0.125 to 0.125
Outputs:
- mixed: bfloat16 [12288, 2048], P('sp', 'tp')
All inputs are finite; a program needn't handle non-finite values.
Results may differ from a plain program's by a relative error of at most 0.02.
Values may be sent and summed in bfloat16 or wider, within the bound.
No kernel may reach another device: no remote copies, remote signals or barrier semaphores. Data moves between devices by JAX's collectives and lax.ppermute only.
A program may use at most 128 MiB of HBM per device.

v0:
```python
import functools
import math

import jax
import jax.numpy as jnp
from jax import lax
from jax.experimental import pallas as pl
from jax.experimental.pallas import tpu as pltpu
from jax.sharding import PartitionSpec as P


NOPE = 64
ROPE = 32
VALUE_DIM = 64
HEAD = NOPE + ROPE
LATENT = 256
REACH = 8
eps = 1e-06
theta = 10000.0
bf = jnp.bfloat16
f32 = jnp.float32

PAY = LATENT + ROPE + 16
ACC = VALUE_DIM + 16


def sp_of(z, y, c):
    return (z % 4) * 8 + (y % 4) * 2 + c


SITES = [(z, y, c) for z in range(4) for y in range(4) for c in range(2)]
SWAP = [(sp_of(z, y, c), sp_of(z, y, 1 - c)) for z, y, c in SITES]


def along(step, second):
    pairs = []
    for z, y, c in SITES:
        on_z = (c == 0) != second
        pairs.append((sp_of(z, y, c), sp_of(z + step, y, c) if on_z else sp_of(z, y + step, c)))
    return pairs


def ring(step):
    return [(i, (i + step) % 4) for i in range(4)]


def params(mib=56):
    return pltpu.CompilerParams(vmem_limit_bytes=mib * 2**20)


VM = pl.BlockSpec(memory_space=pltpu.VMEM)
SM = pl.BlockSpec(memory_space=pltpu.SMEM)


def gained(x, gain):
    return (x * gain).astype(bf)


def project_kernel(ids, *refs, count, seeded):
    xs, refs = refs[:count], refs[count:]
    gains, refs = refs[:count], refs[count:]
    weights, refs = refs[: 6 * count], refs[6 * count :]
    seeds, outs = (refs[:7], refs[7:]) if seeded else ((), refs)
    sums = [s[...] for s in seeds] if seeded else [None] * 7
    values = [x[...].astype(f32) for x in xs]
    square = sum(jnp.sum(x * x, axis=-1, keepdims=True) for x in values)
    square = jnp.broadcast_to(square, outs[0].shape)
    outs[0][...] = square if sums[0] is None else sums[0] + square
    ns = [gained(x, g[0]) for x, g in zip(values, gains)]
    for i in range(6):
        total = sums[i + 1]
        for k in range(count):
            w = weights[6 * k + i][...]
            if i == 1:
                part = lax.dot_general(w, ns[k], (((1,), (1,)), ((), ())), preferred_element_type=f32)
            else:
                part = jnp.dot(ns[k], w, preferred_element_type=f32)
            total = part if total is None else total + part
        outs[i + 1][...] = total


def last_piece(xa, xb, gain):
    x = jnp.concatenate([xa[...], xb[...]], axis=0).astype(f32)
    return x, gained(x, gain[0])


def front_kernel(ids, xa, xb, gain, wl, wr, square, lat0, raw0, lgain, kgain, cos, sin, pay, scale_out):
    x, n = last_piece(xa, xb, gain)
    total = square[...] + jnp.broadcast_to(jnp.sum(x * x, axis=-1, keepdims=True), square.shape)
    scale = lax.rsqrt(total * (1.0 / 2048) + eps)
    scale_out[...] = scale
    lat = lat0[...] + jnp.dot(n, wl[...], preferred_element_type=f32)
    lat = jnp.transpose(lat * scale[:, :1]).astype(bf).astype(f32)
    lat = lat * lax.rsqrt(jnp.mean(lat * lat, axis=0, keepdims=True) + eps) * lgain[...]
    pay[:LATENT, :] = lat.astype(bf)
    raw = raw0[...] + lax.dot_general(wr[...], n, (((1,), (1,)), ((), ())), preferred_element_type=f32)
    raw = (raw * jnp.transpose(scale)[:1]).astype(bf).astype(f32)
    total = jnp.sum(raw * raw, axis=0, keepdims=True)
    k = raw * kgain[...]
    first, second = k[:16], k[16:]
    pay[LATENT : LATENT + 16, :] = (first * cos[...] - second * sin[...]).astype(bf)
    pay[LATENT + 16 : LATENT + 32, :] = (first * sin[...] + second * cos[...]).astype(bf)
    pay[LATENT + 32 :, :] = jnp.broadcast_to(total, (16, total.shape[1])).astype(bf)


def query_kernel(ids, xa, xb, gain, wqd, wpi, scale, lat0, pool0, qgain, wqu, hgain, cos, sin, q, pool_in):
    _, n = last_piece(xa, xb, gain)
    s = scale[:, :1]
    pool_in[...] = ((pool0[...] + jnp.dot(n, wpi[...], preferred_element_type=f32)) * s).astype(bf)
    lat = (lat0[...] + jnp.dot(n, wqd[...], preferred_element_type=f32)) * s
    lat = lat.astype(bf).astype(f32)
    lat = lat * lax.rsqrt(jnp.mean(lat * lat, axis=-1, keepdims=True) + eps) * qgain[...]
    raw = jnp.dot(lat.astype(bf), wqu[...], preferred_element_type=f32)
    raw = jnp.transpose(raw).astype(bf).astype(f32)
    for h in range(raw.shape[0] // HEAD):
        v = raw[h * HEAD : (h + 1) * HEAD]
        v = v * lax.rsqrt(jnp.mean(v * v, axis=0, keepdims=True) + eps) * hgain[...]
        v = v * (HEAD**-0.5 / math.log(2.0))
        first, second = v[NOPE : NOPE + 16], v[NOPE + 16 :]
        q[h, :NOPE, :] = v[:NOPE].astype(bf)
        q[h, NOPE : NOPE + 16, :] = (first * cos[...] - second * sin[...]).astype(bf)
        q[h, NOPE + 16 :, :] = (first * sin[...] + second * cos[...]).astype(bf)


def gate_kernel(ids, xa, xb, gain, wa, wp, scale, a0, p0, gate_a, gate_p):
    _, n = last_piece(xa, xb, gain)
    s = scale[:, :1]
    gate_a[...] = jax.nn.sigmoid((a0[...] + jnp.dot(n, wa[...], preferred_element_type=f32)) * s)
    gate_p[...] = jax.nn.sigmoid((p0[...] + jnp.dot(n, wp[...], preferred_element_type=f32)) * s)


def columns_kernel(ids, wa, wp, *outs):
    for d in range(4):
        at = pl.multiple_of(ids[4 + d] * 512, 512)
        outs[d][:256, :] = wa[:, pl.ds(at, 512)]
        outs[d][256:, :] = wp[:, pl.ds(at, 512)]


def join_kernel(a, b, c, d, out):
    width = a.shape[1]
    for i, x in enumerate((a, b, c, d)):
        out[:, i * width : (i + 1) * width] = x[...]


def pool_merge_kernel(p0, p1, p2, p3, w0, w1, w2, w3, gate, out):
    total = None
    for p, w in ((p0, w0), (p1, w1), (p2, w2), (p3, w3)):
        part = jnp.dot(p[...], w[256:, :], preferred_element_type=f32)
        total = part if total is None else total + part
    out[...] = gate[...] * total


def pool_kernel(ids, before, x, after, mix, scale, out, padded):
    rows = x.shape[0]
    length = ids[2]
    half = ids[1]
    padded[0:REACH, :] = before[...].astype(f32)
    padded[REACH : REACH + rows, :] = x[...].astype(f32)
    padded[REACH + rows :, :] = after[...].astype(f32)
    total = jnp.zeros((rows, x.shape[1]), f32)
    for shift in range(-REACH, REACH):
        inside = (shift >= -half) & (shift <= half - 1)
        total = total + jnp.where(inside, padded[REACH + shift : REACH + shift + rows, :], 0.0)
    at = ids[0] * rows + lax.broadcasted_iota(jnp.int32, (rows, 1), 0)
    count = (jnp.clip(at + half, 0, length) - jnp.clip(at - half, 0, length)).astype(f32)
    mixed = (total / count - padded[REACH : REACH + rows, :]).astype(bf)
    out[...] = (jnp.dot(mixed, mix[...], preferred_element_type=f32) * scale[...]).astype(bf)


def attend_kernel(*refs, pieces, seeded):
    q0, q1, wk, wv, gain = refs[:5]
    refs = refs[5:]
    n_in = sum(len(p) for p in pieces)
    blocks = refs[:n_in]
    refs = refs[n_in:]
    seeds, outs = (refs[:2], refs[2:]) if seeded else ((), refs)
    heads = q0.shape[0]
    half = q0.shape[2]
    at = 0
    for number, piece in enumerate(pieces):
        parts = [blocks[at + i] for i in range(len(piece))]
        at += len(piece)
        whole = parts[0][...] if len(parts) == 1 else jnp.concatenate([p[...] for p in parts], axis=0)
        keys = whole.shape[1]
        latent = whole[:LATENT]
        rope = whole[LATENT : LATENT + ROPE].astype(f32)
        square = whole[LATENT + ROPE :].astype(f32)[0:1]
        unrotated = jnp.dot(wk[...], latent, preferred_element_type=f32)
        values = jnp.dot(wv[...], latent, preferred_element_type=f32).astype(bf)
        row = lax.broadcasted_iota(jnp.int32, (16, keys), 0)
        ones = jnp.where(row == 0, 1.0, 0.0).astype(bf)
        for h in range(heads):
            k = unrotated[h * NOPE : (h + 1) * NOPE]
            scale = lax.rsqrt((jnp.sum(k * k, axis=0, keepdims=True) + square) * (1.0 / HEAD) + eps)
            key = jnp.concatenate([(k * gain[...] * scale).astype(bf), (rope * scale).astype(bf)], axis=0)
            query = jnp.concatenate([q0[h], q1[h]], axis=1)
            scores = lax.dot_general(key, query, (((0,), (0,)), ((), ())), preferred_element_type=f32)
            weights = jnp.exp2(scores).astype(bf)
            v = jnp.concatenate([values[h * VALUE_DIM : (h + 1) * VALUE_DIM], ones], axis=0)
            add = jnp.dot(v, weights, preferred_element_type=f32)
            for i in range(2):
                part = add[:, i * half : (i + 1) * half]
                if number > 0:
                    outs[i][h] += part
                elif seeded:
                    outs[i][h] = seeds[i][h] + part
                else:
                    outs[i][h] = part


def attend(q0, q1, wk, wv, gain, pieces, seeds):
    heads, _, half = q0.shape
    shape = jax.ShapeDtypeStruct((heads, ACC, half), f32)
    arrays = [a for p in pieces for a in p]
    keys = sum(p[0].shape[1] for p in pieces)
    kernel = functools.partial(
        attend_kernel, pieces=[[None] * len(p) for p in pieces], seeded=seeds is not None
    )
    return pl.pallas_call(
        kernel,
        in_specs=[VM] * (5 + len(arrays) + (2 if seeds else 0)),
        out_specs=[VM, VM],
        out_shape=[shape, shape],
        compiler_params=params(),
        cost_estimate=pl.CostEstimate(
            flops=keys * heads * 2 * half * 2 * 512,
            transcendentals=keys * heads * 2 * half,
            bytes_accessed=keys * PAY * 2,
        ),
    )(q0, q1, wk, wv, gain, *arrays, *(seeds or ()))


def finish_kernel(mine, other, out):
    for h in range(mine.shape[0]):
        both = mine[h] + other[h]
        out[h * VALUE_DIM : (h + 1) * VALUE_DIM, :] = (
            both[:VALUE_DIM] / both[VALUE_DIM : VALUE_DIM + 1]
        ).astype(bf)


def merge_kernel(a0, a1, a2, a3, w0, w1, w2, w3, gate, pool, out):
    total = None
    for a, w in ((a0, w0), (a1, w1), (a2, w2), (a3, w3)):
        part = lax.dot_general(a[...], w[:256, :], (((0,), (0,)), ((), ())), preferred_element_type=f32)
        total = part if total is None else total + part
    out[...] = (gate[...] * total + pool[...]).astype(bf)


def call(kernel, ins, specs, shapes, flops, scratch=()):
    return pl.pallas_call(
        kernel,
        in_specs=specs,
        out_specs=jax.tree.map(lambda _: VM, shapes),
        out_shape=shapes,
        scratch_shapes=scratch,
        compiler_params=params(),
        cost_estimate=pl.CostEstimate(flops=flops, transcendentals=0, bytes_accessed=2**20),
    )(*ins)


def picked(kernel, ids, ins, shapes, flops):
    arrays, specs = [], []
    for a in ins:
        if isinstance(a, tuple):
            a, number, axis = a
            if axis is None:
                specs.append(pl.BlockSpec((1, 1, 512), lambda i, p, n=number: (p[n], 0, 0)))
            elif axis == 0:
                specs.append(pl.BlockSpec((512, a.shape[1]), lambda i, p, n=number: (p[n], 0)))
            else:
                specs.append(pl.BlockSpec((a.shape[0], 512), lambda i, p, n=number: (0, p[n])))
        else:
            specs.append(pl.BlockSpec(a.shape, lambda i, p, r=a.ndim: (0,) * r))
        arrays.append(a)
    return pl.pallas_call(
        kernel,
        grid_spec=pltpu.PrefetchScalarGridSpec(
            num_scalar_prefetch=1,
            grid=(1,),
            in_specs=specs,
            out_specs=[pl.BlockSpec(s.shape, lambda i, p, r=len(s.shape): (0,) * r) for s in shapes],
        ),
        out_shape=shapes,
        compiler_params=params(),
        cost_estimate=pl.CostEstimate(flops=flops, transcendentals=0, bytes_accessed=2**20),
    )(ids, *arrays)


def whole(
    tokens,
    norm_gain,
    w_query_down,
    query_gain,
    w_query_up,
    w_latent_down,
    latent_gain,
    w_rotary_key,
    w_latent_up,
    query_head_gain,
    key_head_gain,
    w_pool_in,
    w_pool_mix,
    pool_scale,
    w_attn_out,
    w_pool_out,
    w_gate_attn,
    w_gate_pool,
):
    S = jax.ShapeDtypeStruct
    rows = tokens.shape[0]
    heads = w_query_up.shape[1] // HEAD
    length = rows * lax.axis_size("sp")
    here = lax.axis_index("sp")
    t = lax.axis_index("tp")

    x1 = lax.ppermute(tokens, "tp", ring(1))
    x2 = lax.ppermute(tokens, "tp", ring(-1))
    xa = lax.ppermute(x1[: rows // 2], "tp", ring(1))
    xb = lax.ppermute(x2[rows // 2 :], "tp", ring(-1))

    half = ROPE // 2
    freqs = theta ** (-jnp.arange(half, dtype=f32) / half)
    positions = (here * rows + jnp.arange(rows, dtype=jnp.int32)).astype(f32)
    angles = freqs[:, None] * positions[None, :]
    cos, sin = jnp.cos(angles), jnp.sin(angles)
    ids = (t + jnp.array([0, 3, 1, 2, 0, 1, 2, 3], jnp.int32)) % 4
    up = w_latent_up.reshape(LATENT, heads, NOPE + VALUE_DIM)
    wk = jnp.transpose(up[:, :, :NOPE].reshape(LATENT, heads * NOPE))
    wv = jnp.transpose(up[:, :, NOPE:].reshape(LATENT, heads * VALUE_DIM))
    gain = norm_gain.reshape(4, 1, 512)
    wr = w_rotary_key.T

    def rows_of(n):
        return [(w_latent_down, n, 0), (wr, n, 1), (w_query_down, n, 0), (w_pool_in, n, 0),
                (w_gate_attn, n, 0), (w_gate_pool, n, 0)]

    sums = [S((rows, 128), f32), S((rows, 256), f32), S((ROPE, rows), f32), S((rows, 512), f32),
            S((rows, 256), f32), S((rows, 512), f32), S((rows, 512), f32)]
    own = picked(
        functools.partial(project_kernel, count=1, seeded=False),
        ids, [tokens, (gain, 0, None), *rows_of(0)], sums, 8 * 10**8,
    )
    near = picked(
        functools.partial(project_kernel, count=2, seeded=True),
        ids,
        [x1, x2, (gain, 1, None), (gain, 2, None), *rows_of(1), *rows_of(2), *own],
        sums, 16 * 10**8,
    )
    square, lat0, raw0, query0, pool0, attn0, gate0 = near
    last = [xa, xb, (gain, 3, None)]

    pay, scale = picked(
        front_kernel,
        ids,
        [*last, (w_latent_down, 3, 0), (wr, 3, 1), square, lat0, raw0, latent_gain[:, None],
         key_head_gain[NOPE:, None], cos, sin],
        [S((PAY, rows), bf), S((rows, 128), f32)],
        3 * 10**8,
    )

    cut = PAY // 2
    a1 = lax.ppermute(pay, "sp", along(1, False))
    a2 = lax.ppermute(pay, "sp", along(-1, False))
    a3 = lax.ppermute(pay, "sp", along(2, False))

    q, pool_in = picked(
        query_kernel,
        ids,
        [*last, (w_query_down, 3, 0), (w_pool_in, 3, 0), scale, query0, pool0, query_gain[None, :],
         w_query_up, query_head_gain[:, None], cos, sin],
        [S((heads, HEAD, rows), bf), S((rows, 256), bf)],
        10**9,
    )
    q_other = lax.ppermute(q, "sp", SWAP)

    def attend_on(pieces, seeds):
        return attend(q, q_other, wk, wv, key_head_gain[:NOPE, None], pieces, seeds)

    line = call(join_kernel, (pay, a1, a2, a3), [VM] * 4, S((PAY, 4 * rows), bf), 10**7)
    b1 = lax.ppermute(line, "sp", along(1, True))
    b2 = lax.ppermute(line, "sp", along(-1, True))
    b3 = lax.ppermute(b1[:cut], "sp", along(1, True))
    b4 = lax.ppermute(b2[cut:], "sp", along(-1, True))
    acc = attend_on([[line]], None)
    acc = attend_on([[b1], [b2]], acc)
    acc = attend_on([[b3, b4]], acc)

    count = lax.axis_size("sp")
    before = lax.ppermute(pool_in[rows - REACH :], "sp", [(i, i + 1) for i in range(count - 1)])
    after = lax.ppermute(pool_in[:REACH], "sp", [(i + 1, i) for i in range(count - 1)])
    pool_ids = jnp.stack([here, jnp.left_shift(1, t), jnp.int32(length)]).astype(jnp.int32)
    pool = call(
        pool_kernel,
        (pool_ids, before, pool_in, after, w_pool_mix[0], pool_scale[None, :]),
        [SM] + [VM] * 5,
        S((rows, 256), bf),
        10**8,
        [pltpu.VMEM((rows + 2 * REACH, 256), f32)],
    )
    pools = [pool] + [lax.ppermute(pool, "tp", ring(d)) for d in (1, 2, 3)]

    weights = call(columns_kernel, (ids, w_attn_out, w_pool_out), [SM, VM, VM], [S((512, 512), bf)] * 4, 10**7)
    weights = [weights[0]] + [lax.ppermute(weights[d], "tp", ring(d)) for d in (1, 2, 3)]

    gate_attn, gate_pool = picked(
        gate_kernel,
        ids,
        [*last, (w_gate_attn, 3, 0), (w_gate_pool, 3, 0), scale, attn0, gate0],
        [S((rows, 512), f32)] * 2,
        5 * 10**8,
    )
    pool_branch = call(pool_merge_kernel, (*pools, *weights, gate_pool), [VM] * 9, S((rows, 512), f32), 10**9)

    other = lax.ppermute(acc[1], "sp", SWAP)
    attn = call(finish_kernel, (acc[0], other), [VM, VM], S((heads * VALUE_DIM, rows), bf), 10**7)
    attns = [attn] + [lax.ppermute(attn, "tp", ring(d)) for d in (1, 2, 3)]
    return call(merge_kernel, (*attns, *weights, gate_attn, pool_branch), [VM] * 10, S((rows, 512), bf), 10**9)


def solution(mesh):
    placed = (
        P("sp", "tp"),
        P(),
        P(),
        P(),
        P(None, "tp"),
        P(),
        P(),
        P(),
        P(None, "tp"),
        P(),
        P(),
        P(None, "tp"),
        P("tp", None, None),
        P("tp"),
        P("tp", None),
        P("tp", None),
        P(None, "tp"),
        P(None, "tp"),
    )
    return jax.shard_map(whole, mesh=mesh, in_specs=placed, out_specs=P("sp", "tp"), check_vma=False)
```

profile of v0, /device:TPU:0, one launch (start us, length us, event | category | flops | bytes accessed | tf_op | source)
XLA Modules:
  0.0 136.3 jit_solution(1712373683529203007)
XLA Ops:
  8.1 4.1 %collective-permute-done.refs_0_ = bf16[384,512]{1,0:T(8,128)(2,1)S(1)} collective-permute-done((bf16[384,512]{1,0:T(8,128)(2,1)}, bf16[384,512]{1,0:T(8,128)(2,1)S(1)}, u32[]{:S(2)}, u32[]{:S(2)}) %collective-permute-start) | collective-permute-done | bytes 393248 | tf_op jit(solution)/shard_map/ppermute | solution.py:316
  12.8 2.8 %collective-permute-start.3 = (bf16[192,512]{1,0:T(8,128)(2,1)S(1)}, bf16[192,512]{1,0:T(8,128)(2,1)S(1)}, u32[]{:S(2)}, u32[]{:S(2)}) collective-permute-start(bf16[192,512]{1,0:T(8,128)(2,1)S(1)} %slice.43), channel_id=1, source_target_pairs={{0,3},{1,0},{2,1},{3,2},{4,7},{5,4},{6,5},{7,6},{8,11},{9,8},{10,9... | collective-permute-start | bytes 589832 | tf_op jit(solution)/shard_map/ppermute | solution.py:319
  15.6 4.6 %shard_map.181 = (f32[384,128]{1,0:T(8,128)}, f32[384,256]{1,0:T(8,128)}, f32[32,384]{1,0:T(8,128)}, f32[384,512]{1,0:T(8,128)}, f32[384,256]{1,0:T(8,128)}, /*index=5*/f32[384,512]{1,0:T(8,128)}, f32[384,512]{1,0:T(8,128)}) custom-call(s32[8]{0:T(128)} %and_select_fusion.ids, bf16[384,512]{1,0:T(8,128)(2,1)} %refs_0_.1, f32[4,1,512]{2,1,0:T(1,128)} %bitcast.25, ...), custom_call_target="tpu_custom_call" | custom-call | flops 800000000 | bytes 1048576 | tf_op jit(solution)/shard_map/pallas_call | solution.py:275
  20.2 7.3 %shard_map.182 = (f32[384,128]{1,0:T(8,128)}, f32[384,256]{1,0:T(8,128)}, f32[32,384]{1,0:T(8,128)}, f32[384,512]{1,0:T(8,128)}, f32[384,256]{1,0:T(8,128)}, /*index=5*/f32[384,512]{1,0:T(8,128)}, f32[384,512]{1,0:T(8,128)}) custom-call(s32[8]{0:T(128)} %and_select_fusion.ids, bf16[384,512]{1,0:T(8,128)(2,1)} %copy-done.5, bf16[384,512]{1,0:T(8,128)(2,1)} %copy-done.6, ...), custom_call_target="tpu_custom_call" | custom-call | flops 1600000000 | bytes 1048576 | tf_op jit(solution)/shard_map/pallas_call | solution.py:275
  28.3 3.4 %shard_map.183 = (bf16[304,384]{1,0:T(8,128)(2,1)}, f32[384,128]{1,0:T(8,128)}) custom-call(s32[8]{0:T(128)} %and_select_fusion.ids, bf16[192,512]{1,0:T(8,128)(2,1)} %copy-done.3, bf16[192,512]{1,0:T(8,128)(2,1)} %copy-done.4, f32[4,1,512]{2,1,0:T(1,128)} %bitcast.28, bf16[2048,256]{1,0:T(8,128)(2,1)} %wl.1, bf16[32,2048]{1,0:T(8,128)(2,1)} %bitcast.23, ...), custom_call_target="tpu_custom_call" | custom-call | flops 300000000 | bytes 1048576 | tf_op jit(solution)/shard_map/pallas_call | solution.py:275
  31.8 2.1 %collective-permute-start.5 = (bf16[304,384]{1,0:T(8,128)(2,1)}, bf16[304,384]{1,0:T(8,128)(2,1)S(1)}, u32[]{:S(2)}, u32[]{:S(2)}) collective-permute-start(bf16[304,384]{1,0:T(8,128)(2,1)} %get-tuple-element.49.a), channel_id=1, source_target_pairs={{0,32},{4,12},{8,40},{12,20},{16,48},{20,28},{24,56},{28,4},{32,64... | collective-permute-start | bytes 700424 | tf_op jit(solution)/shard_map/ppermute | solution.py:362
  33.9 2.2 %collective-permute-start.6 = (bf16[304,384]{1,0:T(8,128)(2,1)}, bf16[304,384]{1,0:T(8,128)(2,1)S(1)}, u32[]{:S(2)}, u32[]{:S(2)}) collective-permute-start(bf16[304,384]{1,0:T(8,128)(2,1)} %get-tuple-element.49.a), channel_id=1, source_target_pairs={{0,96},{4,28},{8,104},{12,4},{16,112},{20,12},{24,120},{28,20},{32... | collective-permute-start | bytes 700424 | tf_op jit(solution)/shard_map/ppermute | solution.py:363
  37.9 3.1 %shard_map.190 = (bf16[512,512]{1,0:T(8,128)(2,1)}, bf16[512,512]{1,0:T(8,128)(2,1)}, bf16[512,512]{1,0:T(8,128)(2,1)}, bf16[512,512]{1,0:T(8,128)(2,1)}) custom-call(s32[8]{0:T(128)} %and_select_fusion.ids, bf16[256,2048]{1,0:T(8,128)(2,1)} %wa.2, bf16[256,2048]{1,0:T(8,128)(2,1)} %wp.2), custom_call_target="tpu_custom_call" | custom-call | flops 10000000 | bytes 1048576 | tf_op jit(solution)/shard_map/pallas_call | solution.py:250
  41.7 2.5 %collective-permute-done.7.d = bf16[304,384]{1,0:T(8,128)(2,1)S(1)} collective-permute-done((bf16[304,384]{1,0:T(8,128)(2,1)}, bf16[304,384]{1,0:T(8,128)(2,1)S(1)}, u32[]{:S(2)}, u32[]{:S(2)}) %collective-permute-start.7) | collective-permute-done | bytes 233504 | tf_op jit(solution)/shard_map/ppermute | solution.py:364
  44.9 2.3 %shard_map.185.refs_5_ = bf16[304,1536]{1,0:T(8,128)(2,1)} custom-call(bf16[304,384]{1,0:T(8,128)(2,1)} %get-tuple-element.49.a, bf16[304,384]{1,0:T(8,128)(2,1)} %copy-done.9, bf16[304,384]{1,0:T(8,128)(2,1)} %copy-done.10, bf16[304,384]{1,0:T(8,128)(2,1)} %copy-done.11), custom_call_target="tpu_custom_call" | custom-call | flops 10000000 | bytes 1048576 | tf_op jit(solution)/shard_map/pallas_call | solution.py:250
  50.5 4.5 %shard_map.184 = (bf16[4,96,384]{2,1,0:T(8,128)(2,1)}, bf16[384,256]{1,0:T(8,128)(2,1)}) custom-call(s32[8]{0:T(128)} %and_select_fusion.ids, bf16[192,512]{1,0:T(8,128)(2,1)} %copy-done.3, bf16[192,512]{1,0:T(8,128)(2,1)} %copy-done.4, f32[4,1,512]{2,1,0:T(1,128)} %bitcast.29, bf16[2048,512]{1,0:T(8,128)(2,1)} %wqd.1, bf16[2048,256]{1,0:T(8,128)(2,1)} %wpi.1, ...), custom_call_target="tpu_custom_call" | custom-call | flops 1000000000 | bytes 1048576 | tf_op jit(solution)/shard_map/pallas_call | solution.py:275
  57.6 7.2 %shard_map.186 = (f32[4,80,384]{2,1,0:T(8,128)}, f32[4,80,384]{2,1,0:T(8,128)}) custom-call(bf16[4,96,384]{2,1,0:T(8,128)(2,1)} %get-tuple-element.48.refs_0_, bf16[4,96,384]{2,1,0:T(8,128)(2,1)} %copy-done.27, bf16[256,256]{1,0:T(8,128)(2,1)} %bitcast.35, bf16[256,256]{1,0:T(8,128)(2,1)} %bitcast.32, f32[64,1]{1,0:T(8,128)} %copy.34.refs_4_, ...), custom_call_target="tpu_custom_call" | custom-call | flops 4831838208 | bytes 933888 | tf_op jit(solution)/shard_map/pallas_call | solution.py:219
  65.3 2.9 %collective-permute-start.11 = (bf16[152,1536]{1,0:T(8,128)(2,1)S(1)}, bf16[152,1536]{1,0:T(8,128)(2,1)S(1)}, u32[]{:S(2)}, u32[]{:S(2)}) collective-permute-start(bf16[152,1536]{1,0:T(8,128)(2,1)S(1)} %slice.47), channel_id=1, source_target_pairs={{0,24},{4,100},{8,0},{12,108},{16,8},{20,116},{24,16},{28,124},{32... | collective-permute-start | bytes 1400840 | tf_op jit(solution)/shard_map/ppermute | solution.py:383
  68.2 12.2 %shard_map.187 = (f32[4,80,384]{2,1,0:T(8,128)}, f32[4,80,384]{2,1,0:T(8,128)}) custom-call(bf16[4,96,384]{2,1,0:T(8,128)(2,1)} %get-tuple-element.48.refs_0_, bf16[4,96,384]{2,1,0:T(8,128)(2,1)} %copy-done.27, bf16[256,256]{1,0:T(8,128)(2,1)} %bitcast.36, bf16[256,256]{1,0:T(8,128)(2,1)} %bitcast.33, f32[64,1]{1,0:T(8,128)} %copy.34.refs_4_, ...), custom_call_target="tpu_custom_call" | custom-call | flops 9663676416 | bytes 1867776 | tf_op jit(solution)/shard_map/pallas_call | solution.py:219
  81.3 7.7 %shard_map.188 = (f32[4,80,384]{2,1,0:T(8,128)}, f32[4,80,384]{2,1,0:T(8,128)}) custom-call(bf16[4,96,384]{2,1,0:T(8,128)(2,1)} %get-tuple-element.48.refs_0_, bf16[4,96,384]{2,1,0:T(8,128)(2,1)} %copy-done.27, bf16[256,256]{1,0:T(8,128)(2,1)} %bitcast.37, bf16[256,256]{1,0:T(8,128)(2,1)} %bitcast.34, f32[64,1]{1,0:T(8,128)} %copy.34.refs_4_, ...), custom_call_target="tpu_custom_call" | custom-call | flops 4831838208 | bytes 933888 | tf_op jit(solution)/shard_map/pallas_call | solution.py:219
  97.9 2.9 %shard_map.192.p0 = bf16[384,256]{1,0:T(8,128)(2,1)} custom-call(s32[3]{0:T(128)} %pad_add_fusion.ids, bf16[8,256]{1,0:T(8,128)(2,1)} %copy-done.20, bf16[384,256]{1,0:T(8,128)(2,1)} %get-tuple-element.63.x, bf16[8,256]{1,0:T(8,128)(2,1)} %copy-done.21, bf16[256,256]{1,0:T(8,128)(2,1)} %bitcast.31, f32[1,256]{1,0:T(1,128)} %bitcast.40), custom_call_target="tpu_custom_call" | custom-call | flops 100000000 | bytes 1048576 | tf_op jit(solution)/shard_map/pallas_call | solution.py:250
  101.6 2.9 %collective-permute-start.22 = (bf16[384,256]{1,0:T(8,128)(2,1)}, bf16[384,256]{1,0:T(8,128)(2,1)S(1)}, u32[]{:S(2)}, u32[]{:S(2)}) collective-permute-start(bf16[384,256]{1,0:T(8,128)(2,1)} %shard_map.192.p0), channel_id=1, source_target_pairs={{0,2},{1,3},{2,0},{3,1},{4,6},{5,7},{6,4},{7,5},{8,10},{9,11},{10,... | collective-permute-start | bytes 589832 | tf_op jit(solution)/shard_map/ppermute | solution.py:400
  106.0 1.9 %shard_map.189.a0 = bf16[256,384]{1,0:T(8,128)(2,1)} custom-call(f32[4,80,384]{2,1,0:T(8,128)} %get-tuple-element.54.mine, f32[4,80,384]{2,1,0:T(8,128)} %copy-done.7), custom_call_target="tpu_custom_call" | custom-call | flops 10000000 | bytes 1048576 | tf_op jit(solution)/shard_map/pallas_call | solution.py:250
  108.4 7.1 %collective-permute-done.18.w3 = bf16[512,512]{1,0:T(8,128)(2,1)S(1)} collective-permute-done((bf16[512,512]{1,0:T(8,128)(2,1)S(1)}, bf16[512,512]{1,0:T(8,128)(2,1)S(1)}, u32[]{:S(2)}, u32[]{:S(2)}) %collective-permute-start.18) | collective-permute-done | bytes 524320 | tf_op jit(solution)/shard_map/ppermute | solution.py:403
  116.4 2.1 %collective-permute-start.15 = (bf16[256,384]{1,0:T(8,128)(2,1)}, bf16[256,384]{1,0:T(8,128)(2,1)S(1)}, u32[]{:S(2)}, u32[]{:S(2)}) collective-permute-start(bf16[256,384]{1,0:T(8,128)(2,1)} %shard_map.189.a0), channel_id=1, source_target_pairs={{0,3},{1,0},{2,1},{3,2},{4,7},{5,4},{6,5},{7,6},{8,11},{9,8},{10,9... | collective-permute-start | bytes 589832 | tf_op jit(solution)/shard_map/ppermute | solution.py:416
  118.5 4.2 %shard_map.191 = (f32[384,512]{1,0:T(8,128)}, f32[384,512]{1,0:T(8,128)}) custom-call(s32[8]{0:T(128)} %and_select_fusion.ids, bf16[192,512]{1,0:T(8,128)(2,1)} %copy-done.3, bf16[192,512]{1,0:T(8,128)(2,1)} %copy-done.4, f32[4,1,512]{2,1,0:T(1,128)} %bitcast.30, bf16[2048,512]{1,0:T(8,128)(2,1)} %wa.3, bf16[2048,512]{1,0:T(8,128)(2,1)} %wp.3, ...), custom_call_target="tpu_custom_call" | custom-call | flops 500000000 | bytes 1048576 | tf_op jit(solution)/shard_map/pallas_call | solution.py:275
  124.7 3.6 %shard_map.193.pool = f32[384,512]{1,0:T(8,128)} custom-call(bf16[384,256]{1,0:T(8,128)(2,1)} %shard_map.192.p0, bf16[384,256]{1,0:T(8,128)(2,1)} %copy-done.14, bf16[384,256]{1,0:T(8,128)(2,1)} %copy-done.15, bf16[384,256]{1,0:T(8,128)(2,1)} %copy-done.17, bf16[512,512]{1,0:T(8,128)(2,1)} %get-tuple-element.56.w0, bf16[512,512]{1,0:T(8,128)(2,1)} %copy-done, ...), custom_call_target="tpu_custom_call" | custom-call | flops 1000000000 | bytes 1048576 | tf_op jit(solution)/shard_map/pallas_call | solution.py:250
  128.3 3.7 %collective-permute-done.15.a3 = bf16[256,384]{1,0:T(8,128)(2,1)S(1)} collective-permute-done((bf16[256,384]{1,0:T(8,128)(2,1)}, bf16[256,384]{1,0:T(8,128)(2,1)S(1)}, u32[]{:S(2)}, u32[]{:S(2)}) %collective-permute-start.15) | collective-permute-done | bytes 196640 | tf_op jit(solution)/shard_map/ppermute | solution.py:416
  132.6 3.7 %shard_map.194 = bf16[384,512]{1,0:T(8,128)(2,1)} custom-call(bf16[256,384]{1,0:T(8,128)(2,1)} %shard_map.189.a0, bf16[256,384]{1,0:T(8,128)(2,1)} %copy-done.16, bf16[256,384]{1,0:T(8,128)(2,1)} %copy-done.18, bf16[256,384]{1,0:T(8,128)(2,1)} %copy-done.19, bf16[512,512]{1,0:T(8,128)(2,1)} %get-tuple-element.56.w0, bf16[512,512]{1,0:T(8,128)(2,1)} %copy-done, ...), custom_call_target="tpu_custom_call" | custom-call | flops 1000000000 | bytes 1048576 | tf_op jit(solution)/shard_map/pallas_call | solution.py:250
  (114 shorter events, 35.0 us)
Async XLA Ops:
  0.0 12.2 %collective-permute-start = (bf16[384,512]{1,0:T(8,128)(2,1)}, bf16[384,512]{1,0:T(8,128)(2,1)S(1)}, u32[]{:S(2)}, u32[]{:S(2)}) collective-permute-start(bf16[384,512]{1,0:T(8,128)(2,1)} %refs_0_.1), channel_id=1, source_target_pairs={{0,1},{1,2},{2,3},{3,0},{4,5},{5,6},{6,7},{7,4},{8,9},{9,10},{10,1... | collective-permute-start | bytes 1179656 | tf_op jit(solution)/shard_map/ppermute | solution.py:316
  1.6 11.2 %collective-permute-start.2 = (bf16[384,512]{1,0:T(8,128)(2,1)}, bf16[384,512]{1,0:T(8,128)(2,1)S(1)}, u32[]{:S(2)}, u32[]{:S(2)}) collective-permute-start(bf16[384,512]{1,0:T(8,128)(2,1)} %refs_0_.1), channel_id=1, source_target_pairs={{0,3},{1,0},{2,1},{3,2},{4,7},{5,4},{6,5},{7,6},{8,11},{9,8},{10,9... | collective-permute-start | bytes 1179656 | tf_op jit(solution)/shard_map/ppermute | solution.py:317
  12.2 15.4 %collective-permute-start.1 = (bf16[192,512]{1,0:T(8,128)(2,1)S(1)}, bf16[192,512]{1,0:T(8,128)(2,1)S(1)}, u32[]{:S(2)}, u32[]{:S(2)}) collective-permute-start(bf16[192,512]{1,0:T(8,128)(2,1)S(1)} %slice.42), channel_id=1, source_target_pairs={{0,1},{1,2},{2,3},{3,0},{4,5},{5,6},{6,7},{7,4},{8,9},{9,10},{10,1... | collective-permute-start | bytes 589832 | tf_op jit(solution)/shard_map/ppermute | solution.py:318
  12.8 14.8 %collective-permute-start.3 = (bf16[192,512]{1,0:T(8,128)(2,1)S(1)}, bf16[192,512]{1,0:T(8,128)(2,1)S(1)}, u32[]{:S(2)}, u32[]{:S(2)}) collective-permute-start(bf16[192,512]{1,0:T(8,128)(2,1)S(1)} %slice.43), channel_id=1, source_target_pairs={{0,3},{1,0},{2,1},{3,2},{4,7},{5,4},{6,5},{7,6},{8,11},{9,8},{10,9... | collective-permute-start | bytes 589832 | tf_op jit(solution)/shard_map/ppermute | solution.py:319
  31.8 9.9 %collective-permute-start.5 = (bf16[304,384]{1,0:T(8,128)(2,1)}, bf16[304,384]{1,0:T(8,128)(2,1)S(1)}, u32[]{:S(2)}, u32[]{:S(2)}) collective-permute-start(bf16[304,384]{1,0:T(8,128)(2,1)} %get-tuple-element.49.a), channel_id=1, source_target_pairs={{0,32},{4,12},{8,40},{12,20},{16,48},{20,28},{24,56},{28,4},{32,64... | collective-permute-start | bytes 700424 | tf_op jit(solution)/shard_map/ppermute | solution.py:362
  33.9 7.8 %collective-permute-start.6 = (bf16[304,384]{1,0:T(8,128)(2,1)}, bf16[304,384]{1,0:T(8,128)(2,1)S(1)}, u32[]{:S(2)}, u32[]{:S(2)}) collective-permute-start(bf16[304,384]{1,0:T(8,128)(2,1)} %get-tuple-element.49.a), channel_id=1, source_target_pairs={{0,96},{4,28},{8,104},{12,4},{16,112},{20,12},{24,120},{28,20},{32... | collective-permute-start | bytes 700424 | tf_op jit(solution)/shard_map/ppermute | solution.py:363
  36.1 8.1 %collective-permute-start.7 = (bf16[304,384]{1,0:T(8,128)(2,1)}, bf16[304,384]{1,0:T(8,128)(2,1)S(1)}, u32[]{:S(2)}, u32[]{:S(2)}) collective-permute-start(bf16[304,384]{1,0:T(8,128)(2,1)} %get-tuple-element.49.a), channel_id=1, source_target_pairs={{0,64},{4,20},{8,72},{12,28},{16,80},{20,4},{24,88},{28,12},{32,96... | collective-permute-start | bytes 700424 | tf_op jit(solution)/shard_map/ppermute | solution.py:364
  41.0 60.6 %collective-permute-start.16 = (bf16[512,512]{1,0:T(8,128)(2,1)}, bf16[512,512]{1,0:T(8,128)(2,1)S(1)}, u32[]{:S(2)}, u32[]{:S(2)}) collective-permute-start(bf16[512,512]{1,0:T(8,128)(2,1)} %get-tuple-element.57), channel_id=1, source_target_pairs={{0,1},{1,2},{2,3},{3,0},{4,5},{5,6},{6,7},{7,4},{8,9},{9,10},{10,1... | collective-permute-start | bytes 1572872 | tf_op jit(solution)/shard_map/ppermute | solution.py:403
  47.3 17.5 %collective-permute-start.8 = (bf16[304,1536]{1,0:T(8,128)(2,1)}, bf16[304,1536]{1,0:T(8,128)(2,1)S(1)}, u32[]{:S(2)}, u32[]{:S(2)}) collective-permute-start(bf16[304,1536]{1,0:T(8,128)(2,1)} %shard_map.185.refs_5_), channel_id=1, source_target_pairs={{0,8},{4,36},{8,16},{12,44},{16,24},{20,52},{24,0},{28,60},{32,40}... | collective-permute-start | bytes 2801672 | tf_op jit(solution)/shard_map/ppermute | solution.py:380
  48.9 16.4 %collective-permute-start.10 = (bf16[304,1536]{1,0:T(8,128)(2,1)}, bf16[304,1536]{1,0:T(8,128)(2,1)S(1)}, u32[]{:S(2)}, u32[]{:S(2)}) collective-permute-start(bf16[304,1536]{1,0:T(8,128)(2,1)} %shard_map.185.refs_5_), channel_id=1, source_target_pairs={{0,24},{4,100},{8,0},{12,108},{16,8},{20,116},{24,16},{28,124},{32... | collective-permute-start | bytes 2801672 | tf_op jit(solution)/shard_map/ppermute | solution.py:381
  55.0 1.8 %collective-permute-start.4 = (bf16[4,96,384]{2,1,0:T(8,128)(2,1)}, bf16[4,96,384]{2,1,0:T(8,128)(2,1)S(1)}, u32[]{:S(2)}, u32[]{:S(2)}) collective-permute-start(bf16[4,96,384]{2,1,0:T(8,128)(2,1)} %get-tuple-element.48.refs_0_), channel_id=1, source_target_pairs={{0,4},{4,0},{8,12},{12,8},{16,20},{20,16},{24,28},{28,24},{32,36},... | collective-permute-start | bytes 884744 | tf_op jit(solution)/shard_map/ppermute | solution.py:374
  64.8 15.6 %collective-permute-start.9 = (bf16[152,1536]{1,0:T(8,128)(2,1)S(1)}, bf16[152,1536]{1,0:T(8,128)(2,1)S(1)}, u32[]{:S(2)}, u32[]{:S(2)}) collective-permute-start(bf16[152,1536]{1,0:T(8,128)(2,1)S(1)} %slice.46), channel_id=1, source_target_pairs={{0,8},{4,36},{8,16},{12,44},{16,24},{20,52},{24,0},{28,60},{32,40}... | collective-permute-start | bytes 1400840 | tf_op jit(solution)/shard_map/ppermute | solution.py:382
  65.3 15.1 %collective-permute-start.11 = (bf16[152,1536]{1,0:T(8,128)(2,1)S(1)}, bf16[152,1536]{1,0:T(8,128)(2,1)S(1)}, u32[]{:S(2)}, u32[]{:S(2)}) collective-permute-start(bf16[152,1536]{1,0:T(8,128)(2,1)S(1)} %slice.47), channel_id=1, source_target_pairs={{0,24},{4,100},{8,0},{12,108},{16,8},{20,116},{24,16},{28,124},{32... | collective-permute-start | bytes 1400840 | tf_op jit(solution)/shard_map/ppermute | solution.py:383
  89.0 15.5 %collective-permute-start.12 = (f32[4,80,384]{2,1,0:T(8,128)}, f32[4,80,384]{2,1,0:T(8,128)S(1)}, u32[]{:S(2)}, u32[]{:S(2)}) collective-permute-start(f32[4,80,384]{2,1,0:T(8,128)} %get-tuple-element.55), channel_id=1, source_target_pairs={{0,4},{4,0},{8,12},{12,8},{16,20},{20,16},{24,28},{28,24},{32,36},... | collective-permute-start | bytes 1474568 | tf_op jit(solution)/shard_map/ppermute | solution.py:414
  89.0 18.9 %collective-permute-start.17 = (bf16[512,512]{1,0:T(8,128)(2,1)S(1)}, bf16[512,512]{1,0:T(8,128)(2,1)S(1)}, u32[]{:S(2)}, u32[]{:S(2)}) collective-permute-start(bf16[512,512]{1,0:T(8,128)(2,1)S(1)} %copy-done.24), channel_id=1, source_target_pairs={{0,2},{1,3},{2,0},{3,1},{4,6},{5,7},{6,4},{7,5},{8,10},{9,11},{10,... | collective-permute-start | bytes 1572872 | tf_op jit(solution)/shard_map/ppermute | solution.py:403
  89.7 25.8 %collective-permute-start.18 = (bf16[512,512]{1,0:T(8,128)(2,1)S(1)}, bf16[512,512]{1,0:T(8,128)(2,1)S(1)}, u32[]{:S(2)}, u32[]{:S(2)}) collective-permute-start(bf16[512,512]{1,0:T(8,128)(2,1)S(1)} %copy-done.23), channel_id=1, source_target_pairs={{0,3},{1,0},{2,1},{3,2},{4,7},{5,4},{6,5},{7,6},{8,11},{9,8},{10,9... | collective-permute-start | bytes 1572872 | tf_op jit(solution)/shard_map/ppermute | solution.py:403
  91.5 2.7 %collective-permute-start.19 = (bf16[8,256]{1,0:T(8,128)(2,1)S(1)}, bf16[8,256]{1,0:T(8,128)(2,1)S(1)}, u32[]{:S(2)}, u32[]{:S(2)}) collective-permute-start(bf16[8,256]{1,0:T(8,128)(2,1)S(1)} %get-tuple-element.68), channel_id=1, source_target_pairs={{0,4},{4,8},{8,12},{12,16},{16,20},{20,24},{24,28},{28,32},{32,36}... | collective-permute-start | bytes 12296 | tf_op jit(solution)/shard_map/ppermute | solution.py:389
  94.2 3.0 %collective-permute-start.20 = (bf16[8,256]{1,0:T(8,128)(2,1)S(1)}, bf16[8,256]{1,0:T(8,128)(2,1)S(1)}, u32[]{:S(2)}, u32[]{:S(2)}) collective-permute-start(bf16[8,256]{1,0:T(8,128)(2,1)S(1)} %get-tuple-element.67), channel_id=1, source_target_pairs={{4,0},{8,4},{12,8},{16,12},{20,16},{24,20},{28,24},{32,28},{36,32}... | collective-permute-start | bytes 12296 | tf_op jit(solution)/shard_map/ppermute | solution.py:390
  100.8 15.6 %collective-permute-start.21 = (bf16[384,256]{1,0:T(8,128)(2,1)}, bf16[384,256]{1,0:T(8,128)(2,1)S(1)}, u32[]{:S(2)}, u32[]{:S(2)}) collective-permute-start(bf16[384,256]{1,0:T(8,128)(2,1)} %shard_map.192.p0), channel_id=1, source_target_pairs={{0,1},{1,2},{2,3},{3,0},{4,5},{5,6},{6,7},{7,4},{8,9},{9,10},{10,1... | collective-permute-start | bytes 589832 | tf_op jit(solution)/shard_map/ppermute | solution.py:400
  101.6 21.2 %collective-permute-start.22 = (bf16[384,256]{1,0:T(8,128)(2,1)}, bf16[384,256]{1,0:T(8,128)(2,1)S(1)}, u32[]{:S(2)}, u32[]{:S(2)}) collective-permute-start(bf16[384,256]{1,0:T(8,128)(2,1)} %shard_map.192.p0), channel_id=1, source_target_pairs={{0,2},{1,3},{2,0},{3,1},{4,6},{5,7},{6,4},{7,5},{8,10},{9,11},{10,... | collective-permute-start | bytes 589832 | tf_op jit(solution)/shard_map/ppermute | solution.py:400
  104.5 19.5 %collective-permute-start.23 = (bf16[384,256]{1,0:T(8,128)(2,1)}, bf16[384,256]{1,0:T(8,128)(2,1)S(1)}, u32[]{:S(2)}, u32[]{:S(2)}) collective-permute-start(bf16[384,256]{1,0:T(8,128)(2,1)} %shard_map.192.p0), channel_id=1, source_target_pairs={{0,3},{1,0},{2,1},{3,2},{4,7},{5,4},{6,5},{7,6},{8,11},{9,8},{10,9... | collective-permute-start | bytes 589832 | tf_op jit(solution)/shard_map/ppermute | solution.py:400
  107.9 20.3 %collective-permute-start.13 = (bf16[256,384]{1,0:T(8,128)(2,1)}, bf16[256,384]{1,0:T(8,128)(2,1)S(1)}, u32[]{:S(2)}, u32[]{:S(2)}) collective-permute-start(bf16[256,384]{1,0:T(8,128)(2,1)} %shard_map.189.a0), channel_id=1, source_target_pairs={{0,1},{1,2},{2,3},{3,0},{4,5},{5,6},{6,7},{7,4},{8,9},{9,10},{10,1... | collective-permute-start | bytes 589832 | tf_op jit(solution)/shard_map/ppermute | solution.py:416
  115.5 12.7 %collective-permute-start.14 = (bf16[256,384]{1,0:T(8,128)(2,1)}, bf16[256,384]{1,0:T(8,128)(2,1)S(1)}, u32[]{:S(2)}, u32[]{:S(2)}) collective-permute-start(bf16[256,384]{1,0:T(8,128)(2,1)} %shard_map.189.a0), channel_id=1, source_target_pairs={{0,2},{1,3},{2,0},{3,1},{4,6},{5,7},{6,4},{7,5},{8,10},{9,11},{10,... | collective-permute-start | bytes 589832 | tf_op jit(solution)/shard_map/ppermute | solution.py:416
  116.4 15.5 %collective-permute-start.15 = (bf16[256,384]{1,0:T(8,128)(2,1)}, bf16[256,384]{1,0:T(8,128)(2,1)S(1)}, u32[]{:S(2)}, u32[]{:S(2)}) collective-permute-start(bf16[256,384]{1,0:T(8,128)(2,1)} %shard_map.189.a0), channel_id=1, source_target_pairs={{0,3},{1,0},{2,1},{3,2},{4,7},{5,4},{6,5},{7,6},{8,11},{9,8},{10,9... | collective-permute-start | bytes 589832 | tf_op jit(solution)/shard_map/ppermute | solution.py:416
  (29 other events, 134.0 us)
where the time goes:
time: 137 us; the launch traced here: 136 us
  Pallas kernels  68.7 us (50%)
  starting transfers between devices  33 us (24%)
  waiting for transfers between devices  20.7 us (15%)
  local copies, waits for them, and re-layouts  11.1 us (8%)
  other arithmetic  2.66 us (2%)
    pallas_call x3, Pallas kernels, attend(): pl.pallas_call(kernel, in_specs=[VM] * (5 + len(arrays) + (2 if seeds els...  27.1 us
    pallas_call x5, Pallas kernels, picked(): pl.pallas_call(kernel, grid_spec=pltpu.PrefetchScalarGridSpec(num_scalar_...  24.1 us
    pallas_call x6, Pallas kernels, call(): pl.pallas_call(kernel, in_specs=specs, out_specs=jax.tree.map(lambda _: V...  17.5 us
    ppermute x3, waiting for transfers between devices, whole(): lax.ppermute(weights[d], 'tp', ring(d))  7.09 us
    ppermute x3, starting transfers between devices, whole(): pools = [pool] + [lax.ppermute(pool, 'tp', ring(d)) for d in (1, 2, 3)]  5.2 us
    unnamed x58, local copies, waits for them, and re-layouts  5.11 us
    ppermute x1, waiting for transfers between devices, whole(): x1 = lax.ppermute(tokens, 'tp', ring(1))  4.07 us
    ppermute x3, waiting for transfers between devices, whole(): attns = [attn] + [lax.ppermute(attn, 'tp', ring(d)) for d in (1, 2, 3)]  3.66 us
  transfers between devices with their start and end apart: 24, of which 8 were waited for; matrix products, arithmetic and copies ran while one was open for 6% of the time, Pallas kernels for 45%

commit v1 on v0

v1 whole, which is shorter than its diff:
```python
import functools
import math

import jax
import jax.numpy as jnp
from jax import lax
from jax.experimental import pallas as pl
from jax.experimental.pallas import tpu as pltpu
from jax.sharding import PartitionSpec as P


NOPE = 64
ROPE = 32
VALUE_DIM = 64
HEAD = NOPE + ROPE
LATENT = 256
REACH = 8
eps = 1e-06
theta = 10000.0
bf = jnp.bfloat16
f32 = jnp.float32

PAY = LATENT + ROPE + 16
ACC = VALUE_DIM + 16


def sp_of(z, y, c):
    return (z % 4) * 8 + (y % 4) * 2 + c


SITES = [(z, y, c) for z in range(4) for y in range(4) for c in range(2)]
SWAP = [(sp_of(z, y, c), sp_of(z, y, 1 - c)) for z, y, c in SITES]


def along(step, second):
    pairs = []
    for z, y, c in SITES:
        on_z = (c == 0) != second
        pairs.append((sp_of(z, y, c), sp_of(z + step, y, c) if on_z else sp_of(z, y + step, c)))
    return pairs


def ring(step):
    return [(i, (i + step) % 4) for i in range(4)]


def params(mib=56):
    return pltpu.CompilerParams(vmem_limit_bytes=mib * 2**20)


VM = pl.BlockSpec(memory_space=pltpu.VMEM)
SM = pl.BlockSpec(memory_space=pltpu.SMEM)


def gained(x, gain):
    return (x * gain).astype(bf)


def project_kernel(ids, *refs, first, count, seeded):
    xs, refs = refs[:count], refs[count:]
    gain, weights, refs = refs[0], refs[1:7], refs[7:]
    refs, (sems, *slots) = refs[:-7], refs[-7:]
    seeds, outs = (refs[:7], refs[7:]) if seeded else ((), refs[-7:])
    ats = [pl.multiple_of(ids[first + k] * 512, 512) for k in range(count)]
    copies = []
    for i, w in enumerate(weights):
        for k, at in enumerate(ats):
            source = w.at[:, pl.ds(at, 512)] if i == 1 else w.at[pl.ds(at, 512), :]
            copies.append(pltpu.make_async_copy(source, slots[i].at[k], sems.at[i, k]))
            copies[-1].start()
    values = [x[...].astype(f32) for x in xs]
    square = sum(jnp.sum(x * x, axis=-1, keepdims=True) for x in values)
    square = jnp.broadcast_to(square, outs[0].shape)
    outs[0][...] = seeds[0][...] + square if seeded else square
    ns = [gained(x, gain[:, pl.ds(at, 512)]) for x, at in zip(values, ats)]
    for i in range(6):
        total = seeds[i + 1][...] if seeded else None
        for k, n in enumerate(ns):
            copies[i * count + k].wait()
            part = product(n, slots[i][k], i == 1)
            total = part if total is None else total + part
        outs[i + 1][...] = total


def product(n, w, turned):
    if turned:
        return lax.dot_general(w, n, (((1,), (1,)), ((), ())), preferred_element_type=f32)
    return jnp.dot(n, w, preferred_element_type=f32)


def rows_at(w, at):
    return w[pl.ds(at, 512), :]


def last_piece(ids, x, gain):
    at = pl.multiple_of(ids[3] * 512, 512)
    x = x[...].astype(f32)
    return x, gained(x, gain[:, pl.ds(at, 512)]), at


def front_kernel(ids, x, gain, wl, wr, square, lat0, raw0, gains, cos, sin, pay, scale_out):
    x, n, at = last_piece(ids, x, gain)
    lgain, kgain = gains[:LATENT], gains[LATENT + NOPE : LATENT + HEAD]
    total = square[...] + jnp.broadcast_to(jnp.sum(x * x, axis=-1, keepdims=True), square.shape)
    scale = lax.rsqrt(total * (1.0 / 2048) + eps)
    scale_out[...] = scale
    lat = lat0[...] + product(n, rows_at(wl, at), False)
    lat = jnp.transpose(lat * scale[:, :1]).astype(bf).astype(f32)
    lat = lat * lax.rsqrt(jnp.mean(lat * lat, axis=0, keepdims=True) + eps) * lgain
    pay[:LATENT, :] = lat.astype(bf)
    raw = raw0[...] + product(n, wr[:, pl.ds(at, 512)], True)
    raw = (raw * jnp.transpose(scale)[:1]).astype(bf).astype(f32)
    total = jnp.sum(raw * raw, axis=0, keepdims=True)
    k = raw * kgain
    first, second = k[:16], k[16:]
    pay[LATENT : LATENT + 16, :] = (first * cos[...] - second * sin[...]).astype(bf)
    pay[LATENT + 16 : LATENT + 32, :] = (first * sin[...] + second * cos[...]).astype(bf)
    pay[LATENT + 32 :, :] = jnp.broadcast_to(total, (16, total.shape[1])).astype(bf)


def query_kernel(ids, x, gain, wqd, wpi, scale, lat0, pool0, qgain, wqu, gains, cos, sin, q, pool_in, inner, outer):
    _, n, at = last_piece(ids, x, gain)
    hgain = gains[LATENT + HEAD : LATENT + 2 * HEAD]
    s = scale[:, :1]
    pooled = (pool0[...] + product(n, rows_at(wpi, at), False)) * s
    pool_in[...] = pooled.astype(bf)
    head, end = pooled[:REACH], pooled[pooled.shape[0] - REACH :]
    on_first = ids[8] % 2 == 0
    inner[...] = jnp.where(on_first, end, head).astype(bf)
    outer[...] = jnp.where(on_first, head, end).astype(bf)
    lat = (lat0[...] + product(n, rows_at(wqd, at), False)) * s
    lat = lat.astype(bf).astype(f32)
    lat = lat * lax.rsqrt(jnp.mean(lat * lat, axis=-1, keepdims=True) + eps) * qgain[...]
    raw = jnp.dot(lat.astype(bf), wqu[...], preferred_element_type=f32)
    raw = jnp.transpose(raw).astype(bf).astype(f32)
    for h in range(raw.shape[0] // HEAD):
        v = raw[h * HEAD : (h + 1) * HEAD]
        v = v * lax.rsqrt(jnp.mean(v * v, axis=0, keepdims=True) + eps) * hgain
        v = v * (HEAD**-0.5 / math.log(2.0))
        first, second = v[NOPE : NOPE + 16], v[NOPE + 16 :]
        q[h, :NOPE, :] = v[:NOPE].astype(bf)
        q[h, NOPE : NOPE + 16, :] = (first * cos[...] - second * sin[...]).astype(bf)
        q[h, NOPE + 16 :, :] = (first * sin[...] + second * cos[...]).astype(bf)


def gate_kernel(ids, x, gain, wa, wp, scale, a0, p0, gate_a, gate_p):
    _, n, at = last_piece(ids, x, gain)
    s = scale[:, :1]
    gate_a[...] = jax.nn.sigmoid((a0[...] + product(n, rows_at(wa, at), False)) * s)
    gate_p[...] = jax.nn.sigmoid((p0[...] + product(n, rows_at(wp, at), False)) * s)


def join_kernel(a, b, c, d, out):
    width = a.shape[1]
    for i, x in enumerate((a, b, c, d)):
        out[:, i * width : (i + 1) * width] = x[...]


def pool_merge_kernel(pool, w0, w1, w2, w3, gate, out):
    total = jnp.dot(pool[...], w0[256:, :], preferred_element_type=f32)
    for w in (w1, w2, w3):
        p = jnp.concatenate([w[512:, :256], w[512:, 256:]], axis=0)
        total = total + jnp.dot(p, w[256:512, :], preferred_element_type=f32)
    out[...] = gate[...] * total


def pack_kernel(ids, inner, x, outer, mix, scale, wa, wp, pool, own, s1, s2, s3, padded):
    rows = x.shape[0]
    half, length = ids[9], ids[10]
    on_first = ids[8] % 2 == 0
    inner, outer = inner[...].astype(f32), outer[...].astype(f32)
    padded[0:REACH, :] = jnp.where(on_first, outer, inner)
    padded[REACH : REACH + rows, :] = x[...].astype(f32)
    padded[REACH + rows :, :] = jnp.where(on_first, inner, outer)
    total = jnp.zeros((rows, x.shape[1]), f32)
    for shift in range(-REACH, REACH):
        inside = (shift >= -half) & (shift <= half - 1)
        total = total + jnp.where(inside, padded[REACH + shift : REACH + shift + rows, :], 0.0)
    at = ids[8] * rows + lax.broadcasted_iota(jnp.int32, (rows, 1), 0)
    count = (jnp.clip(at + half, 0, length) - jnp.clip(at - half, 0, length)).astype(f32)
    mixed = (total / count - padded[REACH : REACH + rows, :]).astype(bf)
    out = (jnp.dot(mixed, mix[...], preferred_element_type=f32) * scale[...]).astype(bf)
    pool[...] = out
    for d, s in enumerate((own, s1, s2, s3)):
        at = pl.multiple_of(ids[4 + d] * 512, 512)
        s[:256, :] = wa[:, pl.ds(at, 512)]
        s[256:512, :] = wp[:, pl.ds(at, 512)]
        if d > 0:
            s[512:, :256] = out[: rows // 2]
            s[512:, 256:] = out[rows // 2 :]


def attend_kernel(*refs, pieces, seeded):
    q0, q1, up, gains = refs[:4]
    refs = refs[4:]
    gain = gains[LATENT : LATENT + NOPE]
    n_in = sum(len(p) for p in pieces)
    blocks = refs[:n_in]
    refs = refs[n_in:]
    seeds, outs = (refs[:2], refs[2:]) if seeded else ((), refs)
    heads = q0.shape[0]
    half = q0.shape[2]
    at = 0
    for number, piece in enumerate(pieces):
        parts = [blocks[at + i] for i in range(len(piece))]
        at += len(piece)
        whole = parts[0][...] if len(parts) == 1 else jnp.concatenate([p[...] for p in parts], axis=0)
        keys = whole.shape[1]
        latent = whole[:LATENT]
        rope = whole[LATENT : LATENT + ROPE].astype(f32)
        square = whole[LATENT + ROPE :].astype(f32)[0:1]
        expanded = lax.dot_general(up[...], latent, (((0,), (0,)), ((), ())), preferred_element_type=f32)
        row = lax.broadcasted_iota(jnp.int32, (16, keys), 0)
        ones = jnp.where(row == 0, 1.0, 0.0).astype(bf)
        for h in range(heads):
            k = expanded[h * 128 : h * 128 + NOPE]
            scale = lax.rsqrt((jnp.sum(k * k, axis=0, keepdims=True) + square) * (1.0 / HEAD) + eps)
            key = jnp.concatenate([(k * gain * scale).astype(bf), (rope * scale).astype(bf)], axis=0)
            query = jnp.concatenate([q0[h], q1[h]], axis=1)
            scores = lax.dot_general(key, query, (((0,), (0,)), ((), ())), preferred_element_type=f32)
            weights = jnp.exp2(scores).astype(bf)
            v = jnp.concatenate([expanded[h * 128 + NOPE : (h + 1) * 128].astype(bf), ones], axis=0)
            add = jnp.dot(v, weights, preferred_element_type=f32)
            for i in range(2):
                part = add[:, i * half : (i + 1) * half]
                if number > 0:
                    outs[i][h] += part
                elif seeded:
                    outs[i][h] = seeds[i][h] + part
                else:
                    outs[i][h] = part


def attend(q0, q1, up, gains, pieces, seeds):
    heads, _, half = q0.shape
    shape = jax.ShapeDtypeStruct((heads, ACC, half), f32)
    arrays = [a for p in pieces for a in p]
    keys = sum(p[0].shape[1] for p in pieces)
    kernel = functools.partial(
        attend_kernel, pieces=[[None] * len(p) for p in pieces], seeded=seeds is not None
    )
    return call(
        kernel,
        None,
        [q0, q1, up, gains, *[resident(a) for a in (*arrays, *(seeds or ()))]],
        [kept(shape), kept(shape)],
        keys * heads * 2 * half * 2 * 512,
        mib=28,
        transcendentals=keys * heads * 2 * half,
    )


def finish_kernel(mine, other, out):
    for h in range(mine.shape[0]):
        both = mine[h] + other[h]
        out[h * VALUE_DIM : (h + 1) * VALUE_DIM, :] = (
            both[:VALUE_DIM] / both[VALUE_DIM : VALUE_DIM + 1]
        ).astype(bf)


def merge_kernel(a0, a1, a2, a3, w0, w1, w2, w3, gate, pool, out):
    total = None
    for a, w in ((a0, w0), (a1, w1), (a2, w2), (a3, w3)):
        part = lax.dot_general(a[...], w[:256, :], (((0,), (0,)), ((), ())), preferred_element_type=f32)
        total = part if total is None else total + part
    out[...] = (gate[...] * total + pool[...]).astype(bf)


def resident(x):
    return pltpu.with_memory_space_constraint(x, pltpu.VMEM)


def kept(s):
    return pltpu.VMEM(s.shape, s.dtype)


def call(kernel, ids, ins, shapes, flops, scratch=(), mib=16, transcendentals=0, apart=()):
    first = [] if ids is None else [ids]
    ins = [pltpu.with_memory_space_constraint(x, pltpu.HBM) if i in apart else x for i, x in enumerate(ins)]
    return pl.pallas_call(
        kernel,
        in_specs=[SM] * len(first)
        + [pl.BlockSpec(memory_space=pltpu.HBM) if i in apart else VM for i in range(len(ins))],
        out_specs=jax.tree.map(lambda _: VM, shapes),
        out_shape=shapes,
        scratch_shapes=scratch,
        compiler_params=params(mib),
        cost_estimate=pl.CostEstimate(flops=flops, transcendentals=transcendentals, bytes_accessed=2**20),
    )(*first, *ins)


def whole(
    tokens,
    norm_gain,
    w_query_down,
    query_gain,
    w_query_up,
    w_latent_down,
    latent_gain,
    w_rotary_key,
    w_latent_up,
    query_head_gain,
    key_head_gain,
    w_pool_in,
    w_pool_mix,
    pool_scale,
    w_attn_out,
    w_pool_out,
    w_gate_attn,
    w_gate_pool,
):
    S = jax.ShapeDtypeStruct
    rows = tokens.shape[0]
    heads = w_query_up.shape[1] // HEAD
    length = rows * lax.axis_size("sp")
    here = lax.axis_index("sp")
    t = lax.axis_index("tp")

    x1 = lax.ppermute(tokens, "tp", ring(1))
    x2 = lax.ppermute(tokens, "tp", ring(-1))
    x3 = lax.ppermute(tokens, "tp", ring(2))

    half = ROPE // 2
    freqs = theta ** (-jnp.arange(half, dtype=f32) / half)
    positions = (here * rows + jnp.arange(rows, dtype=jnp.int32)).astype(f32)
    angles = freqs[:, None] * positions[None, :]
    cos, sin = jnp.cos(angles), jnp.sin(angles)
    ids = jnp.concatenate(
        [
            (t + jnp.array([0, 3, 1, 2, 0, 1, 2, 3], jnp.int32)) & 3,
            jnp.stack([here, jnp.left_shift(1, t), jnp.int32(length)]).astype(jnp.int32),
        ]
    )
    gains = jnp.concatenate([latent_gain, key_head_gain, query_head_gain])[:, None]
    gain = norm_gain[None, :]
    wr = w_rotary_key.T

    sums = [S((rows, 128), f32), S((rows, 256), f32), S((ROPE, rows), f32), S((rows, 512), f32),
            S((rows, 256), f32), S((rows, 512), f32), S((rows, 512), f32)]
    projections = [w_latent_down, wr, w_query_down, w_pool_in, w_gate_attn, w_gate_pool]

    def slots(count):
        shapes = [(count, 512, w.shape[1]) for w in projections]
        shapes[1] = (count, ROPE, 512)
        return [pltpu.SemaphoreType.DMA((6, count))] + [pltpu.VMEM(s, bf) for s in shapes]

    own = call(
        functools.partial(project_kernel, first=0, count=1, seeded=False),
        ids, [tokens, gain, *projections, gains, cos, sin], [kept(s) for s in sums], 8 * 10**8,
        slots(1), apart=range(2, 11),
    )
    near = call(
        functools.partial(project_kernel, first=1, count=2, seeded=True),
        ids, [resident(x1), resident(x2), gain, *projections, *[resident(s) for s in own]],
        [kept(s) for s in sums[:3]] + sums[3:], 16 * 10**8,
        slots(2), apart=range(3, 9),
    )
    square, lat0, raw0, query0, pool0, attn0, gate0 = near

    pay, scale = call(
        front_kernel,
        ids,
        [resident(x3), gain, w_latent_down, wr, resident(square), resident(lat0), resident(raw0), gains, cos, sin],
        [kept(S((PAY, rows), bf)), S((rows, 128), f32)],
        3 * 10**8,
    )

    a1 = lax.ppermute(pay, "sp", along(1, False))
    a2 = lax.ppermute(pay, "sp", along(-1, False))
    a3 = lax.ppermute(pay, "sp", along(2, False))

    q, pool_in, inner, outer = call(
        query_kernel,
        ids,
        [x3, gain, w_query_down, w_pool_in, scale, query0, pool0, query_gain[None, :],
         w_query_up, gains, cos, sin],
        [S((heads, HEAD, rows), bf), S((rows, 256), bf), S((REACH, 256), bf), S((REACH, 256), bf)],
        10**9,
    )
    q_other = lax.ppermute(q, "sp", SWAP)
    inner = lax.ppermute(inner, "sp", SWAP)
    count = lax.axis_size("sp")
    outer = lax.ppermute(outer, "sp", [(i, i - 1 + 2 * (i % 2)) for i in range(1, count - 1)])

    def attend_on(pieces, seeds):
        return attend(q, q_other, w_latent_up, gains, pieces, seeds)

    line = call(join_kernel, None, [resident(x) for x in (pay, a1, a2, a3)], kept(S((PAY, 4 * rows), bf)), 10**7)
    b1 = lax.ppermute(line, "sp", along(1, True))
    b2 = lax.ppermute(line, "sp", along(-1, True))
    cut = PAY // 2
    b3 = lax.ppermute(b1[:cut], "sp", along(1, True))
    b4 = lax.ppermute(b2[cut:], "sp", along(-1, True))

    pool, own_w, *packs = call(
        pack_kernel,
        ids,
        [inner, pool_in, outer, w_pool_mix[0], pool_scale[None, :], w_attn_out, w_pool_out],
        [S((rows, 256), bf), S((512, 512), bf)] + [S((704, 512), bf)] * 3,
        10**8,
        [pltpu.VMEM((rows + 2 * REACH, 256), f32)],
    )
    weights = [own_w] + [lax.ppermute(packs[d - 1], "tp", ring(d)) for d in (1, 2, 3)]

    acc = attend_on([[line]], None)
    acc = attend_on([[b1], [b2]], acc)
    acc = attend_on([[b3, b4]], acc)

    gate_attn, gate_pool = call(
        gate_kernel,
        ids,
        [x3, gain, w_gate_attn, w_gate_pool, scale, attn0, gate0],
        [kept(S((rows, 512), f32))] * 2,
        5 * 10**8,
    )
    pool_branch = call(pool_merge_kernel, None, [pool, *weights, resident(gate_pool)], kept(S((rows, 512), f32)), 10**9)

    other = lax.ppermute(acc[1], "sp", SWAP)
    attn = call(finish_kernel, None, [resident(acc[0]), resident(other)], kept(S((heads * VALUE_DIM, rows), bf)), 10**7)
    attns = [attn] + [lax.ppermute(attn, "tp", ring(d)) for d in (1, 2, 3)]
    return call(
        merge_kernel, None, [*[resident(a) for a in attns], *weights, resident(gate_attn), resident(pool_branch)], S((rows, 512), bf), 10**9
    )


def solution(mesh):
    placed = (
        P("sp", "tp"),
        P(),
        P(),
        P(),
        P(None, "tp"),
        P(),
        P(),
        P(),
        P(None, "tp"),
        P(),
        P(),
        P(None, "tp"),
        P("tp", None, None),
        P("tp"),
        P("tp", None),
        P("tp", None),
        P(None, "tp"),
        P(None, "tp"),
    )
    return jax.shard_map(whole, mesh=mesh, in_specs=placed, out_specs=P("sp", "tp"), check_vma=False)
```

time: 137 us -> 103 us (0.75)
  the two profiles are of different devices: /device:TPU:0 before, /device:TPU:27 now
where the time goes in v1:
time: 103 us; the launch traced here: 102 us
  Pallas kernels  36.5 us (35%)
  waiting for transfers between devices  34.9 us (34%)
  starting transfers between devices  25.6 us (25%)
  local copies, waits for them, and re-layouts  2.69 us (3%)
  other arithmetic  2.33 us (2%)
    pallas_call x13, Pallas kernels, call(): pl.pallas_call(kernel, in_specs=[SM] * len(first) + [pl.BlockSpec(memory_...  36.5 us
    ppermute x1, waiting for transfers between devices, whole(): x2 = lax.ppermute(tokens, 'tp', ring(-1))  8.56 us
    ppermute x3, waiting for transfers between devices, whole(): attns = [attn] + [lax.ppermute(attn, 'tp', ring(d)) for d in (1, 2, 3)]  7.51 us
    ppermute x1, waiting for transfers between devices, whole(): lax.ppermute(outer, 'sp', [(i, i - 1 + 2 * (i % 2)) for i in range(1, cou...  6.99 us
    ppermute x3, waiting for transfers between devices, whole(): lax.ppermute(packs[d - 1], 'tp', ring(d))  4.98 us
    ppermute x1, starting transfers between devices, whole(): b2 = lax.ppermute(line, 'sp', along(-1, True))  4.12 us
    ppermute x3, starting transfers between devices, whole(): lax.ppermute(packs[d - 1], 'tp', ring(d))  3.65 us
    ppermute x1, starting transfers between devices, whole(): q_other = lax.ppermute(q, 'sp', SWAP)  3.36 us
  transfers between devices with their start and end apart: 20, of which 8 were waited for; matrix products, arithmetic and copies ran while one was open for 3% of the time, Pallas kernels for 33%

profile of v1, /device:TPU:27, one launch (start us, length us, event | category | flops | bytes accessed | tf_op | source)
XLA Modules:
  0.0 102.3 jit_solution(3556855717984563871)
XLA Ops:
  2.0 1.9 %collective-permute-start.2 = (bf16[384,512]{1,0:T(8,128)(2,1)}, bf16[384,512]{1,0:T(8,128)(2,1)S(1)}, u32[]{:S(2)}, u32[]{:S(2)}) collective-permute-start(bf16[384,512]{1,0:T(8,128)(2,1)} %refs_0_.1), channel_id=1, source_target_pairs={{0,3},{1,0},{2,1},{3,2},{4,7},{5,4},{6,5},{7,6},{8,11},{9,8},{10,9... | collective-permute-start | bytes 1179656 | tf_op jit(solution)/shard_map/ppermute | solution.py:320
  8.8 3.7 %shard_map.181 = (f32[384,128]{1,0:T(8,128)S(1)}, f32[384,256]{1,0:T(8,128)S(1)}, f32[32,384]{1,0:T(8,128)S(1)}, f32[384,512]{1,0:T(8,128)S(1)}, f32[384,256]{1,...) custom-call(s32[11]{0:T(128)S(1)} %pad_add_fusion.ids, bf16[384,512]{1,0:T(8,128)(2,1)S(1)} %copy-done.9, ...), custom_call_target="tpu_custom_call" | custom-call | flops 800000000 | bytes 1048576 | tf_op jit(solution)/shard_map/pallas_call | solution.py:280
  12.5 8.6 %collective-permute-done.2.refs_1_ = bf16[384,512]{1,0:T(8,128)(2,1)S(1)} collective-permute-done((bf16[384,512]{1,0:T(8,128)(2,1)}, bf16[384,512]{1,0:T(8,128)(2,1)S(1)}, u32[]{:S(2)}, u32[]{:S(2)}) %collective-permute-start.2) | collective-permute-done | bytes 393248 | tf_op jit(solution)/shard_map/ppermute | solution.py:320
  21.1 6.3 %shard_map.182 = (f32[384,128]{1,0:T(8,128)S(1)}, f32[384,256]{1,0:T(8,128)S(1)}, f32[32,384]{1,0:T(8,128)S(1)}, f32[384,512]{1,0:T(8,128)S(1)}, f32[384,256]{1,...) custom-call(s32[11]{0:T(128)S(1)} %pad_add_fusion.ids, ...), custom_call_target="tpu_custom_call" | custom-call | flops 1600000000 | bytes 1048576 | tf_op jit(solution)/shard_map/pallas_call | solution.py:280
  29.6 2.7 %collective-permute-start.4 = (bf16[304,384]{1,0:T(8,128)(2,1)S(1)}, bf16[304,384]{1,0:T(8,128)(2,1)S(1)}, u32[]{:S(2)}, u32[]{:S(2)}) collective-permute-start(bf16[304,384]{1,0:T(8,128)(2,1)S(1)} %get-tuple-element.52.a), channel_id=1, source_target_pairs={{0,32},{4,12},{8,40},{12,20},{16,48},{20,28},{24,56},{28,4},{32,64... | collective-permute-start | bytes 700424 | tf_op jit(solution)/shard_map/ppermute | solution.py:368
  32.3 3.1 %collective-permute-done.6.d = bf16[304,384]{1,0:T(8,128)(2,1)S(1)} collective-permute-done((bf16[304,384]{1,0:T(8,128)(2,1)S(1)}, bf16[304,384]{1,0:T(8,128)(2,1)S(1)}, u32[]{:S(2)}, u32[]{:S(2)}) %collective-permute-start.6) | collective-permute-done | bytes 233504 | tf_op jit(solution)/shard_map/ppermute | solution.py:370
  35.4 2.2 %collective-permute-done.5.c = bf16[304,384]{1,0:T(8,128)(2,1)S(1)} collective-permute-done((bf16[304,384]{1,0:T(8,128)(2,1)S(1)}, bf16[304,384]{1,0:T(8,128)(2,1)S(1)}, u32[]{:S(2)}, u32[]{:S(2)}) %collective-permute-start.5) | collective-permute-done | bytes 233504 | tf_op jit(solution)/shard_map/ppermute | solution.py:369
  37.7 4.1 %collective-permute-start.9 = (bf16[304,1536]{1,0:T(8,128)(2,1)S(1)}, bf16[304,1536]{1,0:T(8,128)(2,1)S(1)}, u32[]{:S(2)}, u32[]{:S(2)}) collective-permute-start(bf16[304,1536]{1,0:T(8,128)(2,1)S(1)} %shard_map.185.refs_4_), channel_id=1, source_target_pairs={{0,24},{4,100},{8,0},{12,108},{16,8},{20,116},{24,16},{28,124},{32... | collective-permute-start | bytes 2801672 | tf_op jit(solution)/shard_map/ppermute | solution.py:390
  41.9 1.7 %shard_map.184 = (bf16[4,96,384]{2,1,0:T(8,128)(2,1)S(1)}, bf16[384,256]{1,0:T(8,128)(2,1)S(1)}, bf16[8,256]{1,0:T(8,128)(2,1)S(1)}, bf16[8,256]{1,0:T(8,128)(2,1)S(1)}) custom-call(s32[11]{0:T(128)S(1)} %pad_add_fusion.ids, bf16[384,512]{1,0:T(8,128)(2,1)S(1)} %collective-permute-done.x, f32[1,2048]{1,0:T(1,128)S(1)} %bitcast.14, ...), custom_call_target="tpu_custom_call" | custom-call | flops 1000000000 | bytes 1048576 | tf_op jit(solution)/shard_map/pallas_call | solution.py:280
  43.6 3.4 %collective-permute-start.3 = (bf16[4,96,384]{2,1,0:T(8,128)(2,1)S(1)}, bf16[4,96,384]{2,1,0:T(8,128)(2,1)S(1)}, u32[]{:S(2)}, u32[]{:S(2)}) collective-permute-start(bf16[4,96,384]{2,1,0:T(8,128)(2,1)S(1)} %get-tuple-element.51.refs_0_), channel_id=1, source_target_pairs={{0,4},{4,0},{8,12},{12,8},{16,20},{20,16},{24,28},{28,24},{32,36},... | collective-permute-start | bytes 884744 | tf_op jit(solution)/shard_map/ppermute | solution.py:380
  47.1 1.9 %collective-permute-start.16 = (bf16[8,256]{1,0:T(8,128)(2,1)S(1)}, bf16[8,256]{1,0:T(8,128)(2,1)S(1)}, u32[]{:S(2)}, u32[]{:S(2)}) collective-permute-start(bf16[8,256]{1,0:T(8,128)(2,1)S(1)} %get-tuple-element.61), channel_id=1, source_target_pairs={{4,8},{8,4},{12,16},{16,12},{20,24},{24,20},{28,32},{32,28},{36,40... | collective-permute-start | bytes 12296 | tf_op jit(solution)/shard_map/ppermute | solution.py:383
  49.0 7.0 %collective-permute-done.16.outer = bf16[8,256]{1,0:T(8,128)(2,1)S(1)} collective-permute-done((bf16[8,256]{1,0:T(8,128)(2,1)S(1)}, bf16[8,256]{1,0:T(8,128)(2,1)S(1)}, u32[]{:S(2)}, u32[]{:S(2)}) %collective-permute-start.16) | collective-permute-done | bytes 4128 | tf_op jit(solution)/shard_map/ppermute | solution.py:383
  56.0 1.9 %shard_map.190 = (bf16[384,256]{1,0:T(8,128)(2,1)S(1)}, bf16[512,512]{1,0:T(8,128)(2,1)S(1)}, bf16[704,512]{1,0:T(8,128)(2,1)S(1)}, bf16[704,512]{1,0:T(8,128)(2,1)S(1)}, bf16[704,512]{1,0:T(8,128)(2,1)S(1)}) custom-call(s32[11]{0:T(128)S(1)} %pad_add_fusion.ids, bf16[8,256]{1,0:T(8,128)(2,1)S(1)} %collective-permute-done.15.inner, ...), custom_call_target="tpu_custom_call" | custom-call | flops 100000000 | bytes 1048576 | tf_op jit(solution)/shard_map/pallas_call | solution.py:280
  59.8 1.7 %collective-permute-start.19 = (bf16[704,512]{1,0:T(8,128)(2,1)S(1)}, bf16[704,512]{1,0:T(8,128)(2,1)S(1)}, u32[]{:S(2)}, u32[]{:S(2)}) collective-permute-start(bf16[704,512]{1,0:T(8,128)(2,1)S(1)} %get-tuple-element.65), channel_id=1, source_target_pairs={{0,3},{1,0},{2,1},{3,2},{4,7},{5,4},{6,5},{7,6},{8,11},{9,8},{10,9... | collective-permute-start | bytes 2162696 | tf_op jit(solution)/shard_map/ppermute | solution.py:403
  61.6 4.6 %shard_map.186 = (f32[4,80,384]{2,1,0:T(8,128)S(1)}, f32[4,80,384]{2,1,0:T(8,128)S(1)}) custom-call(bf16[4,96,384]{2,1,0:T(8,128)(2,1)S(1)} %get-tuple-element.51.refs_0_, bf16[4,96,384]{2,1,0:T(8,128)(2,1)S(1)} %collective-permute-done.3.refs_1_, bf16[256,512]{1,0:T(8,128)(2,1)S(1)} %copy-done.18, f32[448,1]{1,0:T(8,128)S(1)} %copy-done.5, ...), custom_call_target="tpu_custom_call" | custom-call | flops 4831838208 | bytes 1048576 | tf_op jit(solution)/shard_map/pallas_call | solution.py:280
  66.4 1.5 %collective-permute-start.8 = (bf16[152,1536]{1,0:T(8,128)(2,1)S(1)}, bf16[152,1536]{1,0:T(8,128)(2,1)S(1)}, u32[]{:S(2)}, u32[]{:S(2)}) collective-permute-start(bf16[152,1536]{1,0:T(8,128)(2,1)S(1)} %slice.8), channel_id=1, source_target_pairs={{0,8},{4,36},{8,16},{12,44},{16,24},{20,52},{24,0},{28,60},{32,40}... | collective-permute-start | bytes 1400840 | tf_op jit(solution)/shard_map/ppermute | solution.py:392
  67.9 9.1 %shard_map.187 = (f32[4,80,384]{2,1,0:T(8,128)S(1)}, f32[4,80,384]{2,1,0:T(8,128)S(1)}) custom-call(bf16[4,96,384]{2,1,0:T(8,128)(2,1)S(1)} %get-tuple-element.51.refs_0_, bf16[4,96,384]{2,1,0:T(8,128)(2,1)S(1)} %collective-permute-done.3.refs_1_, bf16[256,512]{1,0:T(8,128)(2,1)S(1)} %copy-done.18, f32[448,1]{1,0:T(8,128)S(1)} %copy-done.5, ...), custom_call_target="tpu_custom_call" | custom-call | flops 9663676416 | bytes 1048576 | tf_op jit(solution)/shard_map/pallas_call | solution.py:280
  77.0 4.9 %shard_map.188 = (f32[4,80,384]{2,1,0:T(8,128)S(1)}, f32[4,80,384]{2,1,0:T(8,128)S(1)}) custom-call(bf16[4,96,384]{2,1,0:T(8,128)(2,1)S(1)} %get-tuple-element.51.refs_0_, bf16[4,96,384]{2,1,0:T(8,128)(2,1)S(1)} %collective-permute-done.3.refs_1_, bf16[256,512]{1,0:T(8,128)(2,1)S(1)} %copy-done.18, f32[448,1]{1,0:T(8,128)S(1)} %copy-done.5, ...), custom_call_target="tpu_custom_call" | custom-call | flops 4831838208 | bytes 1048576 | tf_op jit(solution)/shard_map/pallas_call | solution.py:280
  82.3 1.5 %collective-permute-done.11.other = f32[4,80,384]{2,1,0:T(8,128)S(1)} collective-permute-done((f32[4,80,384]{2,1,0:T(8,128)S(1)}, f32[4,80,384]{2,1,0:T(8,128)S(1)}, u32[]{:S(2)}, u32[]{:S(2)}) %collective-permute-start.11) | collective-permute-done | bytes 491552 | tf_op jit(solution)/shard_map/ppermute | solution.py:418
  83.9 1.5 %collective-permute-start.14 = (bf16[256,384]{1,0:T(8,128)(2,1)S(1)}, bf16[256,384]{1,0:T(8,128)(2,1)S(1)}, u32[]{:S(2)}, u32[]{:S(2)}) collective-permute-start(bf16[256,384]{1,0:T(8,128)(2,1)S(1)} %shard_map.189.a0), channel_id=1, source_target_pairs={{0,3},{1,0},{2,1},{3,2},{4,7},{5,4},{6,5},{7,6},{8,11},{9,8},{10,9... | collective-permute-start | bytes 589832 | tf_op jit(solution)/shard_map/ppermute | solution.py:420
  87.9 5.0 %collective-permute-done.19.w3 = bf16[704,512]{1,0:T(8,128)(2,1)S(1)} collective-permute-done((bf16[704,512]{1,0:T(8,128)(2,1)S(1)}, bf16[704,512]{1,0:T(8,128)(2,1)S(1)}, u32[]{:S(2)}, u32[]{:S(2)}) %collective-permute-start.19) | collective-permute-done | bytes 720928 | tf_op jit(solution)/shard_map/ppermute | solution.py:403
  93.4 3.6 %collective-permute-done.14.a3 = bf16[256,384]{1,0:T(8,128)(2,1)S(1)} collective-permute-done((bf16[256,384]{1,0:T(8,128)(2,1)S(1)}, bf16[256,384]{1,0:T(8,128)(2,1)S(1)}, u32[]{:S(2)}, u32[]{:S(2)}) %collective-permute-start.14) | collective-permute-done | bytes 196640 | tf_op jit(solution)/shard_map/ppermute | solution.py:420
  97.0 3.9 %collective-permute-done.13.a2 = bf16[256,384]{1,0:T(8,128)(2,1)S(1)} collective-permute-done((bf16[256,384]{1,0:T(8,128)(2,1)S(1)}, bf16[256,384]{1,0:T(8,128)(2,1)S(1)}, u32[]{:S(2)}, u32[]{:S(2)}) %collective-permute-start.13) | collective-permute-done | bytes 196640 | tf_op jit(solution)/shard_map/ppermute | solution.py:420
  100.9 1.4 %shard_map.193 = bf16[384,512]{1,0:T(8,128)(2,1)} custom-call(bf16[256,384]{1,0:T(8,128)(2,1)S(1)} %shard_map.189.a0, bf16[256,384]{1,0:T(8,128)(2,1)S(1)} %collective-permute-done.12.a1, bf16[256,384]{1,0:T(8,128)(2,1)S(1)} %collective-permute-done.13.a2, bf16[256,384]{1,0:T(8,128)(2,1)S(1)} %collective-permute-done.14.a3, ...), custom_call_target="tpu_custom_call" | custom-call | flops 1000000000 | bytes 1048576 | tf_op jit(solution)/shard_map/pallas_call | solution.py:280
  (76 shorter events, 14.8 us)
Async XLA Ops:
  0.0 12.5 %collective-permute-start.1 = (bf16[384,512]{1,0:T(8,128)(2,1)}, bf16[384,512]{1,0:T(8,128)(2,1)S(1)}, u32[]{:S(2)}, u32[]{:S(2)}) collective-permute-start(bf16[384,512]{1,0:T(8,128)(2,1)} %refs_0_.1), channel_id=1, source_target_pairs={{0,1},{1,2},{2,3},{3,0},{4,5},{5,6},{6,7},{7,4},{8,9},{9,10},{10,1... | collective-permute-start | bytes 1179656 | tf_op jit(solution)/shard_map/ppermute | solution.py:319
  1.2 26.2 %collective-permute-start = (bf16[384,512]{1,0:T(8,128)(2,1)}, bf16[384,512]{1,0:T(8,128)(2,1)S(1)}, u32[]{:S(2)}, u32[]{:S(2)}) collective-permute-start(bf16[384,512]{1,0:T(8,128)(2,1)} %refs_0_.1), channel_id=1, source_target_pairs={{0,2},{1,3},{2,0},{3,1},{4,6},{5,7},{6,4},{7,5},{8,10},{9,11},{10,... | collective-permute-start | bytes 1179656 | tf_op jit(solution)/shard_map/ppermute | solution.py:321
  2.0 19.0 %collective-permute-start.2 = (bf16[384,512]{1,0:T(8,128)(2,1)}, bf16[384,512]{1,0:T(8,128)(2,1)S(1)}, u32[]{:S(2)}, u32[]{:S(2)}) collective-permute-start(bf16[384,512]{1,0:T(8,128)(2,1)} %refs_0_.1), channel_id=1, source_target_pairs={{0,3},{1,0},{2,1},{3,2},{4,7},{5,4},{6,5},{7,6},{8,11},{9,8},{10,9... | collective-permute-start | bytes 1179656 | tf_op jit(solution)/shard_map/ppermute | solution.py:320
  27.5 14.4 %copy-start = (bf16[2048,512]{1,0:T(8,128)(2,1)S(1)}, bf16[2048,512]{1,0:T(8,128)(2,1)}, u32[]{:S(2)}) copy-start(bf16[2048,512]{1,0:T(8,128)(2,1)} %wqd.1) | copy-start | bytes 6291460
  27.5 14.3 %copy-start.4 = (bf16[2048,256]{1,0:T(8,128)(2,1)S(1)}, bf16[2048,256]{1,0:T(8,128)(2,1)}, u32[]{:S(2)}) copy-start(bf16[2048,256]{1,0:T(8,128)(2,1)} %wpi.1) | copy-start | bytes 3145732
  27.5 14.3 %copy-start.10 = (bf16[512,384]{1,0:T(8,128)(2,1)S(1)}, bf16[512,384]{1,0:T(8,128)(2,1)}, u32[]{:S(2)}) copy-start(bf16[512,384]{1,0:T(8,128)(2,1)} %wqu.1) | copy-start | bytes 1179652
  28.6 6.8 %collective-permute-start.6 = (bf16[304,384]{1,0:T(8,128)(2,1)S(1)}, bf16[304,384]{1,0:T(8,128)(2,1)S(1)}, u32[]{:S(2)}, u32[]{:S(2)}) collective-permute-start(bf16[304,384]{1,0:T(8,128)(2,1)S(1)} %get-tuple-element.52.a), channel_id=1, source_target_pairs={{0,64},{4,20},{8,72},{12,28},{16,80},{20,4},{24,88},{28,12},{32,96... | collective-permute-start | bytes 700424 | tf_op jit(solution)/shard_map/ppermute | solution.py:370
  29.6 8.0 %collective-permute-start.5 = (bf16[304,384]{1,0:T(8,128)(2,1)S(1)}, bf16[304,384]{1,0:T(8,128)(2,1)S(1)}, u32[]{:S(2)}, u32[]{:S(2)}) collective-permute-start(bf16[304,384]{1,0:T(8,128)(2,1)S(1)} %get-tuple-element.52.a), channel_id=1, source_target_pairs={{0,96},{4,28},{8,104},{12,4},{16,112},{20,12},{24,120},{28,20},{32... | collective-permute-start | bytes 700424 | tf_op jit(solution)/shard_map/ppermute | solution.py:369
  29.6 8.0 %collective-permute-start.4 = (bf16[304,384]{1,0:T(8,128)(2,1)S(1)}, bf16[304,384]{1,0:T(8,128)(2,1)S(1)}, u32[]{:S(2)}, u32[]{:S(2)}) collective-permute-start(bf16[304,384]{1,0:T(8,128)(2,1)S(1)} %get-tuple-element.52.a), channel_id=1, source_target_pairs={{0,32},{4,12},{8,40},{12,20},{16,48},{20,28},{24,56},{28,4},{32,64... | collective-permute-start | bytes 700424 | tf_op jit(solution)/shard_map/ppermute | solution.py:368
  37.7 28.5 %collective-permute-start.9 = (bf16[304,1536]{1,0:T(8,128)(2,1)S(1)}, bf16[304,1536]{1,0:T(8,128)(2,1)S(1)}, u32[]{:S(2)}, u32[]{:S(2)}) collective-permute-start(bf16[304,1536]{1,0:T(8,128)(2,1)S(1)} %shard_map.185.refs_4_), channel_id=1, source_target_pairs={{0,24},{4,100},{8,0},{12,108},{16,8},{20,116},{24,16},{28,124},{32... | collective-permute-start | bytes 2801672 | tf_op jit(solution)/shard_map/ppermute | solution.py:390
  41.8 24.5 %collective-permute-start.7 = (bf16[304,1536]{1,0:T(8,128)(2,1)S(1)}, bf16[304,1536]{1,0:T(8,128)(2,1)S(1)}, u32[]{:S(2)}, u32[]{:S(2)}) collective-permute-start(bf16[304,1536]{1,0:T(8,128)(2,1)S(1)} %shard_map.185.refs_4_), channel_id=1, source_target_pairs={{0,8},{4,36},{8,16},{12,44},{16,24},{20,52},{24,0},{28,60},{32,40}... | collective-permute-start | bytes 2801672 | tf_op jit(solution)/shard_map/ppermute | solution.py:389
  43.6 18.0 %copy-start.18 = (bf16[256,512]{1,0:T(8,128)(2,1)S(1)}, bf16[256,512]{1,0:T(8,128)(2,1)}, u32[]{:S(2)}) copy-start(bf16[256,512]{1,0:T(8,128)(2,1)} %refs_2_.7) | copy-start | bytes 786436
  43.6 16.2 %collective-permute-start.3 = (bf16[4,96,384]{2,1,0:T(8,128)(2,1)S(1)}, bf16[4,96,384]{2,1,0:T(8,128)(2,1)S(1)}, u32[]{:S(2)}, u32[]{:S(2)}) collective-permute-start(bf16[4,96,384]{2,1,0:T(8,128)(2,1)S(1)} %get-tuple-element.51.refs_0_), channel_id=1, source_target_pairs={{0,4},{4,0},{8,12},{12,8},{16,20},{20,16},{24,28},{28,24},{32,36},... | collective-permute-start | bytes 884744 | tf_op jit(solution)/shard_map/ppermute | solution.py:380
  47.0 2.1 %collective-permute-start.15 = (bf16[8,256]{1,0:T(8,128)(2,1)S(1)}, bf16[8,256]{1,0:T(8,128)(2,1)S(1)}, u32[]{:S(2)}, u32[]{:S(2)}) collective-permute-start(bf16[8,256]{1,0:T(8,128)(2,1)S(1)} %get-tuple-element.59), channel_id=1, source_target_pairs={{0,4},{4,0},{8,12},{12,8},{16,20},{20,16},{24,28},{28,24},{32,36},... | collective-permute-start | bytes 12296 | tf_op jit(solution)/shard_map/ppermute | solution.py:381
  47.1 9.0 %collective-permute-start.16 = (bf16[8,256]{1,0:T(8,128)(2,1)S(1)}, bf16[8,256]{1,0:T(8,128)(2,1)S(1)}, u32[]{:S(2)}, u32[]{:S(2)}) collective-permute-start(bf16[8,256]{1,0:T(8,128)(2,1)S(1)} %get-tuple-element.61), channel_id=1, source_target_pairs={{4,8},{8,4},{12,16},{16,12},{20,24},{24,20},{28,32},{32,28},{36,40... | collective-permute-start | bytes 12296 | tf_op jit(solution)/shard_map/ppermute | solution.py:383
  57.9 27.5 %collective-permute-start.17 = (bf16[704,512]{1,0:T(8,128)(2,1)S(1)}, bf16[704,512]{1,0:T(8,128)(2,1)S(1)}, u32[]{:S(2)}, u32[]{:S(2)}) collective-permute-start(bf16[704,512]{1,0:T(8,128)(2,1)S(1)} %get-tuple-element.63), channel_id=1, source_target_pairs={{0,1},{1,2},{2,3},{3,0},{4,5},{5,6},{6,7},{7,4},{8,9},{9,10},{10,1... | collective-permute-start | bytes 2162696 | tf_op jit(solution)/shard_map/ppermute | solution.py:403
  59.0 28.9 %collective-permute-start.18 = (bf16[704,512]{1,0:T(8,128)(2,1)S(1)}, bf16[704,512]{1,0:T(8,128)(2,1)S(1)}, u32[]{:S(2)}, u32[]{:S(2)}) collective-permute-start(bf16[704,512]{1,0:T(8,128)(2,1)S(1)} %get-tuple-element.64), channel_id=1, source_target_pairs={{0,2},{1,3},{2,0},{3,1},{4,6},{5,7},{6,4},{7,5},{8,10},{9,11},{10,... | collective-permute-start | bytes 2162696 | tf_op jit(solution)/shard_map/ppermute | solution.py:403
  59.8 33.0 %collective-permute-start.19 = (bf16[704,512]{1,0:T(8,128)(2,1)S(1)}, bf16[704,512]{1,0:T(8,128)(2,1)S(1)}, u32[]{:S(2)}, u32[]{:S(2)}) collective-permute-start(bf16[704,512]{1,0:T(8,128)(2,1)S(1)} %get-tuple-element.65), channel_id=1, source_target_pairs={{0,3},{1,0},{2,1},{3,2},{4,7},{5,4},{6,5},{7,6},{8,11},{9,8},{10,9... | collective-permute-start | bytes 2162696 | tf_op jit(solution)/shard_map/ppermute | solution.py:403
  66.2 10.8 %collective-permute-start.10 = (bf16[152,1536]{1,0:T(8,128)(2,1)S(1)}, bf16[152,1536]{1,0:T(8,128)(2,1)S(1)}, u32[]{:S(2)}, u32[]{:S(2)}) collective-permute-start(bf16[152,1536]{1,0:T(8,128)(2,1)S(1)} %slice.9), channel_id=1, source_target_pairs={{0,24},{4,100},{8,0},{12,108},{16,8},{20,116},{24,16},{28,124},{32... | collective-permute-start | bytes 1400840 | tf_op jit(solution)/shard_map/ppermute | solution.py:393
  66.4 10.6 %collective-permute-start.8 = (bf16[152,1536]{1,0:T(8,128)(2,1)S(1)}, bf16[152,1536]{1,0:T(8,128)(2,1)S(1)}, u32[]{:S(2)}, u32[]{:S(2)}) collective-permute-start(bf16[152,1536]{1,0:T(8,128)(2,1)S(1)} %slice.8), channel_id=1, source_target_pairs={{0,8},{4,36},{8,16},{12,44},{16,24},{20,52},{24,0},{28,60},{32,40}... | collective-permute-start | bytes 1400840 | tf_op jit(solution)/shard_map/ppermute | solution.py:392
  81.9 1.9 %collective-permute-start.11 = (f32[4,80,384]{2,1,0:T(8,128)S(1)}, f32[4,80,384]{2,1,0:T(8,128)S(1)}, u32[]{:S(2)}, u32[]{:S(2)}) collective-permute-start(f32[4,80,384]{2,1,0:T(8,128)S(1)} %get-tuple-element.58), channel_id=1, source_target_pairs={{0,4},{4,0},{8,12},{12,8},{16,20},{20,16},{24,28},{28,24},{32,36},... | collective-permute-start | bytes 1474568 | tf_op jit(solution)/shard_map/ppermute | solution.py:418
  83.9 13.1 %collective-permute-start.14 = (bf16[256,384]{1,0:T(8,128)(2,1)S(1)}, bf16[256,384]{1,0:T(8,128)(2,1)S(1)}, u32[]{:S(2)}, u32[]{:S(2)}) collective-permute-start(bf16[256,384]{1,0:T(8,128)(2,1)S(1)} %shard_map.189.a0), channel_id=1, source_target_pairs={{0,3},{1,0},{2,1},{3,2},{4,7},{5,4},{6,5},{7,6},{8,11},{9,8},{10,9... | collective-permute-start | bytes 589832 | tf_op jit(solution)/shard_map/ppermute | solution.py:420
  85.4 15.5 %collective-permute-start.13 = (bf16[256,384]{1,0:T(8,128)(2,1)S(1)}, bf16[256,384]{1,0:T(8,128)(2,1)S(1)}, u32[]{:S(2)}, u32[]{:S(2)}) collective-permute-start(bf16[256,384]{1,0:T(8,128)(2,1)S(1)} %shard_map.189.a0), channel_id=1, source_target_pairs={{0,2},{1,3},{2,0},{3,1},{4,6},{5,7},{6,4},{7,5},{8,10},{9,11},{10,... | collective-permute-start | bytes 589832 | tf_op jit(solution)/shard_map/ppermute | solution.py:420
  85.4 15.5 %collective-permute-start.12 = (bf16[256,384]{1,0:T(8,128)(2,1)S(1)}, bf16[256,384]{1,0:T(8,128)(2,1)S(1)}, u32[]{:S(2)}, u32[]{:S(2)}) collective-permute-start(bf16[256,384]{1,0:T(8,128)(2,1)S(1)} %shard_map.189.a0), channel_id=1, source_target_pairs={{0,1},{1,2},{2,3},{3,0},{4,5},{5,6},{6,7},{7,4},{8,9},{9,10},{10,1... | collective-permute-start | bytes 589832 | tf_op jit(solution)/shard_map/ppermute | solution.py:420
  (15 other events, 136.3 us)

commit v2 on v1

v2 whole, which is shorter than its diff:
```python
import functools
import math

import jax
import jax.numpy as jnp
from jax import lax
from jax.experimental import pallas as pl
from jax.experimental.pallas import tpu as pltpu
from jax.sharding import PartitionSpec as P


NOPE = 64
ROPE = 32
VALUE_DIM = 64
HEAD = NOPE + ROPE
LATENT = 256
REACH = 8
eps = 1e-06
theta = 10000.0
bf = jnp.bfloat16
f32 = jnp.float32

PAY = LATENT + ROPE + 16
ACC = VALUE_DIM + 16


def sp_of(z, y, c):
    return (z % 4) * 8 + (y % 4) * 2 + c


SITES = [(z, y, c) for z in range(4) for y in range(4) for c in range(2)]
SWAP = [(sp_of(z, y, c), sp_of(z, y, 1 - c)) for z, y, c in SITES]


def along(step, second):
    pairs = []
    for z, y, c in SITES:
        on_z = (c == 0) != second
        pairs.append((sp_of(z, y, c), sp_of(z + step, y, c) if on_z else sp_of(z, y + step, c)))
    return pairs


def ring(step):
    return [(i, (i + step) % 4) for i in range(4)]


def params(mib=56):
    return pltpu.CompilerParams(vmem_limit_bytes=mib * 2**20)


VM = pl.BlockSpec(memory_space=pltpu.VMEM)
SM = pl.BlockSpec(memory_space=pltpu.SMEM)


def gained(x, gain):
    return (x * gain).astype(bf)


def load_kernel(*refs, count):
    outs, sems = refs[-count - 1 : -1], refs[-1]
    copies = [pltpu.make_async_copy(refs[i], outs[i], sems.at[i]) for i in range(count)]
    for copy in copies:
        copy.start()
    for copy in copies:
        copy.wait()


def project_kernel(ids, x0, x1, x2, gain, wl, wr, wqd, wpi, square, lat, raw, query, pool):
    values, ns, ats = pieces_of(ids, (x0, x1, x2), gain)
    total = sum(jnp.sum(x * x, axis=-1, keepdims=True) for x in values)
    square[...] = jnp.broadcast_to(total, square.shape)
    lat[...] = summed(ns, wl, ats)
    raw[...] = sum(product(n, wr[:, pl.ds(at, 512)], True) for n, at in zip(ns, ats))
    query[...] = summed(ns, wqd, ats)
    pool[...] = summed(ns, wpi, ats)


def pieces_of(ids, xs, gain):
    ats = [pl.multiple_of(ids[k] * 512, 512) for k in range(len(xs))]
    values = [x[...].astype(f32) for x in xs]
    return values, [gained(x, gain[:, pl.ds(at, 512)]) for x, at in zip(values, ats)], ats


def all_pieces(ids, x0, x1, x2, xa, xb, gain):
    _, ns, ats = pieces_of(ids, (x0, x1, x2), gain)
    _, n, at = last_piece(ids, xa, xb, gain)
    return ns + [n], ats + [at]


def summed(ns, w, ats):
    return sum(product(n, rows_at(w, at), False) for n, at in zip(ns, ats))


def product(n, w, turned):
    if turned:
        return lax.dot_general(w, n, (((1,), (1,)), ((), ())), preferred_element_type=f32)
    return jnp.dot(n, w, preferred_element_type=f32)


def rows_at(w, at):
    return w[pl.ds(at, 512), :]


def last_piece(ids, xa, xb, gain):
    at = pl.multiple_of(ids[3] * 512, 512)
    x = jnp.concatenate([xa[...], xb[...]], axis=0).astype(f32)
    return x, gained(x, gain[:, pl.ds(at, 512)]), at


def front_kernel(ids, xa, xb, gain, wl, wr, square, lat0, raw0, gains, cos, sin, pay, scale_out):
    x, n, at = last_piece(ids, xa, xb, gain)
    lgain, kgain = gains[:LATENT], gains[LATENT + NOPE : LATENT + HEAD]
    total = square[...] + jnp.broadcast_to(jnp.sum(x * x, axis=-1, keepdims=True), square.shape)
    scale = lax.rsqrt(total * (1.0 / 2048) + eps)
    scale_out[...] = scale
    lat = lat0[...] + product(n, rows_at(wl, at), False)
    lat = jnp.transpose(lat * scale[:, :1]).astype(bf).astype(f32)
    lat = lat * lax.rsqrt(jnp.mean(lat * lat, axis=0, keepdims=True) + eps) * lgain
    pay[:LATENT, :] = lat.astype(bf)
    raw = raw0[...] + product(n, wr[:, pl.ds(at, 512)], True)
    raw = (raw * jnp.transpose(scale)[:1]).astype(bf).astype(f32)
    total = jnp.sum(raw * raw, axis=0, keepdims=True)
    k = raw * kgain
    first, second = k[:16], k[16:]
    pay[LATENT : LATENT + 16, :] = (first * cos[...] - second * sin[...]).astype(bf)
    pay[LATENT + 16 : LATENT + 32, :] = (first * sin[...] + second * cos[...]).astype(bf)
    pay[LATENT + 32 :, :] = jnp.broadcast_to(total, (16, total.shape[1])).astype(bf)


def query_kernel(ids, xa, xb, gain, wqd, wpi, scale, query0, pool0, qgain, wqu, gains, cos, sin, q, pool_in, outer):
    _, n, at = last_piece(ids, xa, xb, gain)
    hgain = gains[LATENT + HEAD : LATENT + 2 * HEAD]
    s = scale[:, :1]
    pooled = (pool0[...] + product(n, rows_at(wpi, at), False)) * s
    pool_in[...] = pooled.astype(bf)
    head, end = pooled[:REACH], pooled[pooled.shape[0] - REACH :]
    on_first = ids[8] % 2 == 0
    inner = jnp.concatenate([jnp.where(on_first, end, head)] * 2, axis=0).astype(bf)
    q[q.shape[0] - 16 :, :] = jnp.concatenate([inner, inner[:, :128]], axis=1)
    outer[...] = jnp.where(on_first, head, end).astype(bf)
    lat = (query0[...] + product(n, rows_at(wqd, at), False)) * s
    lat = lat.astype(bf).astype(f32)
    lat = lat * lax.rsqrt(jnp.mean(lat * lat, axis=-1, keepdims=True) + eps) * qgain[...]
    raw = jnp.dot(lat.astype(bf), wqu[...], preferred_element_type=f32)
    raw = jnp.transpose(raw).astype(bf).astype(f32)
    for h in range(raw.shape[0] // HEAD):
        v = raw[h * HEAD : (h + 1) * HEAD]
        v = v * lax.rsqrt(jnp.mean(v * v, axis=0, keepdims=True) + eps) * hgain
        v = v * (HEAD**-0.5 / math.log(2.0))
        first, second = v[NOPE : NOPE + 16], v[NOPE + 16 :]
        base = h * HEAD
        q[base : base + NOPE, :] = v[:NOPE].astype(bf)
        q[base + NOPE : base + NOPE + 16, :] = (first * cos[...] - second * sin[...]).astype(bf)
        q[base + NOPE + 16 : base + HEAD, :] = (first * sin[...] + second * cos[...]).astype(bf)


def gate_kernel(ids, x0, x1, x2, xa, xb, gain, wa, wp, scale, gate_a, gate_p):
    ns, ats = all_pieces(ids, x0, x1, x2, xa, xb, gain)
    s = scale[:, :1]
    gate_a[...] = jax.nn.sigmoid(summed(ns, wa, ats) * s)
    gate_p[...] = jax.nn.sigmoid(summed(ns, wp, ats) * s)


def join_kernel(a, b, c, d, out):
    width = a.shape[1]
    for i, x in enumerate((a, b, c, d)):
        out[:, i * width : (i + 1) * width] = x[...]


def chosen(ids, packs, kind):
    mine, other = packs
    take_mine = ids[8] % 2 == kind
    return jnp.where(take_mine, mine[:256, :], other[:256, :])


def pool_merge_kernel(ids, pool, attn, own, f1, f2, f3, s1, s2, s3, gate_a, gate_p, out, attn_w):
    total = jnp.dot(pool[...], own[256:, :], preferred_element_type=f32)
    for k, (f, s) in enumerate(((f1, s1), (f2, s2), (f3, s3))):
        p = jnp.concatenate([f[256:, :256], f[256:, 256:]], axis=0)
        total = total + jnp.dot(p, chosen(ids, (f, s), 1), preferred_element_type=f32)
        attn_w[k * 256 : (k + 1) * 256, :] = chosen(ids, (f, s), 0)
    first = lax.dot_general(attn[...], own[:256, :], (((0,), (0,)), ((), ())), preferred_element_type=f32)
    out[...] = gate_p[...] * total + gate_a[...] * first


def pack_kernel(ids, inner, x, outer, mix, scale, wa, wp, pool, own, s1, s2, s3, padded, sum2, sum4, sum8):
    rows = x.shape[0]
    half, length = ids[9], ids[10]
    on_first = ids[8] % 2 == 0
    inner = inner[inner.shape[0] - 16 :, :256][:REACH].astype(f32)
    outer = outer[...].astype(f32)
    padded[0:REACH, :] = jnp.where(on_first, outer, inner)
    padded[REACH : REACH + rows, :] = x[...].astype(f32)
    padded[REACH + rows :, :] = jnp.where(on_first, inner, outer)
    n = rows + 2 * REACH
    sum2[: n - 1, :] = padded[: n - 1, :] + padded[1:n, :]
    sum4[: n - 3, :] = sum2[: n - 3, :] + sum2[2 : n - 1, :]
    sum8[: n - 7, :] = sum4[: n - 7, :] + sum4[4 : n - 3, :]
    total = sum8[:rows, :] + sum8[REACH : REACH + rows, :]
    total = jnp.where(half == 4, sum8[4 : 4 + rows, :], total)
    total = jnp.where(half == 2, sum4[6 : 6 + rows, :], total)
    total = jnp.where(half == 1, sum2[7 : 7 + rows, :], total)
    at = ids[8] * rows + lax.broadcasted_iota(jnp.int32, (rows, 1), 0)
    count = (jnp.clip(at + half, 0, length) - jnp.clip(at - half, 0, length)).astype(f32)
    mixed = (total / count - padded[REACH : REACH + rows, :]).astype(bf)
    out = (jnp.dot(mixed, mix[...], preferred_element_type=f32) * scale[...]).astype(bf)
    pool[...] = out
    at = pl.multiple_of(ids[4] * 512, 512)
    own[:256, :] = wa[:, pl.ds(at, 512)]
    own[256:, :] = wp[:, pl.ds(at, 512)]
    for d, s in ((1, s1), (2, s2), (3, s3)):
        at = pl.multiple_of(ids[4 + d] * 512, 512)
        s[:256, :] = jnp.where(on_first, wa[:, pl.ds(at, 512)], wp[:, pl.ds(at, 512)])
        s[256:, :256] = out[: rows // 2]
        s[256:, 256:] = out[rows // 2 :]


def attend_kernel(*refs, pieces, seeded):
    q0, q1, up, gains = refs[:4]
    refs = refs[4:]
    gain = gains[LATENT : LATENT + NOPE]
    n_in = sum(len(p) for p in pieces)
    blocks = refs[:n_in]
    refs = refs[n_in:]
    seeds, outs = (refs[:2], refs[2:]) if seeded else ((), refs)
    heads = q0.shape[0] // HEAD
    half = q0.shape[1]
    at = 0
    for number, piece in enumerate(pieces):
        parts = [blocks[at + i] for i in range(len(piece))]
        at += len(piece)
        whole = parts[0][...] if len(parts) == 1 else jnp.concatenate([p[...] for p in parts], axis=0)
        keys = whole.shape[1]
        latent = whole[:LATENT]
        rope = whole[LATENT : LATENT + ROPE].astype(f32)
        square = whole[LATENT + ROPE :].astype(f32)[0:1]
        expanded = lax.dot_general(up[...], latent, (((0,), (0,)), ((), ())), preferred_element_type=f32)
        row = lax.broadcasted_iota(jnp.int32, (16, keys), 0)
        ones = jnp.where(row == 0, 1.0, 0.0).astype(bf)
        for h in range(heads):
            k = expanded[h * 128 : h * 128 + NOPE]
            scale = lax.rsqrt((jnp.sum(k * k, axis=0, keepdims=True) + square) * (1.0 / HEAD) + eps)
            key = jnp.concatenate([(k * gain * scale).astype(bf), (rope * scale).astype(bf)], axis=0)
            query = jnp.concatenate([q[h * HEAD : (h + 1) * HEAD, :] for q in (q0, q1)], axis=1)
            scores = lax.dot_general(key, query, (((0,), (0,)), ((), ())), preferred_element_type=f32)
            weights = jnp.exp2(scores).astype(bf)
            v = jnp.concatenate([expanded[h * 128 + NOPE : (h + 1) * 128].astype(bf), ones], axis=0)
            add = jnp.dot(v, weights, preferred_element_type=f32)
            for i in range(2):
                part = add[:, i * half : (i + 1) * half]
                if number > 0:
                    outs[i][h] += part
                elif seeded:
                    outs[i][h] = (seeds[i][h] + part).astype(outs[i].dtype)
                else:
                    outs[i][h] = part


def attend(q0, q1, up, gains, pieces, seeds, sent_type=f32):
    heads, half = q0.shape[0] // HEAD, q0.shape[1]
    shape = jax.ShapeDtypeStruct((heads, ACC, half), f32)
    arrays = [a for p in pieces for a in p]
    keys = sum(p[0].shape[1] for p in pieces)
    kernel = functools.partial(
        attend_kernel, pieces=[[None] * len(p) for p in pieces], seeded=seeds is not None
    )
    return call(
        kernel,
        None,
        [q0, q1, up, gains, *[resident(a) for a in (*arrays, *(seeds or ()))]],
        [kept(shape), kept(jax.ShapeDtypeStruct(shape.shape, sent_type))],
        keys * heads * 2 * half * 2 * 512,
        mib=28,
        transcendentals=keys * heads * 2 * half,
    )


def finish_kernel(mine, other, out):
    for h in range(mine.shape[0]):
        both = mine[h] + other[h].astype(f32)
        out[h * VALUE_DIM : (h + 1) * VALUE_DIM, :] = (
            both[:VALUE_DIM] / both[VALUE_DIM : VALUE_DIM + 1]
        ).astype(bf)


def merge_kernel(a1, a2, a3, w, gate, rest, out):
    a = jnp.concatenate([a1[...], a2[...], a3[...]], axis=0)
    total = lax.dot_general(a, w[...], (((0,), (0,)), ((), ())), preferred_element_type=f32)
    out[...] = (gate[...] * total + rest[...]).astype(bf)


def resident(x):
    return pltpu.with_memory_space_constraint(x, pltpu.VMEM)


def kept(s):
    return pltpu.VMEM(s.shape, s.dtype)


def call(kernel, ids, ins, shapes, flops, scratch=(), mib=16, transcendentals=0, apart=()):
    first = [] if ids is None else [ids]
    ins = [pltpu.with_memory_space_constraint(x, pltpu.HBM) if i in apart else x for i, x in enumerate(ins)]
    return pl.pallas_call(
        kernel,
        in_specs=[SM] * len(first)
        + [pl.BlockSpec(memory_space=pltpu.HBM) if i in apart else VM for i in range(len(ins))],
        out_specs=jax.tree.map(lambda _: VM, shapes),
        out_shape=shapes,
        scratch_shapes=scratch,
        compiler_params=params(mib),
        cost_estimate=pl.CostEstimate(flops=flops, transcendentals=transcendentals, bytes_accessed=2**20),
    )(*first, *ins)


def whole(
    tokens,
    norm_gain,
    w_query_down,
    query_gain,
    w_query_up,
    w_latent_down,
    latent_gain,
    w_rotary_key,
    w_latent_up,
    query_head_gain,
    key_head_gain,
    w_pool_in,
    w_pool_mix,
    pool_scale,
    w_attn_out,
    w_pool_out,
    w_gate_attn,
    w_gate_pool,
):
    S = jax.ShapeDtypeStruct
    rows = tokens.shape[0]
    heads = w_query_up.shape[1] // HEAD
    length = rows * lax.axis_size("sp")
    here = lax.axis_index("sp")
    t = lax.axis_index("tp")

    x1 = lax.ppermute(tokens, "tp", ring(1))
    x2 = lax.ppermute(tokens, "tp", ring(-1))
    xa = lax.ppermute(x1[: rows // 2], "tp", ring(1))
    xb = lax.ppermute(x2[rows // 2 :], "tp", ring(-1))

    half = ROPE // 2
    freqs = theta ** (-jnp.arange(half, dtype=f32) / half)
    positions = (here * rows + jnp.arange(rows, dtype=jnp.int32)).astype(f32)
    angles = freqs[:, None] * positions[None, :]
    cos, sin = jnp.cos(angles), jnp.sin(angles)
    ids = jnp.concatenate(
        [
            (t + jnp.array([0, 3, 1, 2, 0, 1, 2, 3], jnp.int32)) & 3,
            jnp.stack([here, jnp.left_shift(1, t), jnp.int32(length)]).astype(jnp.int32),
        ]
    )
    gains = jnp.concatenate([latent_gain, key_head_gain, query_head_gain])[:, None]
    gain = norm_gain[None, :]
    wr = w_rotary_key.T

    wanted = [w_latent_down, wr, w_query_down, w_pool_in, w_query_up, gain, tokens, gains, cos, sin, query_gain[None, :]]
    wl, wr, wqd, wpi, wqu, gain, x0, near_gains, cos, sin, qgain = [
        resident(x)
        for x in call(
            functools.partial(load_kernel, count=11),
            None, [*wanted, ids], [kept(S(x.shape, x.dtype)) for x in wanted], 4 * 10**8,
            [pltpu.SemaphoreType.DMA((11,))], apart=range(12),
        )
    ]
    square, lat0, raw0, query0, pool0 = [
        resident(x)
        for x in call(
            project_kernel,
            ids, [x0, resident(x1), resident(x2), gain, wl, wr, wqd, wpi],
            [kept(S(s, f32)) for s in ((rows, 128), (rows, LATENT), (ROPE, rows), (rows, 512), (rows, 256))],
            16 * 10**8,
        )
    ]
    pay, scale = call(
        front_kernel,
        ids,
        [resident(xa), resident(xb), gain, wl, wr, square, lat0, raw0, near_gains, cos, sin],
        [kept(S((PAY, rows), bf)), kept(S((rows, 128), f32))],
        3 * 10**8,
    )
    pieces = [tokens, x1, x2, xa, xb]

    a1 = lax.ppermute(pay, "sp", along(1, False))
    a2 = lax.ppermute(pay, "sp", along(-1, False))
    a3 = lax.ppermute(pay, "sp", along(2, False))

    q, pool_in, outer = call(
        query_kernel,
        ids,
        [resident(xa), resident(xb), gain, wqd, wpi, resident(scale), query0, pool0, qgain,
         wqu, near_gains, cos, sin],
        [S((heads * HEAD + 16, rows), bf), S((rows, 256), bf), S((REACH, 256), bf)],
        10**9,
    )
    q_other = lax.ppermute(q, "sp", SWAP)
    count = lax.axis_size("sp")
    outer = lax.ppermute(outer, "sp", [(i, i - 1 + 2 * (i % 2)) for i in range(1, count - 1)])

    def attend_on(pieces, seeds, name):
        return attend(q, q_other, w_latent_up, gains, pieces, seeds, bf if name == "attend_far" else f32)

    line = call(join_kernel, None, [resident(x) for x in (pay, a1, a2, a3)], kept(S((PAY, 4 * rows), bf)), 10**7)
    b1 = lax.ppermute(line, "sp", along(1, True))
    b2 = lax.ppermute(line, "sp", along(-1, True))
    cut = PAY // 2
    b3 = lax.ppermute(b1[:cut], "sp", along(1, True))
    b4 = lax.ppermute(b2[cut:], "sp", along(-1, True))

    pool, own_w, *packs = call(
        pack_kernel,
        ids,
        [q_other, pool_in, outer, w_pool_mix[0], pool_scale[None, :], w_attn_out, w_pool_out],
        [S((rows, 256), bf), S((512, 512), bf)] + [S((448, 512), bf)] * 3,
        10**8,
        [pltpu.VMEM((rows + 2 * REACH, 256), f32)] * 4,
    )
    packs = [lax.ppermute(packs[d - 1], "tp", ring(d)) for d in (1, 2, 3)]
    swapped = [lax.ppermute(p, "sp", SWAP) for p in packs]
    weights = [own_w, *packs, *swapped]

    acc = attend_on([[line]], None, "attend_line")
    acc = attend_on([[b1], [b2]], acc, "attend_near")
    acc = attend_on([[b3, b4]], acc, "attend_far")

    gate_attn, gate_pool = call(
        gate_kernel,
        ids,
        [*pieces, norm_gain[None, :], w_gate_attn, w_gate_pool, scale],
        [kept(S((rows, 512), f32))] * 2,
        5 * 10**8,
    )
    other = lax.ppermute(acc[1], "sp", SWAP)
    attn = call(finish_kernel, None, [resident(acc[0]), resident(other)], kept(S((heads * VALUE_DIM, rows), bf)), 10**7)
    attns = [attn] + [lax.ppermute(attn, "tp", ring(d)) for d in (1, 2, 3)]
    rest, attn_w = call(
        pool_merge_kernel, ids, [pool, attn, *weights, resident(gate_attn), resident(gate_pool)],
        [kept(S((rows, 512), f32)), kept(S((768, 512), bf))], 10**9,
    )
    return call(
        merge_kernel,
        None,
        [*[resident(a) for a in attns[1:]], resident(attn_w), resident(gate_attn), resident(rest)],
        S((rows, 512), bf), 10**9,
    )


def solution(mesh):
    placed = (
        P("sp", "tp"),
        P(),
        P(),
        P(),
        P(None, "tp"),
        P(),
        P(),
        P(),
        P(None, "tp"),
        P(),
        P(),
        P(None, "tp"),
        P("tp", None, None),
        P("tp"),
        P("tp", None),
        P("tp", None),
        P(None, "tp"),
        P(None, "tp"),
    )
    return jax.shard_map(whole, mesh=mesh, in_specs=placed, out_specs=P("sp", "tp"), check_vma=False)
```

time: 103 us -> 111 us (1.078)
  the two profiles are of different devices: /device:TPU:27 before, /device:TPU:0 now
where the time goes in v2:
time: 111 us
  starting transfers between devices  49.4 us (45%)
  Pallas kernels  32.5 us (29%)
  waiting for transfers between devices  24.7 us (22%)
  other arithmetic  2.85 us (3%)
    pallas_call x13, Pallas kernels, call(): pl.pallas_call(kernel, in_specs=[SM] * len(first) + [pl.BlockSpec(memory_...  32.5 us
    ppermute x3, starting transfers between devices, whole(): swapped = [lax.ppermute(p, 'sp', SWAP) for p in packs]  15.5 us
    ppermute x1, starting transfers between devices, whole(): b4 = lax.ppermute(b2[cut:], 'sp', along(-1, True))  8.36 us
    ppermute x3, waiting for transfers between devices, whole(): attns = [attn] + [lax.ppermute(attn, 'tp', ring(d)) for d in (1, 2, 3)]  7.47 us
    ppermute x1, waiting for transfers between devices, whole(): x2 = lax.ppermute(tokens, 'tp', ring(-1))  6.44 us
    ppermute x1, waiting for transfers between devices, whole(): a2 = lax.ppermute(pay, 'sp', along(-1, False))  4.1 us
    ppermute x3, starting transfers between devices, whole(): packs = [lax.ppermute(packs[d - 1], 'tp', ring(d)) for d in (1, 2, 3)]  4.01 us
    ppermute x1, starting transfers between devices, whole(): a3 = lax.ppermute(pay, 'sp', along(2, False))  3.96 us
  transfers between devices with their start and end apart: 23, of which 11 were waited for; matrix products, arithmetic and copies ran while one was open for 3% of the time, Pallas kernels for 27%

profile of v2, /device:TPU:0, one launch (start us, length us, event | category | flops | bytes accessed | tf_op | source)
XLA Modules:
  0.0 110.6 jit_solution(16388477008742852382)
XLA Ops:
  0.0 2.9 %collective-permute-start.2 = (bf16[384,512]{1,0:T(8,128)(2,1)}, bf16[384,512]{1,0:T(8,128)(2,1)S(1)}, u32[]{:S(2)}, u32[]{:S(2)}) collective-permute-start(bf16[384,512]{1,0:T(8,128)(2,1)} %x0.1), channel_id=1, source_target_pairs={{0,3},{1,0},{2,1},{3,2},{4,7},{5,4},{6,5},{7,6},{8,11},{9,8},{10,9... | collective-permute-start | bytes 1179656 | tf_op jit(solution)/shard_map/ppermute | solution.py:343
  5.1 6.4 %collective-permute-done.2.x2 = bf16[384,512]{1,0:T(8,128)(2,1)S(1)} collective-permute-done((bf16[384,512]{1,0:T(8,128)(2,1)}, bf16[384,512]{1,0:T(8,128)(2,1)S(1)}, u32[]{:S(2)}, u32[]{:S(2)}) %collective-permute-start.2) | collective-permute-done | bytes 393248 | tf_op jit(solution)/shard_map/ppermute | solution.py:343
  11.6 3.7 %collective-permute-start.3 = (bf16[192,512]{1,0:T(8,128)(2,1)S(1)}, bf16[192,512]{1,0:T(8,128)(2,1)S(1)}, u32[]{:S(2)}, u32[]{:S(2)}) collective-permute-start(bf16[192,512]{1,0:T(8,128)(2,1)S(1)} %slice.17), channel_id=1, source_target_pairs={{0,3},{1,0},{2,1},{3,2},{4,7},{5,4},{6,5},{7,6},{8,11},{9,8},{10,9... | collective-permute-start | bytes 589832 | tf_op jit(solution)/shard_map/ppermute | solution.py:345
  16.8 2.6 %shard_map.181 = (bf16[2048,256]{1,0:T(8,128)(2,1)S(1)}, bf16[32,2048]{1,0:T(8,128)(2,1)S(1)}, bf16[2048,512]{1,0:T(8,128)(2,1)S(1)}, bf16[2048,256]{1,0:T(8,128...) custom-call(bf16[2048,256]{1,0:T(8,128)(2,1)} %refs_0_.1, ...), custom_call_target="tpu_custom_call" | custom-call | flops 400000000 | bytes 1048576 | tf_op jit(solution)/shard_map/pallas_call | solution.py:303
  19.4 2.3 %shard_map.182 = (f32[384,128]{1,0:T(8,128)S(1)}, f32[384,256]{1,0:T(8,128)S(1)}, f32[32,384]{1,0:T(8,128)S(1)}, f32[384,512]{1,0:T(8,128)S(1)}, f32[384,256]{1,0:T(8,128)S(1)}) custom-call(s32[11]{0:T(128)S(1)} %copy-done.8, bf16[384,512]{1,0:T(8,128)(2,1)S(1)} %get-tuple-element.46.x0, bf16[384,512]{1,0:T(8,128)(2,1)S(1)} %collective-permute-done.x1, ...), custom_call_target="tpu_custom_call" | custom-call | flops 1600000000 | bytes 1048576 | tf_op jit(solution)/shard_map/pallas_call | solution.py:303
  23.3 4.0 %collective-permute-start.7 = (bf16[304,384]{1,0:T(8,128)(2,1)S(1)}, bf16[304,384]{1,0:T(8,128)(2,1)S(1)}, u32[]{:S(2)}, u32[]{:S(2)}) collective-permute-start(bf16[304,384]{1,0:T(8,128)(2,1)S(1)} %get-tuple-element.59.a), channel_id=1, source_target_pairs={{0,64},{4,20},{8,72},{12,28},{16,80},{20,4},{24,88},{28,12},{32,96... | collective-permute-start | bytes 700424 | tf_op jit(solution)/shard_map/ppermute | solution.py:391
  27.9 1.3 %collective-permute-start.5 = (bf16[304,384]{1,0:T(8,128)(2,1)S(1)}, bf16[304,384]{1,0:T(8,128)(2,1)S(1)}, u32[]{:S(2)}, u32[]{:S(2)}) collective-permute-start(bf16[304,384]{1,0:T(8,128)(2,1)S(1)} %get-tuple-element.59.a), channel_id=1, source_target_pairs={{0,32},{4,12},{8,40},{12,20},{16,48},{20,28},{24,56},{28,4},{32,64... | collective-permute-start | bytes 700424 | tf_op jit(solution)/shard_map/ppermute | solution.py:389
  29.3 2.0 %collective-permute-done.7.d = bf16[304,384]{1,0:T(8,128)(2,1)S(1)} collective-permute-done((bf16[304,384]{1,0:T(8,128)(2,1)S(1)}, bf16[304,384]{1,0:T(8,128)(2,1)S(1)}, u32[]{:S(2)}, u32[]{:S(2)}) %collective-permute-start.7) | collective-permute-done | bytes 233504 | tf_op jit(solution)/shard_map/ppermute | solution.py:391
  31.3 4.1 %collective-permute-done.6.c = bf16[304,384]{1,0:T(8,128)(2,1)S(1)} collective-permute-done((bf16[304,384]{1,0:T(8,128)(2,1)S(1)}, bf16[304,384]{1,0:T(8,128)(2,1)S(1)}, u32[]{:S(2)}, u32[]{:S(2)}) %collective-permute-start.6) | collective-permute-done | bytes 233504 | tf_op jit(solution)/shard_map/ppermute | solution.py:390
  35.5 3.8 %collective-permute-start.10 = (bf16[304,1536]{1,0:T(8,128)(2,1)S(1)}, bf16[304,1536]{1,0:T(8,128)(2,1)S(1)}, u32[]{:S(2)}, u32[]{:S(2)}) collective-permute-start(bf16[304,1536]{1,0:T(8,128)(2,1)S(1)} %shard_map.185.refs_4_), channel_id=1, source_target_pairs={{0,24},{4,100},{8,0},{12,108},{16,8},{20,116},{24,16},{28,124},{32... | collective-permute-start | bytes 2801672 | tf_op jit(solution)/shard_map/ppermute | solution.py:410
  39.3 1.7 %shard_map.184 = (bf16[400,384]{1,0:T(8,128)(2,1)S(1)}, bf16[384,256]{1,0:T(8,128)(2,1)S(1)}, bf16[8,256]{1,0:T(8,128)(2,1)S(1)}) custom-call(s32[11]{0:T(128)S(1)} %copy-done.8, bf16[192,512]{1,0:T(8,128)(2,1)S(1)} %collective-permute-done.1.xa, bf16[192,512]{1,0:T(8,128)(2,1)S(1)} %collective-permute-done.3.xb, f32[1,2048]{1,0:T(1,128)S(1)} %get-tuple-element.41.gain, ...), custom_call_target="tpu_custom_call" | custom-call | flops 1000000000 | bytes 1048576 | tf_op jit(solution)/shard_map/pallas_call | solution.py:303
  42.7 1.3 %shard_map.190 = (bf16[384,256]{1,0:T(8,128)(2,1)S(1)}, bf16[512,512]{1,0:T(8,128)(2,1)S(1)}, bf16[448,512]{1,0:T(8,128)(2,1)S(1)}, bf16[448,512]{1,0:T(8,128)(2,1)S(1)}, bf16[448,512]{1,0:T(8,128)(2,1)S(1)}) custom-call(s32[11]{0:T(128)S(1)} %copy-done.8, bf16[400,384]{1,0:T(8,128)(2,1)S(1)} %collective-permute-done.4.refs_1_.inner, ...), custom_call_target="tpu_custom_call" | custom-call | flops 100000000 | bytes 1048576 | tf_op jit(solution)/shard_map/pallas_call | solution.py:303
  44.1 3.9 %collective-permute-start.18 = (bf16[448,512]{1,0:T(8,128)(2,1)S(1)}, bf16[448,512]{1,0:T(8,128)(2,1)S(1)}, u32[]{:S(2)}, u32[]{:S(2)}) collective-permute-start(bf16[448,512]{1,0:T(8,128)(2,1)S(1)} %get-tuple-element.71), channel_id=1, source_target_pairs={{0,2},{1,3},{2,0},{3,1},{4,6},{5,7},{6,4},{7,5},{8,10},{9,11},{10,... | collective-permute-start | bytes 1376264 | tf_op jit(solution)/shard_map/ppermute | solution.py:423
  48.1 4.6 %shard_map.186 = (f32[4,80,384]{2,1,0:T(8,128)S(1)}, f32[4,80,384]{2,1,0:T(8,128)S(1)}) custom-call(bf16[400,384]{1,0:T(8,128)(2,1)S(1)} %get-tuple-element.58.refs_0_, bf16[400,384]{1,0:T(8,128)(2,1)S(1)} %collective-permute-done.4.refs_1_.inner, bf16[256,512]{1,0:T(8,128)(2,1)S(1)} %copy-done.10, f32[448,1]{1,0:T(8,128)S(1)} %copy-done.5, ...), custom_call_target="tpu_custom_call" | custom-call | flops 4831838208 | bytes 1048576 | tf_op jit(solution)/shard_map/pallas_call | solution.py:303
  53.8 10.3 %collective-permute-start.20 = (bf16[448,512]{1,0:T(8,128)(2,1)S(1)}, bf16[448,512]{1,0:T(8,128)(2,1)S(1)}, u32[]{:S(2)}, u32[]{:S(2)}) collective-permute-start(bf16[448,512]{1,0:T(8,128)(2,1)S(1)} %collective-permute-done.17.f1), channel_id=1, source_target_pairs={{0,4},{4,0},{8,12},{12,8},{16,20},{20,16},{24,28},{28,24},{32,36},... | collective-permute-start | bytes 1376264 | tf_op jit(solution)/shard_map/ppermute | solution.py:424
  64.1 5.0 %collective-permute-start.21 = (bf16[448,512]{1,0:T(8,128)(2,1)S(1)}, bf16[448,512]{1,0:T(8,128)(2,1)S(1)}, u32[]{:S(2)}, u32[]{:S(2)}) collective-permute-start(bf16[448,512]{1,0:T(8,128)(2,1)S(1)} %collective-permute-done.18.f2), channel_id=1, source_target_pairs={{0,4},{4,0},{8,12},{12,8},{16,20},{20,16},{24,28},{28,24},{32,36},... | collective-permute-start | bytes 1376264 | tf_op jit(solution)/shard_map/ppermute | solution.py:424
  69.3 8.4 %collective-permute-start.11 = (bf16[152,1536]{1,0:T(8,128)(2,1)S(1)}, bf16[152,1536]{1,0:T(8,128)(2,1)S(1)}, u32[]{:S(2)}, u32[]{:S(2)}) collective-permute-start(bf16[152,1536]{1,0:T(8,128)(2,1)S(1)} %slice.19), channel_id=1, source_target_pairs={{0,24},{4,100},{8,0},{12,108},{16,8},{20,116},{24,16},{28,124},{32... | collective-permute-start | bytes 1400840 | tf_op jit(solution)/shard_map/ppermute | solution.py:413
  78.0 9.1 %shard_map.187 = (f32[4,80,384]{2,1,0:T(8,128)S(1)}, f32[4,80,384]{2,1,0:T(8,128)S(1)}) custom-call(bf16[400,384]{1,0:T(8,128)(2,1)S(1)} %get-tuple-element.58.refs_0_, bf16[400,384]{1,0:T(8,128)(2,1)S(1)} %collective-permute-done.4.refs_1_.inner, bf16[256,512]{1,0:T(8,128)(2,1)S(1)} %copy-done.10, f32[448,1]{1,0:T(8,128)S(1)} %copy-done.5, ...), custom_call_target="tpu_custom_call" | custom-call | flops 9663676416 | bytes 1048576 | tf_op jit(solution)/shard_map/pallas_call | solution.py:303
  87.8 4.9 %shard_map.188 = (f32[4,80,384]{2,1,0:T(8,128)S(1)}, bf16[4,80,384]{2,1,0:T(8,128)(2,1)S(1)}) custom-call(bf16[400,384]{1,0:T(8,128)(2,1)S(1)} %get-tuple-element.58.refs_0_, bf16[400,384]{1,0:T(8,128)(2,1)S(1)} %collective-permute-done.4.refs_1_.inner, bf16[256,512]{1,0:T(8,128)(2,1)S(1)} %copy-done.10, f32[448,1]{1,0:T(8,128)S(1)} %copy-done.5, ...), custom_call_target="tpu_custom_call" | custom-call | flops 4831838208 | bytes 1048576 | tf_op jit(solution)/shard_map/pallas_call | solution.py:303
  92.8 1.5 %collective-permute-done.12.other = bf16[4,80,384]{2,1,0:T(8,128)(2,1)S(1)} collective-permute-done((bf16[4,80,384]{2,1,0:T(8,128)(2,1)S(1)}, bf16[4,80,384]{2,1,0:T(8,128)(2,1)S(1)}, u32[]{:S(2)}, u32[]{:S(2)}) %collective-permute-start.12) | collective-permute-done | bytes 245792 | tf_op jit(solution)/shard_map/ppermute | solution.py:438
  94.3 2.9 %collective-permute-start.15 = (bf16[256,384]{1,0:T(8,128)(2,1)S(1)}, bf16[256,384]{1,0:T(8,128)(2,1)S(1)}, u32[]{:S(2)}, u32[]{:S(2)}) collective-permute-start(bf16[256,384]{1,0:T(8,128)(2,1)S(1)} %shard_map.189.attn), channel_id=1, source_target_pairs={{0,3},{1,0},{2,1},{3,2},{4,7},{5,4},{6,5},{7,6},{8,11},{9,8},{10,9... | collective-permute-start | bytes 589832 | tf_op jit(solution)/shard_map/ppermute | solution.py:440
  98.2 2.4 %shard_map.191 = (f32[384,512]{1,0:T(8,128)S(1)}, f32[384,512]{1,0:T(8,128)S(1)}) custom-call(s32[11]{0:T(128)S(1)} %copy-done.8, bf16[384,512]{1,0:T(8,128)(2,1)S(1)} %copy-done.2, bf16[384,512]{1,0:T(8,128)(2,1)S(1)} %collective-permute-done.x1, bf16[384,512]{1,0:T(8,128)(2,1)S(1)} %collective-permute-done.2.x2, ...), custom_call_target="tpu_custom_call" | custom-call | flops 500000000 | bytes 1048576 | tf_op jit(solution)/shard_map/pallas_call | solution.py:303
  101.9 4.0 %collective-permute-done.15.a3 = bf16[256,384]{1,0:T(8,128)(2,1)S(1)} collective-permute-done((bf16[256,384]{1,0:T(8,128)(2,1)S(1)}, bf16[256,384]{1,0:T(8,128)(2,1)S(1)}, u32[]{:S(2)}, u32[]{:S(2)}) %collective-permute-start.15) | collective-permute-done | bytes 196640 | tf_op jit(solution)/shard_map/ppermute | solution.py:440
  106.5 2.8 %collective-permute-done.13.a1 = bf16[256,384]{1,0:T(8,128)(2,1)S(1)} collective-permute-done((bf16[256,384]{1,0:T(8,128)(2,1)S(1)}, bf16[256,384]{1,0:T(8,128)(2,1)S(1)}, u32[]{:S(2)}, u32[]{:S(2)}) %collective-permute-start.13) | collective-permute-done | bytes 196640 | tf_op jit(solution)/shard_map/ppermute | solution.py:440
  (68 shorter events, 14.5 us)
Async XLA Ops:
  0.0 11.6 %collective-permute-start.2 = (bf16[384,512]{1,0:T(8,128)(2,1)}, bf16[384,512]{1,0:T(8,128)(2,1)S(1)}, u32[]{:S(2)}, u32[]{:S(2)}) collective-permute-start(bf16[384,512]{1,0:T(8,128)(2,1)} %x0.1), channel_id=1, source_target_pairs={{0,3},{1,0},{2,1},{3,2},{4,7},{5,4},{6,5},{7,6},{8,11},{9,8},{10,9... | collective-permute-start | bytes 1179656 | tf_op jit(solution)/shard_map/ppermute | solution.py:343
  2.9 12.4 %collective-permute-start = (bf16[384,512]{1,0:T(8,128)(2,1)}, bf16[384,512]{1,0:T(8,128)(2,1)S(1)}, u32[]{:S(2)}, u32[]{:S(2)}) collective-permute-start(bf16[384,512]{1,0:T(8,128)(2,1)} %x0.1), channel_id=1, source_target_pairs={{0,1},{1,2},{2,3},{3,0},{4,5},{5,6},{6,7},{7,4},{8,9},{9,10},{10,1... | collective-permute-start | bytes 1179656 | tf_op jit(solution)/shard_map/ppermute | solution.py:342
  11.6 10.1 %collective-permute-start.3 = (bf16[192,512]{1,0:T(8,128)(2,1)S(1)}, bf16[192,512]{1,0:T(8,128)(2,1)S(1)}, u32[]{:S(2)}, u32[]{:S(2)}) collective-permute-start(bf16[192,512]{1,0:T(8,128)(2,1)S(1)} %slice.17), channel_id=1, source_target_pairs={{0,3},{1,0},{2,1},{3,2},{4,7},{5,4},{6,5},{7,6},{8,11},{9,8},{10,9... | collective-permute-start | bytes 589832 | tf_op jit(solution)/shard_map/ppermute | solution.py:345
  15.3 6.9 %collective-permute-start.1 = (bf16[192,512]{1,0:T(8,128)(2,1)S(1)}, bf16[192,512]{1,0:T(8,128)(2,1)S(1)}, u32[]{:S(2)}, u32[]{:S(2)}) collective-permute-start(bf16[192,512]{1,0:T(8,128)(2,1)S(1)} %slice.16), channel_id=1, source_target_pairs={{0,1},{1,2},{2,3},{3,0},{4,5},{5,6},{6,7},{7,4},{8,9},{9,10},{10,1... | collective-permute-start | bytes 589832 | tf_op jit(solution)/shard_map/ppermute | solution.py:344
  23.3 8.0 %collective-permute-start.7 = (bf16[304,384]{1,0:T(8,128)(2,1)S(1)}, bf16[304,384]{1,0:T(8,128)(2,1)S(1)}, u32[]{:S(2)}, u32[]{:S(2)}) collective-permute-start(bf16[304,384]{1,0:T(8,128)(2,1)S(1)} %get-tuple-element.59.a), channel_id=1, source_target_pairs={{0,64},{4,20},{8,72},{12,28},{16,80},{20,4},{24,88},{28,12},{32,96... | collective-permute-start | bytes 700424 | tf_op jit(solution)/shard_map/ppermute | solution.py:391
  27.2 8.2 %collective-permute-start.6 = (bf16[304,384]{1,0:T(8,128)(2,1)S(1)}, bf16[304,384]{1,0:T(8,128)(2,1)S(1)}, u32[]{:S(2)}, u32[]{:S(2)}) collective-permute-start(bf16[304,384]{1,0:T(8,128)(2,1)S(1)} %get-tuple-element.59.a), channel_id=1, source_target_pairs={{0,96},{4,28},{8,104},{12,4},{16,112},{20,12},{24,120},{28,20},{32... | collective-permute-start | bytes 700424 | tf_op jit(solution)/shard_map/ppermute | solution.py:390
  27.9 7.4 %collective-permute-start.5 = (bf16[304,384]{1,0:T(8,128)(2,1)S(1)}, bf16[304,384]{1,0:T(8,128)(2,1)S(1)}, u32[]{:S(2)}, u32[]{:S(2)}) collective-permute-start(bf16[304,384]{1,0:T(8,128)(2,1)S(1)} %get-tuple-element.59.a), channel_id=1, source_target_pairs={{0,32},{4,12},{8,40},{12,20},{16,48},{20,28},{24,56},{28,4},{32,64... | collective-permute-start | bytes 700424 | tf_op jit(solution)/shard_map/ppermute | solution.py:389
  35.5 33.8 %collective-permute-start.10 = (bf16[304,1536]{1,0:T(8,128)(2,1)S(1)}, bf16[304,1536]{1,0:T(8,128)(2,1)S(1)}, u32[]{:S(2)}, u32[]{:S(2)}) collective-permute-start(bf16[304,1536]{1,0:T(8,128)(2,1)S(1)} %shard_map.185.refs_4_), channel_id=1, source_target_pairs={{0,24},{4,100},{8,0},{12,108},{16,8},{20,116},{24,16},{28,124},{32... | collective-permute-start | bytes 2801672 | tf_op jit(solution)/shard_map/ppermute | solution.py:410
  39.3 38.4 %collective-permute-start.8 = (bf16[304,1536]{1,0:T(8,128)(2,1)S(1)}, bf16[304,1536]{1,0:T(8,128)(2,1)S(1)}, u32[]{:S(2)}, u32[]{:S(2)}) collective-permute-start(bf16[304,1536]{1,0:T(8,128)(2,1)S(1)} %shard_map.185.refs_4_), channel_id=1, source_target_pairs={{0,8},{4,36},{8,16},{12,44},{16,24},{20,52},{24,0},{28,60},{32,40}... | collective-permute-start | bytes 2801672 | tf_op jit(solution)/shard_map/ppermute | solution.py:409
  41.0 1.7 %collective-permute-start.4 = (bf16[400,384]{1,0:T(8,128)(2,1)S(1)}, bf16[400,384]{1,0:T(8,128)(2,1)S(1)}, u32[]{:S(2)}, u32[]{:S(2)}) collective-permute-start(bf16[400,384]{1,0:T(8,128)(2,1)S(1)} %get-tuple-element.58.refs_0_), channel_id=1, source_target_pairs={{0,4},{4,0},{8,12},{12,8},{16,20},{20,16},{24,28},{28,24},{32,36},... | collective-permute-start | bytes 921608 | tf_op jit(solution)/shard_map/ppermute | solution.py:401
  41.1 0.8 collective-permute-start.16
  44.0 9.8 %collective-permute-start.17 = (bf16[448,512]{1,0:T(8,128)(2,1)S(1)}, bf16[448,512]{1,0:T(8,128)(2,1)S(1)}, u32[]{:S(2)}, u32[]{:S(2)}) collective-permute-start(bf16[448,512]{1,0:T(8,128)(2,1)S(1)} %get-tuple-element.70), channel_id=1, source_target_pairs={{0,1},{1,2},{2,3},{3,0},{4,5},{5,6},{6,7},{7,4},{8,9},{9,10},{10,1... | collective-permute-start | bytes 1376264 | tf_op jit(solution)/shard_map/ppermute | solution.py:423
  44.1 20.0 %collective-permute-start.18 = (bf16[448,512]{1,0:T(8,128)(2,1)S(1)}, bf16[448,512]{1,0:T(8,128)(2,1)S(1)}, u32[]{:S(2)}, u32[]{:S(2)}) collective-permute-start(bf16[448,512]{1,0:T(8,128)(2,1)S(1)} %get-tuple-element.71), channel_id=1, source_target_pairs={{0,2},{1,3},{2,0},{3,1},{4,6},{5,7},{6,4},{7,5},{8,10},{9,11},{10,... | collective-permute-start | bytes 1376264 | tf_op jit(solution)/shard_map/ppermute | solution.py:423
  48.1 21.0 %collective-permute-start.19 = (bf16[448,512]{1,0:T(8,128)(2,1)S(1)}, bf16[448,512]{1,0:T(8,128)(2,1)S(1)}, u32[]{:S(2)}, u32[]{:S(2)}) collective-permute-start(bf16[448,512]{1,0:T(8,128)(2,1)S(1)} %get-tuple-element.72), channel_id=1, source_target_pairs={{0,3},{1,0},{2,1},{3,2},{4,7},{5,4},{6,5},{7,6},{8,11},{9,8},{10,9... | collective-permute-start | bytes 1376264 | tf_op jit(solution)/shard_map/ppermute | solution.py:423
  53.8 43.5 %collective-permute-start.20 = (bf16[448,512]{1,0:T(8,128)(2,1)S(1)}, bf16[448,512]{1,0:T(8,128)(2,1)S(1)}, u32[]{:S(2)}, u32[]{:S(2)}) collective-permute-start(bf16[448,512]{1,0:T(8,128)(2,1)S(1)} %collective-permute-done.17.f1), channel_id=1, source_target_pairs={{0,4},{4,0},{8,12},{12,8},{16,20},{20,16},{24,28},{28,24},{32,36},... | collective-permute-start | bytes 1376264 | tf_op jit(solution)/shard_map/ppermute | solution.py:424
  64.1 36.5 %collective-permute-start.21 = (bf16[448,512]{1,0:T(8,128)(2,1)S(1)}, bf16[448,512]{1,0:T(8,128)(2,1)S(1)}, u32[]{:S(2)}, u32[]{:S(2)}) collective-permute-start(bf16[448,512]{1,0:T(8,128)(2,1)S(1)} %collective-permute-done.18.f2), channel_id=1, source_target_pairs={{0,4},{4,0},{8,12},{12,8},{16,20},{20,16},{24,28},{28,24},{32,36},... | collective-permute-start | bytes 1376264 | tf_op jit(solution)/shard_map/ppermute | solution.py:424
  69.1 31.5 %collective-permute-start.22 = (bf16[448,512]{1,0:T(8,128)(2,1)S(1)}, bf16[448,512]{1,0:T(8,128)(2,1)S(1)}, u32[]{:S(2)}, u32[]{:S(2)}) collective-permute-start(bf16[448,512]{1,0:T(8,128)(2,1)S(1)} %collective-permute-done.19.f3), channel_id=1, source_target_pairs={{0,4},{4,0},{8,12},{12,8},{16,20},{20,16},{24,28},{28,24},{32,36},... | collective-permute-start | bytes 1376264 | tf_op jit(solution)/shard_map/ppermute | solution.py:424
  69.3 17.8 %collective-permute-start.11 = (bf16[152,1536]{1,0:T(8,128)(2,1)S(1)}, bf16[152,1536]{1,0:T(8,128)(2,1)S(1)}, u32[]{:S(2)}, u32[]{:S(2)}) collective-permute-start(bf16[152,1536]{1,0:T(8,128)(2,1)S(1)} %slice.19), channel_id=1, source_target_pairs={{0,24},{4,100},{8,0},{12,108},{16,8},{20,116},{24,16},{28,124},{32... | collective-permute-start | bytes 1400840 | tf_op jit(solution)/shard_map/ppermute | solution.py:413
  77.7 10.1 %collective-permute-start.9 = (bf16[152,1536]{1,0:T(8,128)(2,1)S(1)}, bf16[152,1536]{1,0:T(8,128)(2,1)S(1)}, u32[]{:S(2)}, u32[]{:S(2)}) collective-permute-start(bf16[152,1536]{1,0:T(8,128)(2,1)S(1)} %slice.18), channel_id=1, source_target_pairs={{0,8},{4,36},{8,16},{12,44},{16,24},{20,52},{24,0},{28,60},{32,40}... | collective-permute-start | bytes 1400840 | tf_op jit(solution)/shard_map/ppermute | solution.py:412
  87.8 10.4 %copy-start.7 = (f32[2048]{0:T(1024)S(1)}, f32[2048]{0:T(1024)}, u32[]{:S(2)}) copy-start(f32[2048]{0:T(1024)} %param.20) | copy-start | bytes 24580
  92.7 1.6 %collective-permute-start.12 = (bf16[4,80,384]{2,1,0:T(8,128)(2,1)S(1)}, bf16[4,80,384]{2,1,0:T(8,128)(2,1)S(1)}, u32[]{:S(2)}, u32[]{:S(2)}) collective-permute-start(bf16[4,80,384]{2,1,0:T(8,128)(2,1)S(1)} %get-tuple-element.65), channel_id=1, source_target_pairs={{0,4},{4,0},{8,12},{12,8},{16,20},{20,16},{24,28},{28,24},{32,36},... | collective-permute-start | bytes 737288 | tf_op jit(solution)/shard_map/ppermute | solution.py:438
  94.3 11.6 %collective-permute-start.15 = (bf16[256,384]{1,0:T(8,128)(2,1)S(1)}, bf16[256,384]{1,0:T(8,128)(2,1)S(1)}, u32[]{:S(2)}, u32[]{:S(2)}) collective-permute-start(bf16[256,384]{1,0:T(8,128)(2,1)S(1)} %shard_map.189.attn), channel_id=1, source_target_pairs={{0,3},{1,0},{2,1},{3,2},{4,7},{5,4},{6,5},{7,6},{8,11},{9,8},{10,9... | collective-permute-start | bytes 589832 | tf_op jit(solution)/shard_map/ppermute | solution.py:440
  97.2 9.3 %collective-permute-start.14 = (bf16[256,384]{1,0:T(8,128)(2,1)S(1)}, bf16[256,384]{1,0:T(8,128)(2,1)S(1)}, u32[]{:S(2)}, u32[]{:S(2)}) collective-permute-start(bf16[256,384]{1,0:T(8,128)(2,1)S(1)} %shard_map.189.attn), channel_id=1, source_target_pairs={{0,2},{1,3},{2,0},{3,1},{4,6},{5,7},{6,4},{7,5},{8,10},{9,11},{10,... | collective-permute-start | bytes 589832 | tf_op jit(solution)/shard_map/ppermute | solution.py:440
  97.2 12.1 %collective-permute-start.13 = (bf16[256,384]{1,0:T(8,128)(2,1)S(1)}, bf16[256,384]{1,0:T(8,128)(2,1)S(1)}, u32[]{:S(2)}, u32[]{:S(2)}) collective-permute-start(bf16[256,384]{1,0:T(8,128)(2,1)S(1)} %shard_map.189.attn), channel_id=1, source_target_pairs={{0,1},{1,2},{2,3},{3,0},{4,5},{5,6},{6,7},{7,4},{8,9},{9,10},{10,1... | collective-permute-start | bytes 589832 | tf_op jit(solution)/shard_map/ppermute | solution.py:440
  (10 other events, 61.7 us)

commit v3 on v2

--- a/solution.py
+++ b/solution.py
@@ -57,16 +57,18 @@
 
 
 def load_kernel(*refs, count):
-    outs, sems = refs[-count - 1 : -1], refs[-1]
+    outs, gains, sems = refs[-count - 2 : -2], refs[-2], refs[-1]
     copies = [pltpu.make_async_copy(refs[i], outs[i], sems.at[i]) for i in range(count)]
     for copy in copies:
         copy.start()
+    row = refs[count][...]
+    gains[...] = jnp.transpose(jnp.broadcast_to(row, (8, row.shape[1])))[:, :1]
     for copy in copies:
         copy.wait()
 
 
-def project_kernel(ids, x0, x1, x2, gain, wl, wr, wqd, wpi, square, lat, raw, query, pool):
-    values, ns, ats = pieces_of(ids, (x0, x1, x2), gain)
+def project_kernel(ids, x0, x1a, x1b, x2a, x2b, gain, wl, wr, wqd, wpi, square, lat, raw, query, pool):
+    values, ns, ats = pieces_of(ids, (x0, (x1a, x1b), (x2a, x2b)), gain)
     total = sum(jnp.sum(x * x, axis=-1, keepdims=True) for x in values)
     square[...] = jnp.broadcast_to(total, square.shape)
     lat[...] = summed(ns, wl, ats)
@@ -75,14 +77,18 @@
     pool[...] = summed(ns, wpi, ats)
 
 
+def stacked(x):
+    return jnp.concatenate([p[...] for p in x], axis=0) if isinstance(x, tuple) else x[...]
+
+
 def pieces_of(ids, xs, gain):
     ats = [pl.multiple_of(ids[k] * 512, 512) for k in range(len(xs))]
-    values = [x[...].astype(f32) for x in xs]
+    values = [stacked(x).astype(f32) for x in xs]
     return values, [gained(x, gain[:, pl.ds(at, 512)]) for x, at in zip(values, ats)], ats
 
 
-def all_pieces(ids, x0, x1, x2, xa, xb, gain):
-    _, ns, ats = pieces_of(ids, (x0, x1, x2), gain)
+def all_pieces(ids, x0, x1a, x1b, x2a, x2b, xa, xb, gain):
+    _, ns, ats = pieces_of(ids, (x0, (x1a, x1b), (x2a, x2b)), gain)
     _, n, at = last_piece(ids, xa, xb, gain)
     return ns + [n], ats + [at]
 
@@ -154,8 +160,8 @@
         q[base + NOPE + 16 : base + HEAD, :] = (first * sin[...] + second * cos[...]).astype(bf)
 
 
-def gate_kernel(ids, x0, x1, x2, xa, xb, gain, wa, wp, scale, gate_a, gate_p):
-    ns, ats = all_pieces(ids, x0, x1, x2, xa, xb, gain)
+def gate_kernel(ids, x0, x1a, x1b, x2a, x2b, xa, xb, gain, wa, wp, scale, gate_a, gate_p):
+    ns, ats = all_pieces(ids, x0, x1a, x1b, x2a, x2b, xa, xb, gain)
     s = scale[:, :1]
     gate_a[...] = jax.nn.sigmoid(summed(ns, wa, ats) * s)
     gate_p[...] = jax.nn.sigmoid(summed(ns, wp, ats) * s)
@@ -339,40 +345,40 @@
     here = lax.axis_index("sp")
     t = lax.axis_index("tp")
 
-    x1 = lax.ppermute(tokens, "tp", ring(1))
-    x2 = lax.ppermute(tokens, "tp", ring(-1))
-    xa = lax.ppermute(x1[: rows // 2], "tp", ring(1))
-    xb = lax.ppermute(x2[rows // 2 :], "tp", ring(-1))
+    top, bottom = tokens[: rows // 2], tokens[rows // 2 :]
+    x1a = lax.ppermute(top, "tp", ring(1))
+    x2b = lax.ppermute(bottom, "tp", ring(-1))
+    x1b = lax.ppermute(bottom, "tp", ring(1))
+    x2a = lax.ppermute(top, "tp", ring(-1))
+    xa = lax.ppermute(x1a, "tp", ring(1))
+    xb = lax.ppermute(x2b, "tp", ring(-1))
 
     half = ROPE // 2
     freqs = theta ** (-jnp.arange(half, dtype=f32) / half)
     positions = (here * rows + jnp.arange(rows, dtype=jnp.int32)).astype(f32)
     angles = freqs[:, None] * positions[None, :]
     cos, sin = jnp.cos(angles), jnp.sin(angles)
-    ids = jnp.concatenate(
-        [
-            (t + jnp.array([0, 3, 1, 2, 0, 1, 2, 3], jnp.int32)) & 3,
-            jnp.stack([here, jnp.left_shift(1, t), jnp.int32(length)]).astype(jnp.int32),
-        ]
-    )
-    gains = jnp.concatenate([latent_gain, key_head_gain, query_head_gain])[:, None]
+    fixed = jnp.array([0, 3, 1, 2, 0, 1, 2, 3, 0, 0, length], jnp.int32)
+    slot = jnp.arange(11, dtype=jnp.int32)
+    ids = jnp.where(slot < 8, (fixed + t) & 3, fixed + (slot == 8) * here + (slot == 9) * jnp.left_shift(1, t))
+    gains = jnp.concatenate([latent_gain, key_head_gain, query_head_gain, jnp.zeros((64,), f32)])[None, :]
     gain = norm_gain[None, :]
     wr = w_rotary_key.T
 
-    wanted = [w_latent_down, wr, w_query_down, w_pool_in, w_query_up, gain, tokens, gains, cos, sin, query_gain[None, :]]
-    wl, wr, wqd, wpi, wqu, gain, x0, near_gains, cos, sin, qgain = [
+    wanted = [w_latent_down, wr, w_query_down, w_pool_in, w_query_up, gain, tokens, cos, sin, query_gain[None, :]]
+    wl, wr, wqd, wpi, wqu, gain, x0, cos, sin, qgain, near_gains = [
         resident(x)
         for x in call(
-            functools.partial(load_kernel, count=11),
-            None, [*wanted, ids], [kept(S(x.shape, x.dtype)) for x in wanted], 4 * 10**8,
-            [pltpu.SemaphoreType.DMA((11,))], apart=range(12),
+            functools.partial(load_kernel, count=10),
+            None, [*wanted, gains, ids], [kept(S(x.shape, x.dtype)) for x in wanted] + [kept(S((512, 1), f32))],
+            4 * 10**8, [pltpu.SemaphoreType.DMA((10,))], apart=(*range(10), 11),
         )
     ]
     square, lat0, raw0, query0, pool0 = [
         resident(x)
         for x in call(
             project_kernel,
-            ids, [x0, resident(x1), resident(x2), gain, wl, wr, wqd, wpi],
+            ids, [x0, *[resident(x) for x in (x1a, x1b, x2a, x2b)], gain, wl, wr, wqd, wpi],
             [kept(S(s, f32)) for s in ((rows, 128), (rows, LATENT), (ROPE, rows), (rows, 512), (rows, 256))],
             16 * 10**8,
         )
@@ -384,7 +390,7 @@
         [kept(S((PAY, rows), bf)), kept(S((rows, 128), f32))],
         3 * 10**8,
     )
-    pieces = [tokens, x1, x2, xa, xb]
+    pieces = [tokens, x1a, x1b, x2a, x2b, xa, xb]
 
     a1 = lax.ppermute(pay, "sp", along(1, False))
     a2 = lax.ppermute(pay, "sp", along(-1, False))
@@ -403,7 +409,7 @@
     outer = lax.ppermute(outer, "sp", [(i, i - 1 + 2 * (i % 2)) for i in range(1, count - 1)])
 
     def attend_on(pieces, seeds, name):
-        return attend(q, q_other, w_latent_up, gains, pieces, seeds, bf if name == "attend_far" else f32)
+        return attend(q, q_other, w_latent_up, near_gains, pieces, seeds, bf if name == "attend_far" else f32)
 
     line = call(join_kernel, None, [resident(x) for x in (pay, a1, a2, a3)], kept(S((PAY, 4 * rows), bf)), 10**7)
     b1 = lax.ppermute(line, "sp", along(1, True))

time: 111 us -> 110 us (level)
  waiting for transfers between devices: 24.7 us -> 23.2 us
    ppermute x4 -> x6, waiting for transfers between devices: 6.97 us -> 3.2 us  [the longest x1 2.16 us: whole(): x2b = lax.ppermute(bottom, 'tp', ring(-1))]
    ppermute x4 -> x6, starting transfers between devices: 6.6 us -> 8.41 us  [the longest x1 2.85 us: whole(): xb = lax.ppermute(x2b, 'tp', ring(-1))]
    ppermute x3, waiting for transfers between devices: 1.12 us -> 2.86 us  [whole(): packs = [lax.ppermute(packs[d - 1], 'tp', ring(d)) for d in (1, 2, 3)]]
    select_n x0 -> x1, other arithmetic: none -> 1.14 us  [whole(): jnp.where(slot < 8, fixed + t & 3, fixed + (slot == 8) * here + (slot ==...]
  transfers between devices with their start and end apart: 23 -> 25, of which waited for: 11 -> 11; matrix products, arithmetic and copies ran while one was open for 3% -> 3% of each run, Pallas kernels for 27% -> 28%
where the time goes in v3:
time: 110 us; the launch traced here: 109 us
  starting transfers between devices  49.1 us (45%)
  Pallas kernels  32.4 us (29%)
  waiting for transfers between devices  23.2 us (21%)
  other arithmetic  2.73 us (2%)
  local copies, waits for them, and re-layouts  1.15 us (1%)
    pallas_call x13, Pallas kernels, call(): pl.pallas_call(kernel, in_specs=[SM] * len(first) + [pl.BlockSpec(memory_...  32.4 us
    ppermute x3, starting transfers between devices, whole(): swapped = [lax.ppermute(p, 'sp', SWAP) for p in packs]  14.4 us
    ppermute x1, starting transfers between devices, whole(): b4 = lax.ppermute(b2[cut:], 'sp', along(-1, True))  8.38 us
    ppermute x3, waiting for transfers between devices, whole(): attns = [attn] + [lax.ppermute(attn, 'tp', ring(d)) for d in (1, 2, 3)]  7.46 us
    ppermute x1, waiting for transfers between devices, whole(): a2 = lax.ppermute(pay, 'sp', along(-1, False))  4.58 us
    ppermute x1, starting transfers between devices, whole(): a3 = lax.ppermute(pay, 'sp', along(2, False))  4.07 us
    ppermute x1, starting transfers between devices, whole(): b2 = lax.ppermute(line, 'sp', along(-1, True))  3.97 us
    ppermute x3, starting transfers between devices, whole(): attns = [attn] + [lax.ppermute(attn, 'tp', ring(d)) for d in (1, 2, 3)]  3.36 us
  transfers between devices with their start and end apart: 25, of which 11 were waited for; matrix products, arithmetic and copies ran while one was open for 3% of the time, Pallas kernels for 28%

profile of v3, /device:TPU:0, one launch (start us, length us, event | category | flops | bytes accessed | tf_op | source)
XLA Modules:
  0.0 108.9 jit_solution(4287113205065565651)
XLA Ops:
  1.1 1.7 %collective-permute-start.4 = (bf16[192,512]{1,0:T(8,128)(2,1)S(1)}, bf16[192,512]{1,0:T(8,128)(2,1)S(1)}, u32[]{:S(2)}, u32[]{:S(2)}) collective-permute-start(bf16[192,512]{1,0:T(8,128)(2,1)S(1)} %get-tuple-element.77), channel_id=1, source_target_pairs={{0,1},{1,2},{2,3},{3,0},{4,5},{5,6},{6,7},{7,4},{8,9},{9,10},{10,1... | collective-permute-start | bytes 589832 | tf_op jit(solution)/shard_map/ppermute | solution.py:351
  2.7 1.6 %collective-permute-start.2 = (bf16[192,512]{1,0:T(8,128)(2,1)S(1)}, bf16[192,512]{1,0:T(8,128)(2,1)S(1)}, u32[]{:S(2)}, u32[]{:S(2)}) collective-permute-start(bf16[192,512]{1,0:T(8,128)(2,1)S(1)} %get-tuple-element.77), channel_id=1, source_target_pairs={{0,3},{1,0},{2,1},{3,2},{4,7},{5,4},{6,5},{7,6},{8,11},{9,8},{10,9... | collective-permute-start | bytes 589832 | tf_op jit(solution)/shard_map/ppermute | solution.py:350
  4.4 1.7 %collective-permute-start.5 = (bf16[192,512]{1,0:T(8,128)(2,1)S(1)}, bf16[192,512]{1,0:T(8,128)(2,1)S(1)}, u32[]{:S(2)}, u32[]{:S(2)}) collective-permute-start(bf16[192,512]{1,0:T(8,128)(2,1)S(1)} %get-tuple-element.78), channel_id=1, source_target_pairs={{0,3},{1,0},{2,1},{3,2},{4,7},{5,4},{6,5},{7,6},{8,11},{9,8},{10,9... | collective-permute-start | bytes 589832 | tf_op jit(solution)/shard_map/ppermute | solution.py:352
  8.3 2.2 %collective-permute-done.2.x2b = bf16[192,512]{1,0:T(8,128)(2,1)S(1)} collective-permute-done((bf16[192,512]{1,0:T(8,128)(2,1)S(1)}, bf16[192,512]{1,0:T(8,128)(2,1)S(1)}, u32[]{:S(2)}, u32[]{:S(2)}) %collective-permute-start.2) | collective-permute-done | bytes 196640 | tf_op jit(solution)/shard_map/ppermute | solution.py:350
  10.5 2.8 %collective-permute-start.3 = (bf16[192,512]{1,0:T(8,128)(2,1)S(1)}, bf16[192,512]{1,0:T(8,128)(2,1)S(1)}, u32[]{:S(2)}, u32[]{:S(2)}) collective-permute-start(bf16[192,512]{1,0:T(8,128)(2,1)S(1)} %collective-permute-done.2.x2b), channel_id=1, source_target_pairs={{0,3},{1,0},{2,1},{3,2},{4,7},{5,4},{6,5},{7,6},{8,11},{9,8},{10,9... | collective-permute-start | bytes 589832 | tf_op jit(solution)/shard_map/ppermute | solution.py:354
  14.4 2.5 %shard_map.181 = (bf16[2048,256]{1,0:T(8,128)(2,1)S(1)}, bf16[32,2048]{1,0:T(8,128)(2,1)S(1)}, bf16[2048,512]{1,0:T(8,128)(2,1)S(1)}, bf16[2048,256]{1,0:T(8,128...) custom-call(bf16[2048,256]{1,0:T(8,128)(2,1)} %refs_0_.1, ...), custom_call_target="tpu_custom_call" | custom-call | flops 400000000 | bytes 1048576 | tf_op jit(solution)/shard_map/pallas_call | solution.py:309
  16.9 2.2 %shard_map.182 = (f32[384,128]{1,0:T(8,128)S(1)}, f32[384,256]{1,0:T(8,128)S(1)}, f32[32,384]{1,0:T(8,128)S(1)}, f32[384,512]{1,0:T(8,128)S(1)}, f32[384,256]{1,0:T(8,128)S(1)}) custom-call(s32[11]{0:T(128)S(1)} %copy-done.7, bf16[384,512]{1,0:T(8,128)(2,1)S(1)} %get-tuple-element.46.x0, bf16[192,512]{1,0:T(8,128)(2,1)S(1)} %collective-permute-done.x1a, ...), custom_call_target="tpu_custom_call" | custom-call | flops 1600000000 | bytes 1048576 | tf_op jit(solution)/shard_map/pallas_call | solution.py:309
  21.3 4.1 %collective-permute-start.9 = (bf16[304,384]{1,0:T(8,128)(2,1)S(1)}, bf16[304,384]{1,0:T(8,128)(2,1)S(1)}, u32[]{:S(2)}, u32[]{:S(2)}) collective-permute-start(bf16[304,384]{1,0:T(8,128)(2,1)S(1)} %get-tuple-element.59.a), channel_id=1, source_target_pairs={{0,64},{4,20},{8,72},{12,28},{16,80},{20,4},{24,88},{28,12},{32,96... | collective-permute-start | bytes 700424 | tf_op jit(solution)/shard_map/ppermute | solution.py:397
  27.4 2.0 %collective-permute-done.9.d = bf16[304,384]{1,0:T(8,128)(2,1)S(1)} collective-permute-done((bf16[304,384]{1,0:T(8,128)(2,1)S(1)}, bf16[304,384]{1,0:T(8,128)(2,1)S(1)}, u32[]{:S(2)}, u32[]{:S(2)}) %collective-permute-start.9) | collective-permute-done | bytes 233504 | tf_op jit(solution)/shard_map/ppermute | solution.py:397
  29.4 4.6 %collective-permute-done.8.c = bf16[304,384]{1,0:T(8,128)(2,1)S(1)} collective-permute-done((bf16[304,384]{1,0:T(8,128)(2,1)S(1)}, bf16[304,384]{1,0:T(8,128)(2,1)S(1)}, u32[]{:S(2)}, u32[]{:S(2)}) %collective-permute-start.8) | collective-permute-done | bytes 233504 | tf_op jit(solution)/shard_map/ppermute | solution.py:396
  34.1 4.0 %collective-permute-start.12 = (bf16[304,1536]{1,0:T(8,128)(2,1)S(1)}, bf16[304,1536]{1,0:T(8,128)(2,1)S(1)}, u32[]{:S(2)}, u32[]{:S(2)}) collective-permute-start(bf16[304,1536]{1,0:T(8,128)(2,1)S(1)} %shard_map.185.refs_4_), channel_id=1, source_target_pairs={{0,24},{4,100},{8,0},{12,108},{16,8},{20,116},{24,16},{28,124},{32... | collective-permute-start | bytes 2801672 | tf_op jit(solution)/shard_map/ppermute | solution.py:416
  38.1 1.7 %shard_map.184 = (bf16[400,384]{1,0:T(8,128)(2,1)S(1)}, bf16[384,256]{1,0:T(8,128)(2,1)S(1)}, bf16[8,256]{1,0:T(8,128)(2,1)S(1)}) custom-call(s32[11]{0:T(128)S(1)} %copy-done.7, bf16[192,512]{1,0:T(8,128)(2,1)S(1)} %collective-permute-done.1.xa, bf16[192,512]{1,0:T(8,128)(2,1)S(1)} %collective-permute-done.3.xb, f32[1,2048]{1,0:T(1,128)S(1)} %get-tuple-element.41.gain, ...), custom_call_target="tpu_custom_call" | custom-call | flops 1000000000 | bytes 1048576 | tf_op jit(solution)/shard_map/pallas_call | solution.py:309
  42.8 3.0 %collective-permute-start.20 = (bf16[448,512]{1,0:T(8,128)(2,1)S(1)}, bf16[448,512]{1,0:T(8,128)(2,1)S(1)}, u32[]{:S(2)}, u32[]{:S(2)}) collective-permute-start(bf16[448,512]{1,0:T(8,128)(2,1)S(1)} %get-tuple-element.71), channel_id=1, source_target_pairs={{0,2},{1,3},{2,0},{3,1},{4,6},{5,7},{6,4},{7,5},{8,10},{9,11},{10,... | collective-permute-start | bytes 1376264 | tf_op jit(solution)/shard_map/ppermute | solution.py:429
  46.1 4.6 %shard_map.186 = (f32[4,80,384]{2,1,0:T(8,128)S(1)}, f32[4,80,384]{2,1,0:T(8,128)S(1)}) custom-call(bf16[400,384]{1,0:T(8,128)(2,1)S(1)} %get-tuple-element.58.refs_0_, bf16[400,384]{1,0:T(8,128)(2,1)S(1)} %collective-permute-done.6.refs_1_.inner, bf16[256,512]{1,0:T(8,128)(2,1)S(1)} %copy-done.9, f32[512,1]{1,0:T(8,128)S(1)} %get-tuple-element.50.gains.refs_3_, ...), custom_call_target="tpu_custom_call" | custom-call | flops 4831838208 | bytes 1048576 | tf_op jit(solution)/shard_map/pallas_call | solution.py:309
  50.7 2.9 %collective-permute-done.19.f1 = bf16[448,512]{1,0:T(8,128)(2,1)S(1)} collective-permute-done((bf16[448,512]{1,0:T(8,128)(2,1)S(1)}, bf16[448,512]{1,0:T(8,128)(2,1)S(1)}, u32[]{:S(2)}, u32[]{:S(2)}) %collective-permute-start.19) | collective-permute-done | bytes 458784 | tf_op jit(solution)/shard_map/ppermute | solution.py:429
  53.5 13.5 %collective-permute-start.22 = (bf16[448,512]{1,0:T(8,128)(2,1)S(1)}, bf16[448,512]{1,0:T(8,128)(2,1)S(1)}, u32[]{:S(2)}, u32[]{:S(2)}) collective-permute-start(bf16[448,512]{1,0:T(8,128)(2,1)S(1)} %collective-permute-done.19.f1), channel_id=1, source_target_pairs={{0,4},{4,0},{8,12},{12,8},{16,20},{20,16},{24,28},{28,24},{32,36},... | collective-permute-start | bytes 1376264 | tf_op jit(solution)/shard_map/ppermute | solution.py:430
  68.0 8.4 %collective-permute-start.13 = (bf16[152,1536]{1,0:T(8,128)(2,1)S(1)}, bf16[152,1536]{1,0:T(8,128)(2,1)S(1)}, u32[]{:S(2)}, u32[]{:S(2)}) collective-permute-start(bf16[152,1536]{1,0:T(8,128)(2,1)S(1)} %slice.17), channel_id=1, source_target_pairs={{0,24},{4,100},{8,0},{12,108},{16,8},{20,116},{24,16},{28,124},{32... | collective-permute-start | bytes 1400840 | tf_op jit(solution)/shard_map/ppermute | solution.py:419
  76.8 9.1 %shard_map.187 = (f32[4,80,384]{2,1,0:T(8,128)S(1)}, f32[4,80,384]{2,1,0:T(8,128)S(1)}) custom-call(bf16[400,384]{1,0:T(8,128)(2,1)S(1)} %get-tuple-element.58.refs_0_, bf16[400,384]{1,0:T(8,128)(2,1)S(1)} %collective-permute-done.6.refs_1_.inner, bf16[256,512]{1,0:T(8,128)(2,1)S(1)} %copy-done.9, f32[512,1]{1,0:T(8,128)S(1)} %get-tuple-element.50.gains.refs_3_, ...), custom_call_target="tpu_custom_call" | custom-call | flops 9663676416 | bytes 1048576 | tf_op jit(solution)/shard_map/pallas_call | solution.py:309
  86.5 4.9 %shard_map.188 = (f32[4,80,384]{2,1,0:T(8,128)S(1)}, bf16[4,80,384]{2,1,0:T(8,128)(2,1)S(1)}) custom-call(bf16[400,384]{1,0:T(8,128)(2,1)S(1)} %get-tuple-element.58.refs_0_, bf16[400,384]{1,0:T(8,128)(2,1)S(1)} %collective-permute-done.6.refs_1_.inner, bf16[256,512]{1,0:T(8,128)(2,1)S(1)} %copy-done.9, f32[512,1]{1,0:T(8,128)S(1)} %get-tuple-element.50.gains.refs_3_, ...), custom_call_target="tpu_custom_call" | custom-call | flops 4831838208 | bytes 1048576 | tf_op jit(solution)/shard_map/pallas_call | solution.py:309
  91.5 1.5 %collective-permute-done.14.other = bf16[4,80,384]{2,1,0:T(8,128)(2,1)S(1)} collective-permute-done((bf16[4,80,384]{2,1,0:T(8,128)(2,1)S(1)}, bf16[4,80,384]{2,1,0:T(8,128)(2,1)S(1)}, u32[]{:S(2)}, u32[]{:S(2)}) %collective-permute-start.14) | collective-permute-done | bytes 245792 | tf_op jit(solution)/shard_map/ppermute | solution.py:444
  93.1 2.4 %collective-permute-start.17 = (bf16[256,384]{1,0:T(8,128)(2,1)S(1)}, bf16[256,384]{1,0:T(8,128)(2,1)S(1)}, u32[]{:S(2)}, u32[]{:S(2)}) collective-permute-start(bf16[256,384]{1,0:T(8,128)(2,1)S(1)} %shard_map.189.attn), channel_id=1, source_target_pairs={{0,3},{1,0},{2,1},{3,2},{4,7},{5,4},{6,5},{7,6},{8,11},{9,8},{10,9... | collective-permute-start | bytes 589832 | tf_op jit(solution)/shard_map/ppermute | solution.py:446
  96.5 2.4 %shard_map.191 = (f32[384,512]{1,0:T(8,128)S(1)}, f32[384,512]{1,0:T(8,128)S(1)}) custom-call(s32[11]{0:T(128)S(1)} %copy-done.7, bf16[384,512]{1,0:T(8,128)(2,1)S(1)} %copy-done, bf16[192,512]{1,0:T(8,128)(2,1)S(1)} %collective-permute-done.x1a, bf16[192,512]{1,0:T(8,128)(2,1)S(1)} %collective-permute-done.4.x1b, ...), custom_call_target="tpu_custom_call" | custom-call | flops 500000000 | bytes 1048576 | tf_op jit(solution)/shard_map/pallas_call | solution.py:309
  100.1 4.1 %collective-permute-done.17.a3 = bf16[256,384]{1,0:T(8,128)(2,1)S(1)} collective-permute-done((bf16[256,384]{1,0:T(8,128)(2,1)S(1)}, bf16[256,384]{1,0:T(8,128)(2,1)S(1)}, u32[]{:S(2)}, u32[]{:S(2)}) %collective-permute-start.17) | collective-permute-done | bytes 196640 | tf_op jit(solution)/shard_map/ppermute | solution.py:446
  104.8 2.8 %collective-permute-done.15.a1 = bf16[256,384]{1,0:T(8,128)(2,1)S(1)} collective-permute-done((bf16[256,384]{1,0:T(8,128)(2,1)S(1)}, bf16[256,384]{1,0:T(8,128)(2,1)S(1)}, u32[]{:S(2)}, u32[]{:S(2)}) %collective-permute-start.15) | collective-permute-done | bytes 196640 | tf_op jit(solution)/shard_map/ppermute | solution.py:446
  (68 shorter events, 18.0 us)
Async XLA Ops:
  1.1 15.9 %collective-permute-start.4 = (bf16[192,512]{1,0:T(8,128)(2,1)S(1)}, bf16[192,512]{1,0:T(8,128)(2,1)S(1)}, u32[]{:S(2)}, u32[]{:S(2)}) collective-permute-start(bf16[192,512]{1,0:T(8,128)(2,1)S(1)} %get-tuple-element.77), channel_id=1, source_target_pairs={{0,1},{1,2},{2,3},{3,0},{4,5},{5,6},{6,7},{7,4},{8,9},{9,10},{10,1... | collective-permute-start | bytes 589832 | tf_op jit(solution)/shard_map/ppermute | solution.py:351
  2.7 7.8 %collective-permute-start.2 = (bf16[192,512]{1,0:T(8,128)(2,1)S(1)}, bf16[192,512]{1,0:T(8,128)(2,1)S(1)}, u32[]{:S(2)}, u32[]{:S(2)}) collective-permute-start(bf16[192,512]{1,0:T(8,128)(2,1)S(1)} %get-tuple-element.77), channel_id=1, source_target_pairs={{0,3},{1,0},{2,1},{3,2},{4,7},{5,4},{6,5},{7,6},{8,11},{9,8},{10,9... | collective-permute-start | bytes 589832 | tf_op jit(solution)/shard_map/ppermute | solution.py:350
  4.4 12.6 %collective-permute-start.5 = (bf16[192,512]{1,0:T(8,128)(2,1)S(1)}, bf16[192,512]{1,0:T(8,128)(2,1)S(1)}, u32[]{:S(2)}, u32[]{:S(2)}) collective-permute-start(bf16[192,512]{1,0:T(8,128)(2,1)S(1)} %get-tuple-element.78), channel_id=1, source_target_pairs={{0,3},{1,0},{2,1},{3,2},{4,7},{5,4},{6,5},{7,6},{8,11},{9,8},{10,9... | collective-permute-start | bytes 589832 | tf_op jit(solution)/shard_map/ppermute | solution.py:352
  6.0 7.3 %collective-permute-start = (bf16[192,512]{1,0:T(8,128)(2,1)S(1)}, bf16[192,512]{1,0:T(8,128)(2,1)S(1)}, u32[]{:S(2)}, u32[]{:S(2)}) collective-permute-start(bf16[192,512]{1,0:T(8,128)(2,1)S(1)} %get-tuple-element.78), channel_id=1, source_target_pairs={{0,1},{1,2},{2,3},{3,0},{4,5},{5,6},{6,7},{7,4},{8,9},{9,10},{10,1... | collective-permute-start | bytes 589832 | tf_op jit(solution)/shard_map/ppermute | solution.py:349
  10.5 8.7 %collective-permute-start.3 = (bf16[192,512]{1,0:T(8,128)(2,1)S(1)}, bf16[192,512]{1,0:T(8,128)(2,1)S(1)}, u32[]{:S(2)}, u32[]{:S(2)}) collective-permute-start(bf16[192,512]{1,0:T(8,128)(2,1)S(1)} %collective-permute-done.2.x2b), channel_id=1, source_target_pairs={{0,3},{1,0},{2,1},{3,2},{4,7},{5,4},{6,5},{7,6},{8,11},{9,8},{10,9... | collective-permute-start | bytes 589832 | tf_op jit(solution)/shard_map/ppermute | solution.py:354
  13.3 6.9 %collective-permute-start.1 = (bf16[192,512]{1,0:T(8,128)(2,1)S(1)}, bf16[192,512]{1,0:T(8,128)(2,1)S(1)}, u32[]{:S(2)}, u32[]{:S(2)}) collective-permute-start(bf16[192,512]{1,0:T(8,128)(2,1)S(1)} %collective-permute-done.x1a), channel_id=1, source_target_pairs={{0,1},{1,2},{2,3},{3,0},{4,5},{5,6},{6,7},{7,4},{8,9},{9,10},{10,1... | collective-permute-start | bytes 589832 | tf_op jit(solution)/shard_map/ppermute | solution.py:353
  21.3 8.1 %collective-permute-start.9 = (bf16[304,384]{1,0:T(8,128)(2,1)S(1)}, bf16[304,384]{1,0:T(8,128)(2,1)S(1)}, u32[]{:S(2)}, u32[]{:S(2)}) collective-permute-start(bf16[304,384]{1,0:T(8,128)(2,1)S(1)} %get-tuple-element.59.a), channel_id=1, source_target_pairs={{0,64},{4,20},{8,72},{12,28},{16,80},{20,4},{24,88},{28,12},{32,96... | collective-permute-start | bytes 700424 | tf_op jit(solution)/shard_map/ppermute | solution.py:397
  25.4 8.6 %collective-permute-start.8 = (bf16[304,384]{1,0:T(8,128)(2,1)S(1)}, bf16[304,384]{1,0:T(8,128)(2,1)S(1)}, u32[]{:S(2)}, u32[]{:S(2)}) collective-permute-start(bf16[304,384]{1,0:T(8,128)(2,1)S(1)} %get-tuple-element.59.a), channel_id=1, source_target_pairs={{0,96},{4,28},{8,104},{12,4},{16,112},{20,12},{24,120},{28,20},{32... | collective-permute-start | bytes 700424 | tf_op jit(solution)/shard_map/ppermute | solution.py:396
  26.1 7.9 %collective-permute-start.7 = (bf16[304,384]{1,0:T(8,128)(2,1)S(1)}, bf16[304,384]{1,0:T(8,128)(2,1)S(1)}, u32[]{:S(2)}, u32[]{:S(2)}) collective-permute-start(bf16[304,384]{1,0:T(8,128)(2,1)S(1)} %get-tuple-element.59.a), channel_id=1, source_target_pairs={{0,32},{4,12},{8,40},{12,20},{16,48},{20,28},{24,56},{28,4},{32,64... | collective-permute-start | bytes 700424 | tf_op jit(solution)/shard_map/ppermute | solution.py:395
  34.1 33.9 %collective-permute-start.12 = (bf16[304,1536]{1,0:T(8,128)(2,1)S(1)}, bf16[304,1536]{1,0:T(8,128)(2,1)S(1)}, u32[]{:S(2)}, u32[]{:S(2)}) collective-permute-start(bf16[304,1536]{1,0:T(8,128)(2,1)S(1)} %shard_map.185.refs_4_), channel_id=1, source_target_pairs={{0,24},{4,100},{8,0},{12,108},{16,8},{20,116},{24,16},{28,124},{32... | collective-permute-start | bytes 2801672 | tf_op jit(solution)/shard_map/ppermute | solution.py:416
  38.0 38.4 %collective-permute-start.10 = (bf16[304,1536]{1,0:T(8,128)(2,1)S(1)}, bf16[304,1536]{1,0:T(8,128)(2,1)S(1)}, u32[]{:S(2)}, u32[]{:S(2)}) collective-permute-start(bf16[304,1536]{1,0:T(8,128)(2,1)S(1)} %shard_map.185.refs_4_), channel_id=1, source_target_pairs={{0,8},{4,36},{8,16},{12,44},{16,24},{20,52},{24,0},{28,60},{32,40}... | collective-permute-start | bytes 2801672 | tf_op jit(solution)/shard_map/ppermute | solution.py:415
  39.8 1.7 %collective-permute-start.6 = (bf16[400,384]{1,0:T(8,128)(2,1)S(1)}, bf16[400,384]{1,0:T(8,128)(2,1)S(1)}, u32[]{:S(2)}, u32[]{:S(2)}) collective-permute-start(bf16[400,384]{1,0:T(8,128)(2,1)S(1)} %get-tuple-element.58.refs_0_), channel_id=1, source_target_pairs={{0,4},{4,0},{8,12},{12,8},{16,20},{20,16},{24,28},{28,24},{32,36},... | collective-permute-start | bytes 921608 | tf_op jit(solution)/shard_map/ppermute | solution.py:407
  42.8 10.8 %collective-permute-start.19 = (bf16[448,512]{1,0:T(8,128)(2,1)S(1)}, bf16[448,512]{1,0:T(8,128)(2,1)S(1)}, u32[]{:S(2)}, u32[]{:S(2)}) collective-permute-start(bf16[448,512]{1,0:T(8,128)(2,1)S(1)} %get-tuple-element.70), channel_id=1, source_target_pairs={{0,1},{1,2},{2,3},{3,0},{4,5},{5,6},{6,7},{7,4},{8,9},{9,10},{10,1... | collective-permute-start | bytes 1376264 | tf_op jit(solution)/shard_map/ppermute | solution.py:429
  42.8 24.2 %collective-permute-start.20 = (bf16[448,512]{1,0:T(8,128)(2,1)S(1)}, bf16[448,512]{1,0:T(8,128)(2,1)S(1)}, u32[]{:S(2)}, u32[]{:S(2)}) collective-permute-start(bf16[448,512]{1,0:T(8,128)(2,1)S(1)} %get-tuple-element.71), channel_id=1, source_target_pairs={{0,2},{1,3},{2,0},{3,1},{4,6},{5,7},{6,4},{7,5},{8,10},{9,11},{10,... | collective-permute-start | bytes 1376264 | tf_op jit(solution)/shard_map/ppermute | solution.py:429
  45.9 21.2 %collective-permute-start.21 = (bf16[448,512]{1,0:T(8,128)(2,1)S(1)}, bf16[448,512]{1,0:T(8,128)(2,1)S(1)}, u32[]{:S(2)}, u32[]{:S(2)}) collective-permute-start(bf16[448,512]{1,0:T(8,128)(2,1)S(1)} %get-tuple-element.72), channel_id=1, source_target_pairs={{0,3},{1,0},{2,1},{3,2},{4,7},{5,4},{6,5},{7,6},{8,11},{9,8},{10,9... | collective-permute-start | bytes 1376264 | tf_op jit(solution)/shard_map/ppermute | solution.py:429
  53.5 42.0 %collective-permute-start.22 = (bf16[448,512]{1,0:T(8,128)(2,1)S(1)}, bf16[448,512]{1,0:T(8,128)(2,1)S(1)}, u32[]{:S(2)}, u32[]{:S(2)}) collective-permute-start(bf16[448,512]{1,0:T(8,128)(2,1)S(1)} %collective-permute-done.19.f1), channel_id=1, source_target_pairs={{0,4},{4,0},{8,12},{12,8},{16,20},{20,16},{24,28},{28,24},{32,36},... | collective-permute-start | bytes 1376264 | tf_op jit(solution)/shard_map/ppermute | solution.py:430
  67.1 31.8 %collective-permute-start.23 = (bf16[448,512]{1,0:T(8,128)(2,1)S(1)}, bf16[448,512]{1,0:T(8,128)(2,1)S(1)}, u32[]{:S(2)}, u32[]{:S(2)}) collective-permute-start(bf16[448,512]{1,0:T(8,128)(2,1)S(1)} %collective-permute-done.20.f2), channel_id=1, source_target_pairs={{0,4},{4,0},{8,12},{12,8},{16,20},{20,16},{24,28},{28,24},{32,36},... | collective-permute-start | bytes 1376264 | tf_op jit(solution)/shard_map/ppermute | solution.py:430
  67.1 31.8 %collective-permute-start.24 = (bf16[448,512]{1,0:T(8,128)(2,1)S(1)}, bf16[448,512]{1,0:T(8,128)(2,1)S(1)}, u32[]{:S(2)}, u32[]{:S(2)}) collective-permute-start(bf16[448,512]{1,0:T(8,128)(2,1)S(1)} %collective-permute-done.21.f3), channel_id=1, source_target_pairs={{0,4},{4,0},{8,12},{12,8},{16,20},{20,16},{24,28},{28,24},{32,36},... | collective-permute-start | bytes 1376264 | tf_op jit(solution)/shard_map/ppermute | solution.py:430
  68.0 17.8 %collective-permute-start.13 = (bf16[152,1536]{1,0:T(8,128)(2,1)S(1)}, bf16[152,1536]{1,0:T(8,128)(2,1)S(1)}, u32[]{:S(2)}, u32[]{:S(2)}) collective-permute-start(bf16[152,1536]{1,0:T(8,128)(2,1)S(1)} %slice.17), channel_id=1, source_target_pairs={{0,24},{4,100},{8,0},{12,108},{16,8},{20,116},{24,16},{28,124},{32... | collective-permute-start | bytes 1400840 | tf_op jit(solution)/shard_map/ppermute | solution.py:419
  76.5 10.1 %collective-permute-start.11 = (bf16[152,1536]{1,0:T(8,128)(2,1)S(1)}, bf16[152,1536]{1,0:T(8,128)(2,1)S(1)}, u32[]{:S(2)}, u32[]{:S(2)}) collective-permute-start(bf16[152,1536]{1,0:T(8,128)(2,1)S(1)} %slice.16), channel_id=1, source_target_pairs={{0,8},{4,36},{8,16},{12,44},{16,24},{20,52},{24,0},{28,60},{32,40}... | collective-permute-start | bytes 1400840 | tf_op jit(solution)/shard_map/ppermute | solution.py:418
  91.4 1.6 %collective-permute-start.14 = (bf16[4,80,384]{2,1,0:T(8,128)(2,1)S(1)}, bf16[4,80,384]{2,1,0:T(8,128)(2,1)S(1)}, u32[]{:S(2)}, u32[]{:S(2)}) collective-permute-start(bf16[4,80,384]{2,1,0:T(8,128)(2,1)S(1)} %get-tuple-element.65), channel_id=1, source_target_pairs={{0,4},{4,0},{8,12},{12,8},{16,20},{20,16},{24,28},{28,24},{32,36},... | collective-permute-start | bytes 737288 | tf_op jit(solution)/shard_map/ppermute | solution.py:444
  93.1 11.1 %collective-permute-start.17 = (bf16[256,384]{1,0:T(8,128)(2,1)S(1)}, bf16[256,384]{1,0:T(8,128)(2,1)S(1)}, u32[]{:S(2)}, u32[]{:S(2)}) collective-permute-start(bf16[256,384]{1,0:T(8,128)(2,1)S(1)} %shard_map.189.attn), channel_id=1, source_target_pairs={{0,3},{1,0},{2,1},{3,2},{4,7},{5,4},{6,5},{7,6},{8,11},{9,8},{10,9... | collective-permute-start | bytes 589832 | tf_op jit(solution)/shard_map/ppermute | solution.py:446
  95.5 9.3 %collective-permute-start.16 = (bf16[256,384]{1,0:T(8,128)(2,1)S(1)}, bf16[256,384]{1,0:T(8,128)(2,1)S(1)}, u32[]{:S(2)}, u32[]{:S(2)}) collective-permute-start(bf16[256,384]{1,0:T(8,128)(2,1)S(1)} %shard_map.189.attn), channel_id=1, source_target_pairs={{0,2},{1,3},{2,0},{3,1},{4,6},{5,7},{6,4},{7,5},{8,10},{9,11},{10,... | collective-permute-start | bytes 589832 | tf_op jit(solution)/shard_map/ppermute | solution.py:446
  95.5 12.1 %collective-permute-start.15 = (bf16[256,384]{1,0:T(8,128)(2,1)S(1)}, bf16[256,384]{1,0:T(8,128)(2,1)S(1)}, u32[]{:S(2)}, u32[]{:S(2)}) collective-permute-start(bf16[256,384]{1,0:T(8,128)(2,1)S(1)} %shard_map.189.attn), channel_id=1, source_target_pairs={{0,1},{1,2},{2,3},{3,0},{4,5},{5,6},{6,7},{7,4},{8,9},{9,10},{10,1... | collective-permute-start | bytes 589832 | tf_op jit(solution)/shard_map/ppermute | solution.py:446
  (11 other events, 63.0 us)

commit v4 on v3

--- a/solution.py
+++ b/solution.py
@@ -143,7 +143,7 @@
     on_first = ids[8] % 2 == 0
     inner = jnp.concatenate([jnp.where(on_first, end, head)] * 2, axis=0).astype(bf)
     q[q.shape[0] - 16 :, :] = jnp.concatenate([inner, inner[:, :128]], axis=1)
-    outer[...] = jnp.where(on_first, head, end).astype(bf)
+    outer[...] = jnp.concatenate([jnp.where(on_first, head, end)] * 2, axis=0).astype(bf)
     lat = (query0[...] + product(n, rows_at(wqd, at), False)) * s
     lat = lat.astype(bf).astype(f32)
     lat = lat * lax.rsqrt(jnp.mean(lat * lat, axis=-1, keepdims=True) + eps) * qgain[...]
@@ -194,14 +194,15 @@
     half, length = ids[9], ids[10]
     on_first = ids[8] % 2 == 0
     inner = inner[inner.shape[0] - 16 :, :256][:REACH].astype(f32)
-    outer = outer[...].astype(f32)
+    outer = outer[...][:REACH].astype(f32)
     padded[0:REACH, :] = jnp.where(on_first, outer, inner)
     padded[REACH : REACH + rows, :] = x[...].astype(f32)
-    padded[REACH + rows :, :] = jnp.where(on_first, inner, outer)
+    padded[REACH + rows : rows + 2 * REACH, :] = jnp.where(on_first, inner, outer)
     n = rows + 2 * REACH
-    sum2[: n - 1, :] = padded[: n - 1, :] + padded[1:n, :]
-    sum4[: n - 3, :] = sum2[: n - 3, :] + sum2[2 : n - 1, :]
-    sum8[: n - 7, :] = sum4[: n - 7, :] + sum4[4 : n - 3, :]
+    padded[n:, :] = sum2[n:, :] = sum4[n:, :] = jnp.zeros((REACH, x.shape[1]), f32)
+    sum2[:n, :] = padded[:n, :] + padded[1 : n + 1, :]
+    sum4[:n, :] = sum2[:n, :] + sum2[2 : n + 2, :]
+    sum8[:n, :] = sum4[:n, :] + sum4[4 : n + 4, :]
     total = sum8[:rows, :] + sum8[REACH : REACH + rows, :]
     total = jnp.where(half == 4, sum8[4 : 4 + rows, :], total)
     total = jnp.where(half == 2, sum4[6 : 6 + rows, :], total)
@@ -401,7 +402,7 @@
         ids,
         [resident(xa), resident(xb), gain, wqd, wpi, resident(scale), query0, pool0, qgain,
          wqu, near_gains, cos, sin],
-        [S((heads * HEAD + 16, rows), bf), S((rows, 256), bf), S((REACH, 256), bf)],
+        [S((heads * HEAD + 16, rows), bf), S((rows, 256), bf), S((2 * REACH, 256), bf)],
         10**9,
     )
     q_other = lax.ppermute(q, "sp", SWAP)
@@ -414,7 +415,7 @@
     line = call(join_kernel, None, [resident(x) for x in (pay, a1, a2, a3)], kept(S((PAY, 4 * rows), bf)), 10**7)
     b1 = lax.ppermute(line, "sp", along(1, True))
     b2 = lax.ppermute(line, "sp", along(-1, True))
-    cut = PAY // 2
+    cut = 160
     b3 = lax.ppermute(b1[:cut], "sp", along(1, True))
     b4 = lax.ppermute(b2[cut:], "sp", along(-1, True))
 
@@ -424,7 +425,7 @@
         [q_other, pool_in, outer, w_pool_mix[0], pool_scale[None, :], w_attn_out, w_pool_out],
         [S((rows, 256), bf), S((512, 512), bf)] + [S((448, 512), bf)] * 3,
         10**8,
-        [pltpu.VMEM((rows + 2 * REACH, 256), f32)] * 4,
+        [pltpu.VMEM((rows + 3 * REACH, 256), f32)] * 4,
     )
     packs = [lax.ppermute(packs[d - 1], "tp", ring(d)) for d in (1, 2, 3)]
     swapped = [lax.ppermute(p, "sp", SWAP) for p in packs]

time: 110 us -> 110 us (level)
  transfers between devices with their start and end apart: 25 -> 25, of which waited for: 11 -> 11; matrix products, arithmetic and copies ran while one was open for 3% -> 3% of each run, Pallas kernels for 28% -> 27%
where the time goes in v4:
time: 110 us; the launch traced here: 109 us
  starting transfers between devices  49.2 us (45%)
  Pallas kernels  32.4 us (29%)
  waiting for transfers between devices  23.5 us (21%)
  other arithmetic  2.73 us (2%)
  local copies, waits for them, and re-layouts  1.15 us (1%)
    pallas_call x13, Pallas kernels, call(): pl.pallas_call(kernel, in_specs=[SM] * len(first) + [pl.BlockSpec(memory_...  32.4 us
    ppermute x3, starting transfers between devices, whole(): swapped = [lax.ppermute(p, 'sp', SWAP) for p in packs]  14.5 us
    ppermute x1, starting transfers between devices, whole(): b4 = lax.ppermute(b2[cut:], 'sp', along(-1, True))  8.43 us
    ppermute x3, waiting for transfers between devices, whole(): attns = [attn] + [lax.ppermute(attn, 'tp', ring(d)) for d in (1, 2, 3)]  7.46 us
    ppermute x1, waiting for transfers between devices, whole(): a2 = lax.ppermute(pay, 'sp', along(-1, False))  4.57 us
    ppermute x1, starting transfers between devices, whole(): a3 = lax.ppermute(pay, 'sp', along(2, False))  4.07 us
    ppermute x1, starting transfers between devices, whole(): b2 = lax.ppermute(line, 'sp', along(-1, True))  3.98 us
    ppermute x3, starting transfers between devices, whole(): attns = [attn] + [lax.ppermute(attn, 'tp', ring(d)) for d in (1, 2, 3)]  3.36 us
  transfers between devices with their start and end apart: 25, of which 11 were waited for; matrix products, arithmetic and copies ran while one was open for 3% of the time, Pallas kernels for 27%

profile of v4, /device:TPU:0, one launch (start us, length us, event | category | flops | bytes accessed | tf_op | source)
XLA Modules:
  0.0 109.2 jit_solution(16793796911451694613)
XLA Ops:
  1.1 1.7 %collective-permute-start.4 = (bf16[192,512]{1,0:T(8,128)(2,1)S(1)}, bf16[192,512]{1,0:T(8,128)(2,1)S(1)}, u32[]{:S(2)}, u32[]{:S(2)}) collective-permute-start(bf16[192,512]{1,0:T(8,128)(2,1)S(1)} %get-tuple-element.77), channel_id=1, source_target_pairs={{0,1},{1,2},{2,3},{3,0},{4,5},{5,6},{6,7},{7,4},{8,9},{9,10},{10,1... | collective-permute-start | bytes 589832 | tf_op jit(solution)/shard_map/ppermute | solution.py:352
  2.7 1.6 %collective-permute-start.2 = (bf16[192,512]{1,0:T(8,128)(2,1)S(1)}, bf16[192,512]{1,0:T(8,128)(2,1)S(1)}, u32[]{:S(2)}, u32[]{:S(2)}) collective-permute-start(bf16[192,512]{1,0:T(8,128)(2,1)S(1)} %get-tuple-element.77), channel_id=1, source_target_pairs={{0,3},{1,0},{2,1},{3,2},{4,7},{5,4},{6,5},{7,6},{8,11},{9,8},{10,9... | collective-permute-start | bytes 589832 | tf_op jit(solution)/shard_map/ppermute | solution.py:351
  4.4 1.7 %collective-permute-start.5 = (bf16[192,512]{1,0:T(8,128)(2,1)S(1)}, bf16[192,512]{1,0:T(8,128)(2,1)S(1)}, u32[]{:S(2)}, u32[]{:S(2)}) collective-permute-start(bf16[192,512]{1,0:T(8,128)(2,1)S(1)} %get-tuple-element.78), channel_id=1, source_target_pairs={{0,3},{1,0},{2,1},{3,2},{4,7},{5,4},{6,5},{7,6},{8,11},{9,8},{10,9... | collective-permute-start | bytes 589832 | tf_op jit(solution)/shard_map/ppermute | solution.py:353
  8.3 2.2 %collective-permute-done.2.x2b = bf16[192,512]{1,0:T(8,128)(2,1)S(1)} collective-permute-done((bf16[192,512]{1,0:T(8,128)(2,1)S(1)}, bf16[192,512]{1,0:T(8,128)(2,1)S(1)}, u32[]{:S(2)}, u32[]{:S(2)}) %collective-permute-start.2) | collective-permute-done | bytes 196640 | tf_op jit(solution)/shard_map/ppermute | solution.py:351
  10.5 2.8 %collective-permute-start.3 = (bf16[192,512]{1,0:T(8,128)(2,1)S(1)}, bf16[192,512]{1,0:T(8,128)(2,1)S(1)}, u32[]{:S(2)}, u32[]{:S(2)}) collective-permute-start(bf16[192,512]{1,0:T(8,128)(2,1)S(1)} %collective-permute-done.2.x2b), channel_id=1, source_target_pairs={{0,3},{1,0},{2,1},{3,2},{4,7},{5,4},{6,5},{7,6},{8,11},{9,8},{10,9... | collective-permute-start | bytes 589832 | tf_op jit(solution)/shard_map/ppermute | solution.py:355
  14.4 2.5 %shard_map.181 = (bf16[2048,256]{1,0:T(8,128)(2,1)S(1)}, bf16[32,2048]{1,0:T(8,128)(2,1)S(1)}, bf16[2048,512]{1,0:T(8,128)(2,1)S(1)}, bf16[2048,256]{1,0:T(8,128...) custom-call(bf16[2048,256]{1,0:T(8,128)(2,1)} %refs_0_.1, ...), custom_call_target="tpu_custom_call" | custom-call | flops 400000000 | bytes 1048576 | tf_op jit(solution)/shard_map/pallas_call | solution.py:310
  16.9 2.3 %shard_map.182 = (f32[384,128]{1,0:T(8,128)S(1)}, f32[384,256]{1,0:T(8,128)S(1)}, f32[32,384]{1,0:T(8,128)S(1)}, f32[384,512]{1,0:T(8,128)S(1)}, f32[384,256]{1,0:T(8,128)S(1)}) custom-call(s32[11]{0:T(128)S(1)} %copy-done.7, bf16[384,512]{1,0:T(8,128)(2,1)S(1)} %get-tuple-element.46.x0, bf16[192,512]{1,0:T(8,128)(2,1)S(1)} %collective-permute-done.x1a, ...), custom_call_target="tpu_custom_call" | custom-call | flops 1600000000 | bytes 1048576 | tf_op jit(solution)/shard_map/pallas_call | solution.py:310
  21.3 4.1 %collective-permute-start.9 = (bf16[304,384]{1,0:T(8,128)(2,1)S(1)}, bf16[304,384]{1,0:T(8,128)(2,1)S(1)}, u32[]{:S(2)}, u32[]{:S(2)}) collective-permute-start(bf16[304,384]{1,0:T(8,128)(2,1)S(1)} %get-tuple-element.59.a), channel_id=1, source_target_pairs={{0,64},{4,20},{8,72},{12,28},{16,80},{20,4},{24,88},{28,12},{32,96... | collective-permute-start | bytes 700424 | tf_op jit(solution)/shard_map/ppermute | solution.py:398
  27.4 2.0 %collective-permute-done.9.d = bf16[304,384]{1,0:T(8,128)(2,1)S(1)} collective-permute-done((bf16[304,384]{1,0:T(8,128)(2,1)S(1)}, bf16[304,384]{1,0:T(8,128)(2,1)S(1)}, u32[]{:S(2)}, u32[]{:S(2)}) %collective-permute-start.9) | collective-permute-done | bytes 233504 | tf_op jit(solution)/shard_map/ppermute | solution.py:398
  29.4 4.6 %collective-permute-done.8.c = bf16[304,384]{1,0:T(8,128)(2,1)S(1)} collective-permute-done((bf16[304,384]{1,0:T(8,128)(2,1)S(1)}, bf16[304,384]{1,0:T(8,128)(2,1)S(1)}, u32[]{:S(2)}, u32[]{:S(2)}) %collective-permute-start.8) | collective-permute-done | bytes 233504 | tf_op jit(solution)/shard_map/ppermute | solution.py:397
  34.1 4.0 %collective-permute-start.12 = (bf16[304,1536]{1,0:T(8,128)(2,1)S(1)}, bf16[304,1536]{1,0:T(8,128)(2,1)S(1)}, u32[]{:S(2)}, u32[]{:S(2)}) collective-permute-start(bf16[304,1536]{1,0:T(8,128)(2,1)S(1)} %shard_map.185.refs_4_), channel_id=1, source_target_pairs={{0,24},{4,100},{8,0},{12,108},{16,8},{20,116},{24,16},{28,124},{32... | collective-permute-start | bytes 2801672 | tf_op jit(solution)/shard_map/ppermute | solution.py:417
  38.1 1.7 %shard_map.184 = (bf16[400,384]{1,0:T(8,128)(2,1)S(1)}, bf16[384,256]{1,0:T(8,128)(2,1)S(1)}, bf16[16,256]{1,0:T(8,128)(2,1)S(1)}) custom-call(s32[11]{0:T(128)S(1)} %copy-done.7, bf16[192,512]{1,0:T(8,128)(2,1)S(1)} %collective-permute-done.1.xa, bf16[192,512]{1,0:T(8,128)(2,1)S(1)} %collective-permute-done.3.xb, f32[1,2048]{1,0:T(1,128)S(1)} %get-tuple-element.41.gain, ...), custom_call_target="tpu_custom_call" | custom-call | flops 1000000000 | bytes 1048576 | tf_op jit(solution)/shard_map/pallas_call | solution.py:310
  42.8 3.1 %collective-permute-start.20 = (bf16[448,512]{1,0:T(8,128)(2,1)S(1)}, bf16[448,512]{1,0:T(8,128)(2,1)S(1)}, u32[]{:S(2)}, u32[]{:S(2)}) collective-permute-start(bf16[448,512]{1,0:T(8,128)(2,1)S(1)} %get-tuple-element.71), channel_id=1, source_target_pairs={{0,2},{1,3},{2,0},{3,1},{4,6},{5,7},{6,4},{7,5},{8,10},{9,11},{10,... | collective-permute-start | bytes 1376264 | tf_op jit(solution)/shard_map/ppermute | solution.py:430
  46.1 4.6 %shard_map.186 = (f32[4,80,384]{2,1,0:T(8,128)S(1)}, f32[4,80,384]{2,1,0:T(8,128)S(1)}) custom-call(bf16[400,384]{1,0:T(8,128)(2,1)S(1)} %get-tuple-element.58.refs_0_, bf16[400,384]{1,0:T(8,128)(2,1)S(1)} %collective-permute-done.6.refs_1_.inner, bf16[256,512]{1,0:T(8,128)(2,1)S(1)} %copy-done.9, f32[512,1]{1,0:T(8,128)S(1)} %get-tuple-element.50.gains.refs_3_, ...), custom_call_target="tpu_custom_call" | custom-call | flops 4831838208 | bytes 1048576 | tf_op jit(solution)/shard_map/pallas_call | solution.py:310
  50.7 2.8 %collective-permute-done.19.f1 = bf16[448,512]{1,0:T(8,128)(2,1)S(1)} collective-permute-done((bf16[448,512]{1,0:T(8,128)(2,1)S(1)}, bf16[448,512]{1,0:T(8,128)(2,1)S(1)}, u32[]{:S(2)}, u32[]{:S(2)}) %collective-permute-start.19) | collective-permute-done | bytes 458784 | tf_op jit(solution)/shard_map/ppermute | solution.py:430
  53.5 13.6 %collective-permute-start.22 = (bf16[448,512]{1,0:T(8,128)(2,1)S(1)}, bf16[448,512]{1,0:T(8,128)(2,1)S(1)}, u32[]{:S(2)}, u32[]{:S(2)}) collective-permute-start(bf16[448,512]{1,0:T(8,128)(2,1)S(1)} %collective-permute-done.19.f1), channel_id=1, source_target_pairs={{0,4},{4,0},{8,12},{12,8},{16,20},{20,16},{24,28},{28,24},{32,36},... | collective-permute-start | bytes 1376264 | tf_op jit(solution)/shard_map/ppermute | solution.py:431
  68.0 8.4 %collective-permute-start.13 = (bf16[144,1536]{1,0:T(8,128)(2,1)S(1)}, bf16[144,1536]{1,0:T(8,128)(2,1)S(1)}, u32[]{:S(2)}, u32[]{:S(2)}) collective-permute-start(bf16[144,1536]{1,0:T(8,128)(2,1)S(1)} %slice.17), channel_id=1, source_target_pairs={{0,24},{4,100},{8,0},{12,108},{16,8},{20,116},{24,16},{28,124},{32... | collective-permute-start | bytes 1327112 | tf_op jit(solution)/shard_map/ppermute | solution.py:420
  76.8 9.1 %shard_map.187 = (f32[4,80,384]{2,1,0:T(8,128)S(1)}, f32[4,80,384]{2,1,0:T(8,128)S(1)}) custom-call(bf16[400,384]{1,0:T(8,128)(2,1)S(1)} %get-tuple-element.58.refs_0_, bf16[400,384]{1,0:T(8,128)(2,1)S(1)} %collective-permute-done.6.refs_1_.inner, bf16[256,512]{1,0:T(8,128)(2,1)S(1)} %copy-done.9, f32[512,1]{1,0:T(8,128)S(1)} %get-tuple-element.50.gains.refs_3_, ...), custom_call_target="tpu_custom_call" | custom-call | flops 9663676416 | bytes 1048576 | tf_op jit(solution)/shard_map/pallas_call | solution.py:310
  86.8 4.9 %shard_map.188 = (f32[4,80,384]{2,1,0:T(8,128)S(1)}, bf16[4,80,384]{2,1,0:T(8,128)(2,1)S(1)}) custom-call(bf16[400,384]{1,0:T(8,128)(2,1)S(1)} %get-tuple-element.58.refs_0_, bf16[400,384]{1,0:T(8,128)(2,1)S(1)} %collective-permute-done.6.refs_1_.inner, bf16[256,512]{1,0:T(8,128)(2,1)S(1)} %copy-done.9, f32[512,1]{1,0:T(8,128)S(1)} %get-tuple-element.50.gains.refs_3_, ...), custom_call_target="tpu_custom_call" | custom-call | flops 4831838208 | bytes 1048576 | tf_op jit(solution)/shard_map/pallas_call | solution.py:310
  91.8 1.5 %collective-permute-done.14.other = bf16[4,80,384]{2,1,0:T(8,128)(2,1)S(1)} collective-permute-done((bf16[4,80,384]{2,1,0:T(8,128)(2,1)S(1)}, bf16[4,80,384]{2,1,0:T(8,128)(2,1)S(1)}, u32[]{:S(2)}, u32[]{:S(2)}) %collective-permute-start.14) | collective-permute-done | bytes 245792 | tf_op jit(solution)/shard_map/ppermute | solution.py:445
  93.4 2.4 %collective-permute-start.17 = (bf16[256,384]{1,0:T(8,128)(2,1)S(1)}, bf16[256,384]{1,0:T(8,128)(2,1)S(1)}, u32[]{:S(2)}, u32[]{:S(2)}) collective-permute-start(bf16[256,384]{1,0:T(8,128)(2,1)S(1)} %shard_map.189.attn), channel_id=1, source_target_pairs={{0,3},{1,0},{2,1},{3,2},{4,7},{5,4},{6,5},{7,6},{8,11},{9,8},{10,9... | collective-permute-start | bytes 589832 | tf_op jit(solution)/shard_map/ppermute | solution.py:447
  96.8 2.4 %shard_map.191 = (f32[384,512]{1,0:T(8,128)S(1)}, f32[384,512]{1,0:T(8,128)S(1)}) custom-call(s32[11]{0:T(128)S(1)} %copy-done.7, bf16[384,512]{1,0:T(8,128)(2,1)S(1)} %copy-done, bf16[192,512]{1,0:T(8,128)(2,1)S(1)} %collective-permute-done.x1a, bf16[192,512]{1,0:T(8,128)(2,1)S(1)} %collective-permute-done.4.x1b, ...), custom_call_target="tpu_custom_call" | custom-call | flops 500000000 | bytes 1048576 | tf_op jit(solution)/shard_map/pallas_call | solution.py:310
  100.4 4.1 %collective-permute-done.17.a3 = bf16[256,384]{1,0:T(8,128)(2,1)S(1)} collective-permute-done((bf16[256,384]{1,0:T(8,128)(2,1)S(1)}, bf16[256,384]{1,0:T(8,128)(2,1)S(1)}, u32[]{:S(2)}, u32[]{:S(2)}) %collective-permute-start.17) | collective-permute-done | bytes 196640 | tf_op jit(solution)/shard_map/ppermute | solution.py:447
  105.1 2.8 %collective-permute-done.15.a1 = bf16[256,384]{1,0:T(8,128)(2,1)S(1)} collective-permute-done((bf16[256,384]{1,0:T(8,128)(2,1)S(1)}, bf16[256,384]{1,0:T(8,128)(2,1)S(1)}, u32[]{:S(2)}, u32[]{:S(2)}) %collective-permute-start.15) | collective-permute-done | bytes 196640 | tf_op jit(solution)/shard_map/ppermute | solution.py:447
  (68 shorter events, 18.2 us)
Async XLA Ops:
  1.1 15.9 %collective-permute-start.4 = (bf16[192,512]{1,0:T(8,128)(2,1)S(1)}, bf16[192,512]{1,0:T(8,128)(2,1)S(1)}, u32[]{:S(2)}, u32[]{:S(2)}) collective-permute-start(bf16[192,512]{1,0:T(8,128)(2,1)S(1)} %get-tuple-element.77), channel_id=1, source_target_pairs={{0,1},{1,2},{2,3},{3,0},{4,5},{5,6},{6,7},{7,4},{8,9},{9,10},{10,1... | collective-permute-start | bytes 589832 | tf_op jit(solution)/shard_map/ppermute | solution.py:352
  2.7 7.8 %collective-permute-start.2 = (bf16[192,512]{1,0:T(8,128)(2,1)S(1)}, bf16[192,512]{1,0:T(8,128)(2,1)S(1)}, u32[]{:S(2)}, u32[]{:S(2)}) collective-permute-start(bf16[192,512]{1,0:T(8,128)(2,1)S(1)} %get-tuple-element.77), channel_id=1, source_target_pairs={{0,3},{1,0},{2,1},{3,2},{4,7},{5,4},{6,5},{7,6},{8,11},{9,8},{10,9... | collective-permute-start | bytes 589832 | tf_op jit(solution)/shard_map/ppermute | solution.py:351
  4.4 12.6 %collective-permute-start.5 = (bf16[192,512]{1,0:T(8,128)(2,1)S(1)}, bf16[192,512]{1,0:T(8,128)(2,1)S(1)}, u32[]{:S(2)}, u32[]{:S(2)}) collective-permute-start(bf16[192,512]{1,0:T(8,128)(2,1)S(1)} %get-tuple-element.78), channel_id=1, source_target_pairs={{0,3},{1,0},{2,1},{3,2},{4,7},{5,4},{6,5},{7,6},{8,11},{9,8},{10,9... | collective-permute-start | bytes 589832 | tf_op jit(solution)/shard_map/ppermute | solution.py:353
  6.0 7.3 %collective-permute-start = (bf16[192,512]{1,0:T(8,128)(2,1)S(1)}, bf16[192,512]{1,0:T(8,128)(2,1)S(1)}, u32[]{:S(2)}, u32[]{:S(2)}) collective-permute-start(bf16[192,512]{1,0:T(8,128)(2,1)S(1)} %get-tuple-element.78), channel_id=1, source_target_pairs={{0,1},{1,2},{2,3},{3,0},{4,5},{5,6},{6,7},{7,4},{8,9},{9,10},{10,1... | collective-permute-start | bytes 589832 | tf_op jit(solution)/shard_map/ppermute | solution.py:350
  10.5 8.7 %collective-permute-start.3 = (bf16[192,512]{1,0:T(8,128)(2,1)S(1)}, bf16[192,512]{1,0:T(8,128)(2,1)S(1)}, u32[]{:S(2)}, u32[]{:S(2)}) collective-permute-start(bf16[192,512]{1,0:T(8,128)(2,1)S(1)} %collective-permute-done.2.x2b), channel_id=1, source_target_pairs={{0,3},{1,0},{2,1},{3,2},{4,7},{5,4},{6,5},{7,6},{8,11},{9,8},{10,9... | collective-permute-start | bytes 589832 | tf_op jit(solution)/shard_map/ppermute | solution.py:355
  13.3 6.9 %collective-permute-start.1 = (bf16[192,512]{1,0:T(8,128)(2,1)S(1)}, bf16[192,512]{1,0:T(8,128)(2,1)S(1)}, u32[]{:S(2)}, u32[]{:S(2)}) collective-permute-start(bf16[192,512]{1,0:T(8,128)(2,1)S(1)} %collective-permute-done.x1a), channel_id=1, source_target_pairs={{0,1},{1,2},{2,3},{3,0},{4,5},{5,6},{6,7},{7,4},{8,9},{9,10},{10,1... | collective-permute-start | bytes 589832 | tf_op jit(solution)/shard_map/ppermute | solution.py:354
  21.3 8.1 %collective-permute-start.9 = (bf16[304,384]{1,0:T(8,128)(2,1)S(1)}, bf16[304,384]{1,0:T(8,128)(2,1)S(1)}, u32[]{:S(2)}, u32[]{:S(2)}) collective-permute-start(bf16[304,384]{1,0:T(8,128)(2,1)S(1)} %get-tuple-element.59.a), channel_id=1, source_target_pairs={{0,64},{4,20},{8,72},{12,28},{16,80},{20,4},{24,88},{28,12},{32,96... | collective-permute-start | bytes 700424 | tf_op jit(solution)/shard_map/ppermute | solution.py:398
  25.4 8.6 %collective-permute-start.8 = (bf16[304,384]{1,0:T(8,128)(2,1)S(1)}, bf16[304,384]{1,0:T(8,128)(2,1)S(1)}, u32[]{:S(2)}, u32[]{:S(2)}) collective-permute-start(bf16[304,384]{1,0:T(8,128)(2,1)S(1)} %get-tuple-element.59.a), channel_id=1, source_target_pairs={{0,96},{4,28},{8,104},{12,4},{16,112},{20,12},{24,120},{28,20},{32... | collective-permute-start | bytes 700424 | tf_op jit(solution)/shard_map/ppermute | solution.py:397
  26.1 7.9 %collective-permute-start.7 = (bf16[304,384]{1,0:T(8,128)(2,1)S(1)}, bf16[304,384]{1,0:T(8,128)(2,1)S(1)}, u32[]{:S(2)}, u32[]{:S(2)}) collective-permute-start(bf16[304,384]{1,0:T(8,128)(2,1)S(1)} %get-tuple-element.59.a), channel_id=1, source_target_pairs={{0,32},{4,12},{8,40},{12,20},{16,48},{20,28},{24,56},{28,4},{32,64... | collective-permute-start | bytes 700424 | tf_op jit(solution)/shard_map/ppermute | solution.py:396
  34.1 33.9 %collective-permute-start.12 = (bf16[304,1536]{1,0:T(8,128)(2,1)S(1)}, bf16[304,1536]{1,0:T(8,128)(2,1)S(1)}, u32[]{:S(2)}, u32[]{:S(2)}) collective-permute-start(bf16[304,1536]{1,0:T(8,128)(2,1)S(1)} %shard_map.185.refs_4_), channel_id=1, source_target_pairs={{0,24},{4,100},{8,0},{12,108},{16,8},{20,116},{24,16},{28,124},{32... | collective-permute-start | bytes 2801672 | tf_op jit(solution)/shard_map/ppermute | solution.py:417
  38.0 38.4 %collective-permute-start.10 = (bf16[304,1536]{1,0:T(8,128)(2,1)S(1)}, bf16[304,1536]{1,0:T(8,128)(2,1)S(1)}, u32[]{:S(2)}, u32[]{:S(2)}) collective-permute-start(bf16[304,1536]{1,0:T(8,128)(2,1)S(1)} %shard_map.185.refs_4_), channel_id=1, source_target_pairs={{0,8},{4,36},{8,16},{12,44},{16,24},{20,52},{24,0},{28,60},{32,40}... | collective-permute-start | bytes 2801672 | tf_op jit(solution)/shard_map/ppermute | solution.py:416
  39.8 1.7 %collective-permute-start.6 = (bf16[400,384]{1,0:T(8,128)(2,1)S(1)}, bf16[400,384]{1,0:T(8,128)(2,1)S(1)}, u32[]{:S(2)}, u32[]{:S(2)}) collective-permute-start(bf16[400,384]{1,0:T(8,128)(2,1)S(1)} %get-tuple-element.58.refs_0_), channel_id=1, source_target_pairs={{0,4},{4,0},{8,12},{12,8},{16,20},{20,16},{24,28},{28,24},{32,36},... | collective-permute-start | bytes 921608 | tf_op jit(solution)/shard_map/ppermute | solution.py:408
  42.8 10.8 %collective-permute-start.19 = (bf16[448,512]{1,0:T(8,128)(2,1)S(1)}, bf16[448,512]{1,0:T(8,128)(2,1)S(1)}, u32[]{:S(2)}, u32[]{:S(2)}) collective-permute-start(bf16[448,512]{1,0:T(8,128)(2,1)S(1)} %get-tuple-element.70), channel_id=1, source_target_pairs={{0,1},{1,2},{2,3},{3,0},{4,5},{5,6},{6,7},{7,4},{8,9},{9,10},{10,1... | collective-permute-start | bytes 1376264 | tf_op jit(solution)/shard_map/ppermute | solution.py:430
  42.8 24.2 %collective-permute-start.20 = (bf16[448,512]{1,0:T(8,128)(2,1)S(1)}, bf16[448,512]{1,0:T(8,128)(2,1)S(1)}, u32[]{:S(2)}, u32[]{:S(2)}) collective-permute-start(bf16[448,512]{1,0:T(8,128)(2,1)S(1)} %get-tuple-element.71), channel_id=1, source_target_pairs={{0,2},{1,3},{2,0},{3,1},{4,6},{5,7},{6,4},{7,5},{8,10},{9,11},{10,... | collective-permute-start | bytes 1376264 | tf_op jit(solution)/shard_map/ppermute | solution.py:430
  45.9 21.2 %collective-permute-start.21 = (bf16[448,512]{1,0:T(8,128)(2,1)S(1)}, bf16[448,512]{1,0:T(8,128)(2,1)S(1)}, u32[]{:S(2)}, u32[]{:S(2)}) collective-permute-start(bf16[448,512]{1,0:T(8,128)(2,1)S(1)} %get-tuple-element.72), channel_id=1, source_target_pairs={{0,3},{1,0},{2,1},{3,2},{4,7},{5,4},{6,5},{7,6},{8,11},{9,8},{10,9... | collective-permute-start | bytes 1376264 | tf_op jit(solution)/shard_map/ppermute | solution.py:430
  53.5 42.3 %collective-permute-start.22 = (bf16[448,512]{1,0:T(8,128)(2,1)S(1)}, bf16[448,512]{1,0:T(8,128)(2,1)S(1)}, u32[]{:S(2)}, u32[]{:S(2)}) collective-permute-start(bf16[448,512]{1,0:T(8,128)(2,1)S(1)} %collective-permute-done.19.f1), channel_id=1, source_target_pairs={{0,4},{4,0},{8,12},{12,8},{16,20},{20,16},{24,28},{28,24},{32,36},... | collective-permute-start | bytes 1376264 | tf_op jit(solution)/shard_map/ppermute | solution.py:431
  67.1 32.1 %collective-permute-start.23 = (bf16[448,512]{1,0:T(8,128)(2,1)S(1)}, bf16[448,512]{1,0:T(8,128)(2,1)S(1)}, u32[]{:S(2)}, u32[]{:S(2)}) collective-permute-start(bf16[448,512]{1,0:T(8,128)(2,1)S(1)} %collective-permute-done.20.f2), channel_id=1, source_target_pairs={{0,4},{4,0},{8,12},{12,8},{16,20},{20,16},{24,28},{28,24},{32,36},... | collective-permute-start | bytes 1376264 | tf_op jit(solution)/shard_map/ppermute | solution.py:431
  67.1 32.1 %collective-permute-start.24 = (bf16[448,512]{1,0:T(8,128)(2,1)S(1)}, bf16[448,512]{1,0:T(8,128)(2,1)S(1)}, u32[]{:S(2)}, u32[]{:S(2)}) collective-permute-start(bf16[448,512]{1,0:T(8,128)(2,1)S(1)} %collective-permute-done.21.f3), channel_id=1, source_target_pairs={{0,4},{4,0},{8,12},{12,8},{16,20},{20,16},{24,28},{28,24},{32,36},... | collective-permute-start | bytes 1376264 | tf_op jit(solution)/shard_map/ppermute | solution.py:431
  68.0 17.8 %collective-permute-start.13 = (bf16[144,1536]{1,0:T(8,128)(2,1)S(1)}, bf16[144,1536]{1,0:T(8,128)(2,1)S(1)}, u32[]{:S(2)}, u32[]{:S(2)}) collective-permute-start(bf16[144,1536]{1,0:T(8,128)(2,1)S(1)} %slice.17), channel_id=1, source_target_pairs={{0,24},{4,100},{8,0},{12,108},{16,8},{20,116},{24,16},{28,124},{32... | collective-permute-start | bytes 1327112 | tf_op jit(solution)/shard_map/ppermute | solution.py:420
  76.5 10.3 %collective-permute-start.11 = (bf16[160,1536]{1,0:T(8,128)(2,1)S(1)}, bf16[160,1536]{1,0:T(8,128)(2,1)S(1)}, u32[]{:S(2)}, u32[]{:S(2)}) collective-permute-start(bf16[160,1536]{1,0:T(8,128)(2,1)S(1)} %slice.16), channel_id=1, source_target_pairs={{0,8},{4,36},{8,16},{12,44},{16,24},{20,52},{24,0},{28,60},{32,40}... | collective-permute-start | bytes 1474568 | tf_op jit(solution)/shard_map/ppermute | solution.py:419
  91.7 1.6 %collective-permute-start.14 = (bf16[4,80,384]{2,1,0:T(8,128)(2,1)S(1)}, bf16[4,80,384]{2,1,0:T(8,128)(2,1)S(1)}, u32[]{:S(2)}, u32[]{:S(2)}) collective-permute-start(bf16[4,80,384]{2,1,0:T(8,128)(2,1)S(1)} %get-tuple-element.65), channel_id=1, source_target_pairs={{0,4},{4,0},{8,12},{12,8},{16,20},{20,16},{24,28},{28,24},{32,36},... | collective-permute-start | bytes 737288 | tf_op jit(solution)/shard_map/ppermute | solution.py:445
  93.4 11.1 %collective-permute-start.17 = (bf16[256,384]{1,0:T(8,128)(2,1)S(1)}, bf16[256,384]{1,0:T(8,128)(2,1)S(1)}, u32[]{:S(2)}, u32[]{:S(2)}) collective-permute-start(bf16[256,384]{1,0:T(8,128)(2,1)S(1)} %shard_map.189.attn), channel_id=1, source_target_pairs={{0,3},{1,0},{2,1},{3,2},{4,7},{5,4},{6,5},{7,6},{8,11},{9,8},{10,9... | collective-permute-start | bytes 589832 | tf_op jit(solution)/shard_map/ppermute | solution.py:447
  95.8 9.3 %collective-permute-start.16 = (bf16[256,384]{1,0:T(8,128)(2,1)S(1)}, bf16[256,384]{1,0:T(8,128)(2,1)S(1)}, u32[]{:S(2)}, u32[]{:S(2)}) collective-permute-start(bf16[256,384]{1,0:T(8,128)(2,1)S(1)} %shard_map.189.attn), channel_id=1, source_target_pairs={{0,2},{1,3},{2,0},{3,1},{4,6},{5,7},{6,4},{7,5},{8,10},{9,11},{10,... | collective-permute-start | bytes 589832 | tf_op jit(solution)/shard_map/ppermute | solution.py:447
  95.8 12.1 %collective-permute-start.15 = (bf16[256,384]{1,0:T(8,128)(2,1)S(1)}, bf16[256,384]{1,0:T(8,128)(2,1)S(1)}, u32[]{:S(2)}, u32[]{:S(2)}) collective-permute-start(bf16[256,384]{1,0:T(8,128)(2,1)S(1)} %shard_map.189.attn), channel_id=1, source_target_pairs={{0,1},{1,2},{2,3},{3,0},{4,5},{5,6},{6,7},{7,4},{8,9},{9,10},{10,1... | collective-permute-start | bytes 589832 | tf_op jit(solution)/shard_map/ppermute | solution.py:447
  (11 other events, 63.0 us)
